TPU v7x, 1024 devices: a 2x16x16 block of a 4x16x16 slice. The times are simulated.
1024 devices in a mesh: grp: 2 (over x), sp: 16 (over z), tp: 32 (over y, core).
Axes of the slice: x: 2, y: 16, z: 16, core: 2. Of those that a mesh axis runs over, the one named last changes fastest.
The devices are a block of a 4x16x16 slice.
Arguments:
- prompt_layer_input: bfloat16 [24, 2048, 2048], P('grp', 'sp'), parts along dimension 0, may hold values from -10 to 10
- next_token_input: bfloat16 [24, 2048], P('grp'), parts along dimension 0, may hold values from -6 to 6
- value_projection: bfloat16 [2048, 2048], P(None, 'tp'), may hold values from -0.125 to 0.125
- output_gate_matrix: bfloat16 [2048, 2048], P(None, 'tp'), may hold values from -0.125 to 0.125
- key_projection: bfloat16 [2048, 256], replicated, may hold values from -0.0390625 to 0.0390625
- query_projection: bfloat16 [2048, 256], replicated, may hold values from -0.125 to 0.125
- step_projection: bfloat16 [2048, 32], replicated, may hold values from -0.125 to 0.125
- value_filter_taps: bfloat16 [4, 2048], replicated, may hold values from -3 to 3
- key_filter_taps: bfloat16 [4, 256], replicated, may hold values from -3 to 3
- query_filter_taps: bfloat16 [4, 256], replicated, may hold values from -3 to 3
- step_size_bias: float32 [32], replicated, may hold values from -4.3 to -0.7
- head_decay_logarithm: float32 [32], replicated, may hold values from -8.5 to -0.5
- direct_path_weight: float32 [32], replicated, may hold values from 0.1 to 1.9
- gated_norm_gain: float32 [32, 64], replicated, may hold values from 0.1 to 1.9
- position_decay_offset: float32 [24, 2048, 32], P('grp', 'sp'), parts along dimension 0, may hold values from -2.1 to 0
Outputs:
- state_cache: bfloat16 [24, 32, 64, 128], P('grp', 'tp', 'sp'), parts along dimension 0
- first_read: bfloat16 [24, 32, 64], P('grp', 'tp', 'sp'), parts along dimension 0
There are 2 independent parts, one for each index of `grp`. A program takes and returns all parts, laid end to end along the dimension named above; an argument that names none is the same for every part. Nothing has to cross between parts.
All inputs are finite; a program needn't handle non-finite values.
Results may differ from a plain program's by a relative error of at most 0.011.
Values may be sent and summed in bfloat16 or wider, within the bound.
No kernel may reach another device: no remote copies, remote signals or barrier semaphores. Data moves between devices by JAX's collectives and lax.ppermute only.
A program may use at most 32 MiB of HBM per device.

v0:
```python
import functools

import jax
import jax.numpy as jnp
from jax import lax
from jax.sharding import Mesh
from jax.sharding import PartitionSpec as P

HEADS = 32
P_SIZE = 64
GROUPS = 2
STATE = 128
CONV = 4
SPAN = 64
TP = ("tp_0", "tp_1")
SP_TP = ("sp", "tp_0", "tp_1")


epsilon = 1e-06


def joined_along(tiles, dim):
    shape = list(tiles.shape[1:])
    shape[dim] *= tiles.shape[0]
    return jnp.moveaxis(tiles, 0, dim).reshape(shape)


def sent_to_all(shard, axis):
    length = lax.axis_size(axis)
    return lax.all_to_all(
        jnp.broadcast_to(shard[None], (length, *shard.shape)), axis, 0, 0, tiled=True
    )


def gather_directly(shard, axis, dim):
    return joined_along(sent_to_all(shard, axis), dim)


def one_axis_at_a_time(shard, axes):
    return functools.reduce(lax.psum, axes, shard)


def shards(
    prompt_layer_input,
    next_token_input,
    value_projection,
    output_gate_matrix,
    key_projection,
    query_projection,
    step_projection,
    value_filter_taps,
    key_filter_taps,
    query_filter_taps,
    step_size_bias,
    head_decay_logarithm,
    direct_path_weight,
    gated_norm_gain,
    position_decay_offset,
):
    seq_count, local_len, width = prompt_layer_input.shape
    resident_heads = value_projection.shape[1] // P_SIZE
    feature_cols = resident_heads * P_SIZE
    shard_count = lax.axis_size("sp")
    rows_here = P_SIZE // shard_count
    shard_index = lax.axis_index("sp")
    leading_head = lax.axis_index(TP) * resident_heads
    group_index = leading_head // (HEADS // GROUPS)
    row_first = shard_index * rows_here
    in_cols = lax.dynamic_slice_in_dim(key_projection, group_index * STATE, STATE, 1)
    out_cols = lax.dynamic_slice_in_dim(query_projection, group_index * STATE, STATE, 1)
    weights_here = jnp.concatenate([value_projection, in_cols, out_cols], axis=1)
    step_cols = lax.dynamic_slice_in_dim(step_projection, leading_head, resident_heads, 1)
    kernel = jnp.concatenate(
        [
            lax.dynamic_slice_in_dim(value_filter_taps, leading_head * P_SIZE, feature_cols, 1),
            lax.dynamic_slice_in_dim(key_filter_taps, group_index * STATE, STATE, 1),
            lax.dynamic_slice_in_dim(query_filter_taps, group_index * STATE, STATE, 1),
        ],
        axis=1,
    ).astype(jnp.float32)
    head_decay_speed = jnp.exp(
        lax.dynamic_slice_in_dim(head_decay_logarithm, leading_head, resident_heads, 0)
    )
    bias_here = lax.dynamic_slice_in_dim(step_size_bias, leading_head, resident_heads, 0)
    skip_here = lax.dynamic_slice_in_dim(direct_path_weight, leading_head, resident_heads, 0)
    gain_here = lax.dynamic_slice(
        gated_norm_gain, (leading_head, row_first), (resident_heads, rows_here)
    )
    token_rows = prompt_layer_input.reshape(seq_count * local_len, width)
    projected = jnp.dot(token_rows, weights_here, preferred_element_type=jnp.float32).astype(
        jnp.bfloat16
    )
    projected = projected.reshape(seq_count, local_len, feature_cols + 2 * STATE)
    trailing = projected[:, local_len - (CONV - 1) :]
    gathered = gather_directly(trailing, "sp", 1)
    previous = lax.dynamic_slice_in_dim(
        gathered, jnp.maximum(shard_index - 1, 0) * (CONV - 1), CONV - 1, 1
    )
    before = jnp.where(shard_index > 0, previous, jnp.zeros_like(previous))
    newest = gathered[:, (shard_count - 1) * (CONV - 1) :]
    padded = jnp.concatenate([before, projected], axis=1)
    total = padded[:, 0:local_len].astype(jnp.float32) * kernel[0]
    for tap in range(1, CONV):
        total = total + padded[:, tap : tap + local_len].astype(jnp.float32) * kernel[tap]
    mixed = jax.nn.silu(total).astype(jnp.bfloat16)
    step_raw = jnp.dot(token_rows, step_cols, preferred_element_type=jnp.float32).astype(
        jnp.bfloat16
    )
    discrete_step = jax.nn.softplus(step_raw.astype(jnp.float32) + bias_here).reshape(
        seq_count, local_len, resident_heads
    )
    decay_spikes = lax.dynamic_slice_in_dim(position_decay_offset, leading_head, resident_heads, 2)
    logarithmic_decay = decay_spikes - head_decay_speed * discrete_step
    block_count = local_len // SPAN
    cumulative = jnp.cumsum(
        logarithmic_decay.reshape(seq_count, block_count, SPAN, resident_heads), axis=2
    )
    decay_weight = jnp.exp(cumulative[:, :, -1:] - cumulative) * discrete_step.reshape(
        seq_count, block_count, SPAN, resident_heads
    )
    head_input = mixed[:, :, :feature_cols].reshape(
        seq_count, block_count, SPAN, resident_heads, P_SIZE
    )
    weighted = (head_input.astype(jnp.float32) * decay_weight[..., None]).astype(jnp.bfloat16)
    in_map = mixed[:, :, feature_cols : feature_cols + STATE].reshape(
        seq_count, block_count, SPAN, STATE
    )
    block_state = jnp.einsum(
        "bcshp,bcsn->bchpn", weighted, in_map, preferred_element_type=jnp.float32
    )
    block_log = cumulative[:, :, -1]
    own_log = jnp.sum(block_log, axis=1)
    after_block = jnp.exp(own_log[:, None] - jnp.cumsum(block_log, axis=1))
    local_state = jnp.sum(after_block[..., None, None] * block_state, axis=1)
    shard_logs = gather_directly(own_log[None], "sp", 0)
    shard_states = lax.all_to_all(local_state[None], "sp", split_axis=3, concat_axis=0, tiled=True)
    later_log = jnp.cumsum(shard_logs[::-1], axis=0)[::-1] - shard_logs
    own_rows = jnp.sum(jnp.exp(later_log)[..., None, None] * shard_states, axis=0)
    state_cache = own_rows.astype(jnp.bfloat16)
    new_raw = jnp.dot(next_token_input, weights_here, preferred_element_type=jnp.float32).astype(
        jnp.bfloat16
    )
    new_step = jnp.dot(next_token_input, step_cols, preferred_element_type=jnp.float32).astype(
        jnp.bfloat16
    )
    new_gate = jnp.dot(
        next_token_input, output_gate_matrix, preferred_element_type=jnp.float32
    ).astype(jnp.bfloat16)
    window = jnp.concatenate([newest, new_raw[:, None]], axis=1)
    new_mixed = jax.nn.silu(jnp.sum(window.astype(jnp.float32) * kernel[None], axis=1)).astype(
        jnp.bfloat16
    )
    new_input = lax.dynamic_slice_in_dim(
        new_mixed[:, :feature_cols].reshape(seq_count, resident_heads, P_SIZE),
        row_first,
        rows_here,
        2,
    ).astype(jnp.float32)
    new_in = new_mixed[:, feature_cols : feature_cols + STATE].astype(jnp.float32)
    new_out = new_mixed[:, feature_cols + STATE :].astype(jnp.float32)
    new_step_size = jax.nn.softplus(new_step.astype(jnp.float32) + bias_here)
    cache_values = lax.optimization_barrier(state_cache).astype(jnp.float32)
    new_state = (
        jnp.exp(-head_decay_speed * new_step_size)[:, :, None, None] * cache_values
        + (new_step_size[:, :, None] * new_input)[..., None] * new_in[:, None, None, :]
    )
    readout = (
        jnp.sum(new_state * new_out[:, None, None, :], axis=-1)
        + skip_here[None, :, None] * new_input
    )
    gate_rows = lax.dynamic_slice_in_dim(
        new_gate.reshape(seq_count, resident_heads, P_SIZE), row_first, rows_here, 2
    )
    gated = readout * jax.nn.silu(gate_rows.astype(jnp.float32))
    squares = one_axis_at_a_time(jnp.sum(gated * gated, axis=(1, 2)), SP_TP)
    scale = lax.rsqrt(squares / (HEADS * P_SIZE) + epsilon)
    first_read = (gated * scale[:, None, None] * gain_here[None]).astype(jnp.bfloat16)
    return (state_cache, first_read)


def solution(mesh):
    split = Mesh(
        mesh.devices.reshape(mesh.shape["grp"], mesh.shape["sp"], 16, 2),
        ("grp", "sp", "tp_0", "tp_1"),
    )
    return jax.shard_map(
        shards,
        mesh=split,
        in_specs=(
            P("grp", "sp", None),
            P("grp", None),
            P(None, TP),
            P(None, TP),
            P(),
            P(),
            P(),
            P(),
            P(),
            P(),
            P(),
            P(),
            P(),
            P(),
            P("grp", "sp", None),
        ),
        out_specs=(P("grp", TP, "sp", None), P("grp", TP, "sp")),
        check_vma=False,
    )
```

profile of v0, /device:TPU:5, one launch (start us, length us, event | category | flops | bytes accessed | tf_op | source)
XLA Modules:
  0.0 251.8 jit_solution(4153112434344448460)
XLA Ops:
  0.7 1.3 copy.117
  1.9 1.5 constant_dynamic-slice_fusion.4
  3.4 0.8 copy-done.1
  4.2 0.2 copy-done.3
  4.4 6.1 %fusion = bf16[1536,320]{0,1:T(8,128)(2,1)S(1)} fusion(bf16[1536,2048]{1,0:T(8,128)(2,1)} %bitcast.59, bf16[2048,128]{1,0:T(8,128)(2,1)S(1)} %get-tuple-element.20, bf16[2048,128]{1,0:T(8,128)(2,1)S(1)} %get-tuple-element.21, bf16[2048,64]{1,0:T(8,128)(2,1)S(1)} %copy.117), kind=kOutput, calls=%fused_computation.1 | convolution fusion | flops 2017689600 | bytes 8585216 | tf_op jit(solution)/shard_map/dot_general | solution.py:90
  10.5 0.7 copy.118
  11.3 1.0 broadcast_in_dim.11
  12.3 83.6 %all-to-all-start.1 = ((bf16[16,12,3,320]{3,2,1,0:T(4,128)(2,1)}), bf16[16,12,3,320]{3,2,1,0:T(4,128)(2,1)}, u32[]{:S(2)}, u32[]{:S(2)}) async-start(bf16[16,12,3,320]{3,2,1,0:T(4,128)(2,1)} %broadcast_in_dim.11), calls=%async_computation.1 | async-start | bytes 1179648 | tf_op jit(solution)/shard_map/all_to_all | solution.py:30
  95.9 0.6 dynamic_slice.39
  97.2 0.7 dynamic_slice.41
  97.9 4.5 %convolution_reduce_fusion = bf16[1536]{0:T(1024)(128)(2,1)S(1)} fusion(bf16[1536,2048]{1,0:T(8,128)(2,1)} %bitcast.60, bf16[2048,32]{0,1:T(8,128)(2,1)} %param.21, s32[]{:T(128)S(6)} %select_n.48), kind=kOutput, calls=%fused_computation.12 | convolution fusion | flops 6291456 | bytes 6302724 | tf_op jit(solution)/shard_map/dot_general | solution.py:106
  102.4 0.8 constant_dynamic-slice_fusion.6
  103.2 1.3 copy_subtract_fusion
  104.6 1.0 copy.111
  105.6 13.2 %fusion.26 = f32[12,2,64,1]{3,0,1,2:T(8,128)S(1)} fusion(f32[12,2,64,1]{3,0,1,2:T(8,128)S(1)} %copy.111), kind=kOutput, calls=%fused_computation.75 | output fusion | flops 96768 | bytes 12288 | tf_op jit(solution)/shard_map/jit(cumsum)/reduce_window_sum | solution.py:115
  118.7 0.7 slice_reduce_fusion.1
  119.5 0.5 copy.124
  120.0 0.8 copy.121
  120.8 1.2 dynamic_slice.48
  122.0 0.8 reshape_reshape.3
  122.9 0.7 subtract_exponential_fusion.1
  123.6 0.7 copy.116
  124.3 1.8 fusion.2
  126.2 0.8 constant_dynamic-slice_fusion.2
  127.4 0.6 broadcast_in_dim.10
  128.0 11.5 %all-to-all-start = ((f32[16,1,12,1]{2,3,1,0:T(1,128)}), f32[16,1,12,1]{2,3,1,0:T(1,128)S(1)}, u32[]{:S(2)}, u32[]{:S(2)}) async-start(f32[16,1,12,1]{2,3,1,0:T(1,128)} %broadcast_in_dim.10), calls=%async_computation | async-start | bytes 16384 | tf_op jit(solution)/shard_map/all_to_all | solution.py:30
  139.5 1.3 copy.119
  140.8 0.4 reshape.266
  141.2 0.5 copy.135
  141.8 2.3 multiply_convert_fusion
  144.2 0.2 copy.125
  144.4 0.5 reshape.268
  144.9 0.4 multiply_convert_fusion.1
  145.3 0.3 fusion.1
  145.5 1.1 copy.127
  146.7 3.7 %all-to-all-done = f32[16,1,12,1]{2,3,1,0:T(1,128)S(1)} async-done(((f32[16,1,12,1]{2,3,1,0:T(1,128)}), f32[16,1,12,1]{2,3,1,0:T(1,128)S(1)}, u32[]{:S(2)}, u32[]{:S(2)}) %all-to-all-start) | async-done | bytes 800 | tf_op jit(solution)/shard_map/all_to_all | solution.py:30
  150.4 7.8 %all-to-all-start.2 = ((f32[1,12,1,64,128]{4,2,1,0,3:T(1,128)}), f32[1,12,1,64,128]{4,2,1,0,3:T(1,128)S(1)}, u32[]{:S(2)}, u32[]{:S(2)}) async-start(f32[1,12,1,64,128]{4,2,1,0,3:T(1,128)} %copy.127), calls=%async_computation.2 | async-start | bytes 786432 | tf_op jit(solution)/shard_map/all_to_all | solution.py:136
  158.1 1.6 multiply_exponential_fusion
  160.2 0.7 fusion.27
  160.9 0.2 copy.133
  161.4 11.1 %all-to-all-done.2 = f32[1,12,1,64,128]{4,2,1,0,3:T(1,128)S(1)} async-done(((f32[1,12,1,64,128]{4,2,1,0,3:T(1,128)}), f32[1,12,1,64,128]{4,2,1,0,3:T(1,128)S(1)}, u32[]{:S(2)}, u32[]{:S(2)}) %all-to-all-start.2) | async-done | bytes 393248 | tf_op jit(solution)/shard_map/all_to_all | solution.py:136
  172.5 0.3 multiply_reduce_fusion
  173.0 0.8 multiply_reduce_fusion.3
  173.7 25.4 %psum.21 = f32[12]{0:T(128)S(1)} all-reduce(f32[12]{0:T(128)S(1)} %get-tuple-element.8), channel_id=1, replica_groups=mesh['grp'=2,'sp'=16,'tp_0'=16,'tp_1'=2] {'sp'}, use_global_device_ids=true, to_apply=%region_9.10 | all-reduce | flops 12 | bytes 96 | tf_op jit(solution)/shard_map/psum | solution.py:40
  199.1 32.4 %psum.22 = f32[12]{0:T(128)S(1)} all-reduce(f32[12]{0:T(128)S(1)} %psum.21), channel_id=1, replica_groups=mesh['grp'=2,'sp'=16,'tp_0'=16,'tp_1'=2] {'tp_0'}, use_global_device_ids=true, to_apply=%region_10.11 | all-reduce | flops 12 | bytes 96 | tf_op jit(solution)/shard_map/psum | solution.py:40
  231.5 0.8 dynamic-slice_bitcast_fusion
  232.3 18.8 %psum.23 = f32[12]{0:T(128)S(1)} all-reduce(f32[12]{0:T(128)S(1)} %psum.22), channel_id=1, replica_groups=mesh['grp'=2,'sp'=16,'tp_0'=16,'tp_1'=2] {'tp_1'}, use_global_device_ids=true, to_apply=%region_11.12 | all-reduce | flops 12 | bytes 96 | tf_op jit(solution)/shard_map/psum | solution.py:40
  251.1 0.7 copy.131
  (55 shorter events, 2.0 us)
Async XLA Ops:
  0.6 126.5 %copy-start = (bf16[2048,64]{0,1:T(8,128)(2,1)S(1)}, bf16[2048,64]{0,1:T(8,128)(2,1)}, u32[]{:S(2)}) copy-start(bf16[2048,64]{0,1:T(8,128)(2,1)} %param.18) | copy-start | bytes 786436
  1.9 1.5 copy-start.5
  3.4 0.8 copy-start.1
  3.4 1.0 copy-start.3
  10.5 85.4 %copy-start.12 = (f32[32]{0:T(128)S(1)}, f32[32]{0:T(128)}, u32[]{:S(2)}) copy-start(f32[32]{0:T(128)} %param.26) | copy-start | bytes 388
  10.5 86.7 %copy-start.13 = (f32[32]{0:T(128)S(1)}, f32[32]{0:T(128)}, u32[]{:S(2)}) copy-start(f32[32]{0:T(128)} %param.25) | copy-start | bytes 388
  12.3 115.1 %all-to-all-start.1 = ((bf16[16,12,3,320]{3,2,1,0:T(4,128)(2,1)}), bf16[16,12,3,320]{3,2,1,0:T(4,128)(2,1)}, u32[]{:S(2)}, u32[]{:S(2)}) async-start(bf16[16,12,3,320]{3,2,1,0:T(4,128)(2,1)} %broadcast_in_dim.11), calls=%async_computation.1 | async-start | bytes 1179648 | tf_op jit(solution)/shard_map/all_to_all | solution.py:30
  118.7 5.6 %copy-start.2 = (bf16[2048,128]{1,0:T(8,128)(2,1)S(1)}, bf16[2048,128]{1,0:T(8,128)(2,1)}, u32[]{:S(2)}) copy-start(bf16[2048,128]{1,0:T(8,128)(2,1)} %copy-done.1) | copy-start | bytes 1572868
  118.7 5.6 %copy-start.4 = (bf16[2048,128]{1,0:T(8,128)(2,1)S(1)}, bf16[2048,128]{1,0:T(8,128)(2,1)}, u32[]{:S(2)}) copy-start(bf16[2048,128]{1,0:T(8,128)(2,1)} %copy-done.3) | copy-start | bytes 1572868
  120.0 4.3 %copy-start.6 = (bf16[12,2048]{1,0:T(8,128)(2,1)S(1)}, bf16[12,2048]{1,0:T(8,128)(2,1)}, u32[]{:S(2)}) copy-start(bf16[12,2048]{1,0:T(8,128)(2,1)} %param.16) | copy-start | bytes 147460
  124.3 2.6 %copy-start.10 = (bf16[4,256]{1,0:T(4,128)(2,1)S(1)}, bf16[4,256]{1,0:T(4,128)(2,1)}, u32[]{:S(2)}) copy-start(bf16[4,256]{1,0:T(4,128)(2,1)} %param.24) | copy-start | bytes 6148
  124.3 2.6 %copy-start.11 = (bf16[4,256]{1,0:T(4,128)(2,1)S(1)}, bf16[4,256]{1,0:T(4,128)(2,1)}, u32[]{:S(2)}) copy-start(bf16[4,256]{1,0:T(4,128)(2,1)} %param.23) | copy-start | bytes 6148
  124.3 3.0 %copy-start.9 = (f32[12]{0:T(128)S(1)}, f32[12]{0:T(128)}, u32[]{:S(2)}) copy-start(f32[12]{0:T(128)} %get-tuple-element.2) | copy-start | bytes 148
  128.0 22.4 %all-to-all-start = ((f32[16,1,12,1]{2,3,1,0:T(1,128)}), f32[16,1,12,1]{2,3,1,0:T(1,128)S(1)}, u32[]{:S(2)}, u32[]{:S(2)}) async-start(f32[16,1,12,1]{2,3,1,0:T(1,128)} %broadcast_in_dim.10), calls=%async_computation | async-start | bytes 16384 | tf_op jit(solution)/shard_map/all_to_all | solution.py:30
  144.1 1.1 copy-start.8
  150.4 22.1 %all-to-all-start.2 = ((f32[1,12,1,64,128]{4,2,1,0,3:T(1,128)}), f32[1,12,1,64,128]{4,2,1,0,3:T(1,128)S(1)}, u32[]{:S(2)}, u32[]{:S(2)}) async-start(f32[1,12,1,64,128]{4,2,1,0,3:T(1,128)} %copy.127), calls=%async_computation.2 | async-start | bytes 786432 | tf_op jit(solution)/shard_map/all_to_all | solution.py:136
  172.8 79.0 %copy-start.7 = (bf16[12,4,128]{2,1,0:T(4,128)(2,1)}, bf16[12,4,128]{2,1,0:T(4,128)(2,1)S(1)}, u32[]{:S(2)}) copy-start(bf16[12,4,128]{2,1,0:T(4,128)(2,1)S(1)} %multiply_reduce_fusion) | copy-start | bytes 36868
where the time goes:
time: 253 us; the launch traced here: 252 us
  starting transfers between devices  103 us (41%)
  blocking collectives  76.6 us (30%)
  other arithmetic  21 us (8%)
  local copies, waits for them, and re-layouts  20.3 us (8%)
  waiting for transfers between devices  14.8 us (6%)
  matrix products  14.5 us (6%)
    all_to_all x2, starting transfers between devices, sent_to_all(): lax.all_to_all(jnp.broadcast_to(shard[None], (length, *shard.shape)), axi...  95.1 us
    psum x3, blocking collectives, one_axis_at_a_time(): return functools.reduce(lax.psum, axes, shard)  76.6 us
    another operation x1, other arithmetic, shards(): jnp.cumsum(logarithmic_decay.reshape(seq_count, block_count, SPAN, reside...  13.2 us
    all_to_all x1, waiting for transfers between devices, shards(): lax.all_to_all(local_state[None], 'sp', split_axis=3, concat_axis=0, tile...  11.1 us
    all_to_all x1, starting transfers between devices, shards(): lax.all_to_all(local_state[None], 'sp', split_axis=3, concat_axis=0, tile...  7.76 us
    dot_general x1, matrix products, shards(): jnp.dot(token_rows, weights_here, preferred_element_type=jnp.float32)  6.11 us
  transfers between devices with their start and end apart: 3, of which 2 were waited for; matrix products, arithmetic and copies ran while one was open for 16% of the time, Pallas kernels for 0%

commit v1 on v0

v1 whole, which is shorter than its diff:
```python
import jax
import jax.numpy as jnp
from jax import lax
from jax.experimental import pallas as pl
from jax.experimental.pallas import tpu as pltpu
from jax.sharding import Mesh
from jax.sharding import PartitionSpec as P

HEADS = 32
P_SIZE = 64
GROUPS = 2
STATE = 128
CONV = 4
LANES = 128
TP = ("tp_0", "tp_1")
EPSILON = 1e-06

F32 = jnp.float32
BF16 = jnp.bfloat16


def rounded(value):
    return value.astype(BF16).astype(F32)


def silu(value):
    return value / (1.0 + jnp.exp(-value))


def softplus(value):
    return jnp.maximum(value, 0.0) + jnp.log1p(jnp.exp(-jnp.abs(value)))


def dot(a, b, dims=((1,), (0,))):
    return lax.dot_general(a, b, (dims, ((), ())), preferred_element_type=F32)


def pieces(value):
    first = value.astype(BF16)
    rest = value - first.astype(F32)
    second = rest.astype(BF16)
    third = (rest - second.astype(F32)).astype(BF16)
    return first, second, third


def dot01(matrix, value):
    a, b, c = pieces(value)
    return dot(jnp.concatenate([matrix] * 3, axis=1), jnp.concatenate([a, b, c], axis=0))


def iota(shape, dim):
    return lax.broadcasted_iota(jnp.int32, shape, dim)


def own_half(row, head):
    return jnp.where(head % 2 == 0, row, pltpu.roll(row, 64, axis=1))


def pick(row, lane):
    return jnp.sum(jnp.where(iota(row.shape, 1) == lane, row, 0.0), axis=1, keepdims=True)


def pick_row(matrix, row):
    matrix = matrix.astype(F32)
    return jnp.sum(jnp.where(iota(matrix.shape, 0) == row, matrix, 0.0), axis=0, keepdims=True)


def local_body(
    x_hbm, value_ref, key_ref, step_ref, vt_ref, kt_ref, bias_ref, decay_ref, off_ref,
    state_ref, trail_ref, lead_ref, lead_weight_ref, logs_ref, taps_ref,
    x_ref, w_ref, trail_f32, sems, *, per,
):
    prompts, length, width = x_hbm.shape
    copies = []
    for i in range(prompts // per):
        part = pl.ds(i * per, per)
        copies.append(pltpu.make_async_copy(x_hbm.at[part], x_ref.at[part], sems.at[i]))
    for copy in copies:
        copy.start()
    head = lax.axis_index(TP)
    group = head // (HEADS // GROUPS)
    step_row = jnp.broadcast_to(pick_row(step_ref[...], head), (P_SIZE, width)).astype(BF16)
    w_ref[:, :LANES] = jnp.transpose(jnp.concatenate([value_ref[...], step_row], axis=0))
    trail_f32[...] = jnp.zeros_like(trail_f32)
    logs_ref[...] = jnp.zeros_like(logs_ref)
    at = pl.multiple_of(group * STATE, STATE)
    w_ref[:, LANES:] = key_ref[:, pl.ds(at, STATE)]
    pair = pl.multiple_of((head // 2) * LANES, LANES)
    value_taps = own_half(vt_ref[:, pl.ds(pair, LANES)].astype(F32), head)
    taps = jnp.concatenate([value_taps, kt_ref[:, pl.ds(at, STATE)].astype(F32)], axis=1)
    taps_ref[:CONV] = taps
    bias = pick(bias_ref[...], head)
    speed = jnp.exp(pick(decay_ref[...], head))
    later = (iota((length, length), 1) > iota((length, length), 0)).astype(BF16)
    position = iota((length, LANES), 0)
    for i in range(prompts // per):
        copies[i].wait()
        rows = x_ref[i * per : (i + 1) * per].reshape(per * length, width)
        raw_all = rounded(dot(rows, w_ref[...]))
        steps, logs, mixes = [], [], []
        for j in range(per):
            b = i * per + j
            raw = raw_all[j * length : (j + 1) * length]
            for k in range(CONV - 1):
                lead_ref[k, b : b + 1, :] = raw[k : k + 1]
                last = length - (CONV - 1) + k
                trail_f32[k, b : b + 1, :] = raw[last : last + 1]
            step = softplus(pltpu.roll(raw[:, :LANES], 64, axis=1) + bias)
            offset = jnp.broadcast_to(pick_row(off_ref[b], head), (length, length))
            log = jnp.transpose(offset) - speed * step
            total = raw * taps[CONV - 1 : CONV]
            for k in range(CONV - 1):
                total = total + pltpu.roll(raw, CONV - 1 - k, axis=0) * taps[k : k + 1]
            steps.append(step)
            logs.append(log)
            mixes.append(rounded(silu(total)))
        after = dot01(later, jnp.concatenate(logs, axis=1))
        for j in range(per):
            b = i * per + j
            after_here = after[:, j * LANES : (j + 1) * LANES]
            weight = jnp.exp(after_here) * steps[j]
            logs_ref[b : b + 1, :] = after_here[:1] + logs[j][:1]
            for k in range(CONV - 1):
                lead_weight_ref[k, b : b + 1, :] = weight[k : k + 1]
            weighted = jnp.where(position >= CONV - 1, mixes[j][:, :LANES] * weight, 0.0)
            state = dot(
                weighted.astype(BF16), mixes[j][:, LANES:].astype(BF16), ((0,), (0,))
            )
            state_ref[b] = state[:P_SIZE]
    trail_ref[...] = trail_f32[...].astype(BF16)


def token_body(
    x_ref, next_ref, value_ref, gate_ref, key_ref, query_ref, step_ref, qt_ref, bias_ref,
    decay_ref, skip_ref, trail_ref, taps_ref,
    out_map_ref, direct_ref, decay_out_ref, gate_out_ref,
    pad_ref, last_ref,
):
    prompts, block, width = x_ref.shape
    head = lax.axis_index(TP)
    group = head // (HEADS // GROUPS)
    at = pl.multiple_of(group * STATE, STATE)
    query = query_ref[:, pl.ds(at, STATE)]
    query_taps = qt_ref[:, pl.ds(at, STATE)].astype(F32)
    taps = taps_ref[...]
    last_ref[...] = rounded(dot(x_ref[...].reshape(prompts * block, width), query)).reshape(
        prompts, block, STATE
    )
    pad_ref[...] = jnp.zeros_like(pad_ref)
    pad_ref[:prompts] = next_ref[...].astype(F32)
    token = pad_ref[...].astype(BF16)
    new_value = rounded(dot(token, value_ref[...], ((1,), (1,))))
    new_key = rounded(dot(token, key_ref[:, pl.ds(at, STATE)]))
    new_query = rounded(dot(token, query))
    new_step = pick(rounded(dot(token, step_ref[...], ((1,), (1,)))), head)
    new_gate = rounded(dot(token, gate_ref[...], ((1,), (1,))))
    trail = trail_ref[...].astype(F32)
    value_sum = trail[0, :, :P_SIZE] * taps[:1, :P_SIZE]
    key_sum = trail[0, :, LANES:] * taps[:1, LANES:]
    query_sum = last_ref[:, block - 3, :] * query_taps[:1]
    for k in range(1, CONV - 1):
        value_sum = value_sum + trail[k, :, :P_SIZE] * taps[k : k + 1, :P_SIZE]
        key_sum = key_sum + trail[k, :, LANES:] * taps[k : k + 1, LANES:]
        query_sum = query_sum + last_ref[:, block - 3 + k, :] * query_taps[k : k + 1]
    new_input = rounded(silu(value_sum + new_value * taps[CONV - 1 : CONV, :P_SIZE]))
    new_in = rounded(silu(key_sum + new_key * taps[CONV - 1 : CONV, LANES:]))
    new_out = rounded(silu(query_sum + new_query[:prompts] * query_taps[CONV - 1 : CONV]))
    out_map_ref[...] = jnp.zeros_like(out_map_ref)
    out_map_ref[:prompts] = new_out
    step = softplus(new_step + pick(bias_ref[...], head))
    speed = jnp.exp(pick(decay_ref[...], head))
    decay_out_ref[...] = jnp.broadcast_to(jnp.exp(-speed * step), decay_out_ref.shape)
    agreement = jnp.sum(new_in * out_map_ref[...], axis=1, keepdims=True)
    direct_ref[...] = new_input * (step * agreement + pick(skip_ref[...], head))
    gate_out_ref[...] = silu(new_gate)


def pack_body(
    halo_ref, lead_ref, lead_weight_ref, logs_ref, taps_ref, state_ref, out_map_ref, direct_ref,
    out_ref,
):
    prompts, rows, _ = state_ref.shape
    dests = out_ref.shape[0]
    keep = rows // dests
    taps = taps_ref[...]
    window = [halo_ref[k].astype(F32) for k in range(CONV - 1)]
    window = window + [lead_ref[k] for k in range(CONV - 1)]
    weighted, maps = [], []
    for t in range(CONV - 1):
        total = window[t] * taps[:1]
        for k in range(1, CONV):
            total = total + window[t + k] * taps[k : k + 1]
        mixed = rounded(silu(total))
        weighted.append(jnp.transpose(rounded(mixed[:, :LANES] * lead_weight_ref[t])))
        maps.append(mixed[:, LANES:])
    states = []
    for b in range(prompts):
        state = state_ref[b]
        for t in range(CONV - 1):
            state = state + weighted[t][:rows, b : b + 1] * maps[t][b : b + 1]
        states.append(state)
    pair_rows = 2 * keep
    blocks = rows // pair_rows
    low = iota((blocks, pair_rows, STATE), 1) < keep
    for b in range(0, prompts, 2):
        one = states[b].reshape(blocks, pair_rows, STATE)
        two = states[b + 1].reshape(blocks, pair_rows, STATE)
        even = jnp.where(low, one, pltpu.roll(two, keep, axis=1))
        odd = jnp.where(low, pltpu.roll(one, keep, axis=1), two)
        at = b * keep
        for k in range(blocks):
            out_ref[2 * k, at : at + pair_rows, :] = even[k].astype(BF16)
            out_ref[2 * k + 1, at : at + pair_rows, :] = odd[k].astype(BF16)
    base = prompts * keep
    padded = out_map_ref.shape[0]
    direct = direct_ref[...]
    high = rounded(direct)
    low_part = direct - high
    log_parts = [part.astype(F32) for part in pieces(logs_ref[...])]
    lane = iota((padded, LANES), 1)
    log_lanes = jnp.where(
        lane == 2 * keep,
        log_parts[0],
        jnp.where(lane == 2 * keep + 1, log_parts[1], log_parts[2]),
    )
    new_out = out_map_ref[...].astype(BF16)
    wide = jnp.concatenate([high, low_part], axis=1)
    for d in range(dests):
        first = pltpu.roll(wide, (LANES - d * keep) % LANES, axis=1)
        second = pltpu.roll(wide, (LANES - P_SIZE - d * keep + keep) % LANES, axis=1)
        misc = jnp.where(lane < keep, first, jnp.where(lane < 2 * keep, second, log_lanes))
        out_ref[d, base : base + padded, :] = new_out
        out_ref[d, base + padded :, :] = misc.astype(BF16)


def read_body(
    parts_ref, decay_ref, gate_ref,
    cache_ref, gated_ref, squares_ref,
    *, prompts, keep,
):
    sources = parts_ref.shape[0]
    rows = prompts * keep
    padded = decay_ref.shape[0]
    shard = lax.axis_index("sp")
    repeat = (iota((rows, padded), 1) == iota((rows, padded), 0) // keep).astype(BF16)
    within = iota((rows, LANES), 0) % keep
    lane = iota((rows, LANES), 1)
    total = jnp.zeros((rows, STATE), F32)
    for s in range(sources):
        misc = dot(repeat, parts_ref[s, rows + padded :, :])
        log = jnp.sum(
            jnp.where((lane >= 2 * keep) & (lane < 2 * keep + 3), misc, 0.0), axis=1, keepdims=True
        )
        total = total * jnp.exp(log) + parts_ref[s, :rows, :].astype(F32)
    cache = total.astype(BF16)
    cache_ref[...] = cache
    new_out = dot(repeat, parts_ref[sources - 1, rows : rows + padded, :])
    read = jnp.sum(cache.astype(F32) * new_out, axis=1, keepdims=True)
    direct = jnp.sum(
        jnp.where((lane < 2 * keep) & (lane % keep == within), misc, 0.0), axis=1, keepdims=True
    )
    decay = dot01(repeat, decay_ref[...])
    gate = dot01(repeat, jnp.concatenate([gate_ref[...], gate_ref[...]], axis=1))
    gate = jnp.sum(jnp.where(lane == shard * keep + within, gate, 0.0), axis=1, keepdims=True)
    gated = (decay * read + direct) * gate
    spread = jnp.where(lane == iota((rows, LANES), 0) // keep, gated, 0.0)
    gather = (iota((8, rows), 0) == iota((8, rows), 1) % keep).astype(BF16)
    gated = dot01(gather, spread)
    gated_ref[...] = gated
    squares = jnp.sum(gated * gated, axis=0, keepdims=True)
    squares_ref[...] = jnp.broadcast_to(squares[None], squares_ref.shape)


def sum_body(parts_ref, out_ref):
    total = jnp.sum(parts_ref[...], axis=0, keepdims=True)
    out_ref[...] = jnp.broadcast_to(total, out_ref.shape)


def final_body(parts_ref, gated_ref, gain_ref, out_ref):
    _, keep, prompts = out_ref.shape
    heads, rows = gain_ref.shape
    head = lax.axis_index(TP)
    shard = lax.axis_index("sp")
    total = jnp.sum(parts_ref[...], axis=0)
    scale = lax.rsqrt(total / (heads * rows) + EPSILON)
    gain = jnp.broadcast_to(pick_row(gain_ref[...], head), (8, rows))
    own = iota((8, rows), 1) == shard * keep + iota((8, rows), 0)
    gain = jnp.sum(jnp.where(own, gain, 0.0), axis=1, keepdims=True)
    out = gated_ref[...] * scale * gain
    out_ref[0] = out[:keep, :prompts].astype(BF16)


def whole(count):
    return [pl.BlockSpec(memory_space=pltpu.VMEM) for _ in range(count)]


def call(body, outs, *operands, specs=None, scratch=(), name=None):
    return pl.pallas_call(
        body,
        in_specs=specs or whole(len(operands)),
        out_specs=whole(len(outs)),
        out_shape=outs,
        scratch_shapes=scratch,
        name=name,
    )(*operands)


def shards(
    prompt_layer_input,
    next_token_input,
    value_projection,
    output_gate_matrix,
    key_projection,
    query_projection,
    step_projection,
    value_filter_taps,
    key_filter_taps,
    query_filter_taps,
    step_size_bias,
    head_decay_logarithm,
    direct_path_weight,
    gated_norm_gain,
    position_decay_offset,
):
    prompts, length, width = prompt_layer_input.shape
    dests = lax.axis_size("sp")
    keep = P_SIZE // dests
    padded = -(-prompts // 8) * 8
    bias = step_size_bias[None]
    decay_rate = head_decay_logarithm[None]
    skip = direct_path_weight[None]
    out = jax.ShapeDtypeStruct
    value_rows = value_projection.T
    gate_rows = output_gate_matrix.T
    step_rows = step_projection.T
    offset_rows = jnp.swapaxes(position_decay_offset, 1, 2)

    per = 2
    state, trail, lead, lead_weight, logs, taps = call(
        lambda *refs: local_body(*refs, per=per),
        [
            out((prompts, P_SIZE, STATE), F32),
            out((CONV - 1, padded, 2 * LANES), BF16),
            out((CONV - 1, padded, 2 * LANES), F32),
            out((CONV - 1, padded, LANES), F32),
            out((padded, LANES), F32),
            out((8, 2 * LANES), F32),
        ],
        prompt_layer_input,
        value_rows,
        key_projection,
        step_rows,
        value_filter_taps,
        key_filter_taps,
        bias,
        decay_rate,
        offset_rows,
        specs=[pl.BlockSpec(memory_space=pl.ANY)] + whole(8),
        scratch=[
            pltpu.VMEM((prompts, length, width), BF16),
            pltpu.VMEM((width, 2 * LANES), BF16),
            pltpu.VMEM((CONV - 1, padded, 2 * LANES), F32),
            pltpu.SemaphoreType.DMA((prompts // per,)),
        ],
        name="local",
    )
    halo = lax.ppermute(trail, "sp", [(i, i + 1) for i in range(dests - 1)])
    block = 16
    token_operands = (
        prompt_layer_input,
        next_token_input,
        value_rows,
        gate_rows,
        key_projection,
        query_projection,
        step_rows,
        query_filter_taps,
        bias,
        decay_rate,
        skip,
        trail,
        taps,
    )
    tail = length // block - 1
    out_map, direct, new_decay, new_gate = pl.pallas_call(
        token_body,
        grid=(1,),
        in_specs=[pl.BlockSpec((prompts, block, width), lambda i: (0, tail, 0))]
        + whole(len(token_operands) - 1),
        out_specs=whole(4),
        out_shape=[
            out((padded, STATE), F32),
            out((padded, P_SIZE), F32),
            out((padded, LANES), F32),
            out((padded, P_SIZE), F32),
        ],
        scratch_shapes=[
            pltpu.VMEM((padded, width), F32),
            pltpu.VMEM((prompts, block, STATE), F32),
        ],
        name="token",
    )(*token_operands)
    (payload,) = call(
        pack_body,
        [out((dests, prompts * keep + 2 * padded, STATE), BF16)],
        halo,
        lead,
        lead_weight,
        logs,
        taps,
        state,
        out_map,
        direct,
        name="pack",
    )
    received = lax.all_to_all(payload, "sp", 0, 0, tiled=True)
    cache, gated, squares = call(
        lambda *refs: read_body(*refs, prompts=prompts, keep=keep),
        [
            out((prompts * keep, STATE), BF16),
            out((8, LANES), F32),
            out((dests, 1, LANES), F32),
        ],
        received,
        new_decay,
        new_gate,
        name="read",
    )
    squares = lax.all_to_all(squares, "sp", 0, 0, tiled=True)
    tp_size = lax.axis_size(TP)
    (squares,) = call(sum_body, [out((tp_size, 1, LANES), F32)], squares, name="sum")
    squares = lax.all_to_all(squares, TP, 0, 0, tiled=True)
    (first_read,) = call(
        final_body, [out((1, keep, prompts), BF16)], squares, gated, gated_norm_gain, name="final"
    )
    return cache.reshape(prompts, 1, keep, STATE), jnp.transpose(first_read, (2, 0, 1))


def solution(mesh):
    split = Mesh(
        mesh.devices.reshape(mesh.shape["grp"], mesh.shape["sp"], mesh.shape["tp"] // 2, 2),
        ("grp", "sp", "tp_0", "tp_1"),
    )
    return jax.shard_map(
        shards,
        mesh=split,
        in_specs=(
            P("grp", "sp", None),
            P("grp", None),
            P(None, TP),
            P(None, TP),
            P(),
            P(),
            P(),
            P(),
            P(),
            P(),
            P(),
            P(),
            P(),
            P(),
            P("grp", "sp", None),
        ),
        out_specs=(P("grp", TP, "sp", None), P("grp", TP, "sp")),
        check_vma=False,
    )
```

time: 253 us -> 176 us (0.70)
  starting transfers between devices: 103 us -> 9.19 us
  blocking collectives: 76.6 us -> 144 us
  Pallas kernels: 0 us -> 21.3 us
  other arithmetic: 21 us -> 0 us
  local copies, waits for them, and re-layouts: 20.3 us -> 0.59 us
  waiting for transfers between devices: 14.8 us -> 0.01 us
  matrix products: 14.5 us -> 0 us
    all_to_all x0 -> x3, blocking collectives: none -> 144 us  [the longest x1 91.1 us: shards(): received = lax.all_to_all(payload, 'sp', 0, 0, tiled=True)]
    all_to_all x3 -> x0, starting transfers between devices: 103 us -> none  [the longest x2 95.1 us: sent_to_all(): lax.all_to_all(jnp.broadcast_to(shard[None], (length, *shard.shape)), axi...]
    psum x3 -> x0, blocking collectives: 76.6 us -> none  [one_axis_at_a_time(): return functools.reduce(lax.psum, axes, shard)]
    pallas_call x0 -> x6, Pallas kernels: none -> 21.3 us  [the longest x5 17.9 us: call(): pl.pallas_call(body, in_specs=specs or whole(len(operands)), out_specs=wh...]
    all_to_all x3 -> x0, waiting for transfers between devices: 14.8 us -> none  [the longest x1 11.1 us: shards(): lax.all_to_all(local_state[None], 'sp', split_axis=3, concat_axis=0, tile...]
    dot_general x6 -> x0, matrix products: 14.5 us -> none  [the longest x1 6.11 us: shards(): jnp.dot(token_rows, weights_here, preferred_element_type=jnp.float32)]
    another operation x3 -> x0, other arithmetic: 13.9 us -> none  [the longest x1 13.2 us: shards(): jnp.cumsum(logarithmic_decay.reshape(seq_count, block_count, SPAN, reside...]
    ppermute x0 -> x1, starting transfers between devices: none -> 9.19 us  [shards(): halo = lax.ppermute(trail, 'sp', [(i, i + 1) for i in range(dests - 1)])]
  transfers between devices with their start and end apart: 3 -> 1, of which waited for: 2 -> 0; matrix products, arithmetic and copies ran while one was open for 16% -> 0% of each run, Pallas kernels for 0% -> 2%
where the time goes in v1:
time: 176 us
  blocking collectives  144 us (82%)
  Pallas kernels  21.3 us (12%)
  starting transfers between devices  9.19 us (5%)
    all_to_all x1, blocking collectives, shards(): received = lax.all_to_all(payload, 'sp', 0, 0, tiled=True)  91.1 us
    all_to_all x1, blocking collectives, shards(): squares = lax.all_to_all(squares, TP, 0, 0, tiled=True)  28.7 us
    all_to_all x1, blocking collectives, shards(): squares = lax.all_to_all(squares, 'sp', 0, 0, tiled=True)  24.1 us
    pallas_call x5, Pallas kernels, call(): pl.pallas_call(body, in_specs=specs or whole(len(operands)), out_specs=wh...  17.9 us
    ppermute x1, starting transfers between devices, shards(): halo = lax.ppermute(trail, 'sp', [(i, i + 1) for i in range(dests - 1)])  9.19 us
  transfers between devices with their start and end apart: 1, of which 0 were waited for; matrix products, arithmetic and copies ran while one was open for 0% of the time, Pallas kernels for 2%

profile of v1, /device:TPU:5, one launch (start us, length us, event | category | flops | bytes accessed | tf_op | source)
XLA Modules:
  0.0 175.7 jit_solution(4665924880516538138)
XLA Ops:
  0.6 10.8 %local.1 = (f32[12,64,128]{2,1,0:T(8,128)}, bf16[3,16,256]{2,1,0:T(8,128)(2,1)}, f32[3,16,256]{2,1,0:T(8,128)}, f32[3,16,128]{2,1,0:T(8,128)}, f32[16,128]{1,0:T(8,128)}, /*index=5*/f32[8,256]{1,0:T(8,128)}) custom-call(bf16[12,128,2048]{2,1,0:T(8,128)(2,1)} %x_ref.1, bf16[64,2048]{1,0:T(8,128)(2,1)} %bitcast.11, bf16[2048,256]{1,0:T(8,128)(2,1)} %key_ref.1, ...), custom_call_target="tpu_custom_call" | custom-call | tf_op jit(solution)/shard_map/local/pallas_call | solution.py:298
  11.4 9.2 %collective-permute-start = (bf16[3,16,256]{2,1,0:T(8,128)(2,1)}, bf16[3,16,256]{2,1,0:T(8,128)(2,1)S(1)}, u32[]{:S(2)}, u32[]{:S(2)}) collective-permute-start(bf16[3,16,256]{2,1,0:T(8,128)(2,1)} %get-tuple-element.15.trail_ref), channel_id=1, source_target_pairs={{0,32},{32,64},{64,96},{96,128},{128,160},{160,192},{192,224},{224... | collective-permute-start | bytes 73736 | tf_op jit(solution)/shard_map/ppermute | solution.py:367
  20.6 3.4 %token_.1 = (f32[16,128]{1,0:T(8,128)}, f32[16,64]{1,0:T(8,128)}, f32[16,128]{1,0:T(8,128)}, f32[16,64]{1,0:T(8,128)}) custom-call(bf16[12,128,2048]{2,1,0:T(8,128)(2,1)} %x_ref.1, bf16[12,2048]{1,0:T(8,128)(2,1)} %next_ref.1, bf16[64,2048]{1,0:T(8,128)(2,1)} %bitcast.12, bf16[64,2048]{1,0:T(8,128)(2,1)} %bitcast.15, bf16[2048,256]{1,0:T(8,128)(2,1)} %key_ref.1, ...), custom_call_target="tpu_custom_call" | custom-call | tf_op jit(solution)/shard_map/token/pallas_call | solution.py:385
  24.0 0.0 collective-permute-done.halo_ref
  24.0 0.0 copy-start
  24.0 0.6 copy-done
  24.6 2.2 %pack.1 = bf16[16,80,128]{2,1,0:T(8,128)(2,1)} custom-call(bf16[3,16,256]{2,1,0:T(8,128)(2,1)} %copy-done, f32[3,16,256]{2,1,0:T(8,128)} %get-tuple-element.16.lead_ref, f32[3,16,128]{2,1,0:T(8,128)} %get-tuple-element.17.lead_weight_ref, f32[16,128]{1,0:T(8,128)} %get-tuple-element.18.logs_ref, f32[8,256]{1,0:T(8,128)} %get-tuple-element.19.taps_ref, ...), custom_call_target="tpu_custom_call" | custom-call | tf_op jit(solution)/shard_map/pack/pallas_call | solution.py:298
  26.9 91.1 %all_to_all.15.refs_0_ = bf16[16,80,128]{2,1,0:T(8,128)(2,1)} all-to-all(bf16[16,80,128]{2,1,0:T(8,128)(2,1)} %pack.1), channel_id=1, replica_groups=mesh['grp'=2,'sp'=16,'tp_0'=16,'tp_1'=2] {'sp'}, dimensions={0} | all-to-all | bytes 655360 | tf_op jit(solution)/shard_map/all_to_all | solution.py:416
  118.0 2.1 %read.1 = (bf16[48,128]{1,0:T(8,128)(2,1)}, f32[8,128]{1,0:T(8,128)}, f32[16,1,128]{2,1,0:T(1,128)}) custom-call(bf16[16,80,128]{2,1,0:T(8,128)(2,1)} %all_to_all.15.refs_0_, f32[16,128]{1,0:T(8,128)} %get-tuple-element.23.refs_1_, f32[16,64]{1,0:T(8,128)} %get-tuple-element.24.refs_2_), custom_call_target="tpu_custom_call" | custom-call | tf_op jit(solution)/shard_map/read/pallas_call | solution.py:298
  120.1 24.1 %all_to_all.16.parts_ref = f32[16,1,128]{2,1,0:T(1,128)} all-to-all(f32[16,1,128]{2,1,0:T(1,128)} %get-tuple-element.26), channel_id=1, replica_groups=mesh['grp'=2,'sp'=16,'tp_0'=16,'tp_1'=2] {'sp'}, dimensions={0} | all-to-all | bytes 16384 | tf_op jit(solution)/shard_map/all_to_all | solution.py:429
  144.2 1.3 sum.1
  145.6 28.7 %all_to_all.17.parts_ref = f32[32,1,128]{2,1,0:T(1,128)} all-to-all(f32[32,1,128]{2,1,0:T(1,128)} %sum.1), channel_id=1, replica_groups=mesh['grp'=2,'sp'=16,'tp_0'=16,'tp_1'=2] {'tp_0','tp_1'}, dimensions={0} | all-to-all | bytes 32768 | tf_op jit(solution)/shard_map/all_to_all | solution.py:432
  174.3 1.4 final.1
Async XLA Ops:
  11.4 12.6 %collective-permute-start = (bf16[3,16,256]{2,1,0:T(8,128)(2,1)}, bf16[3,16,256]{2,1,0:T(8,128)(2,1)S(1)}, u32[]{:S(2)}, u32[]{:S(2)}) collective-permute-start(bf16[3,16,256]{2,1,0:T(8,128)(2,1)} %get-tuple-element.15.trail_ref), channel_id=1, source_target_pairs={{0,32},{32,64},{64,96},{96,128},{128,160},{160,192},{192,224},{224... | collective-permute-start | bytes 73736 | tf_op jit(solution)/shard_map/ppermute | solution.py:367
  24.0 0.6 copy-start

commit v2 on v1

v2 whole, which is shorter than its diff:
```python
import jax
import jax.numpy as jnp
from jax import lax
from jax.experimental import pallas as pl
from jax.experimental.pallas import tpu as pltpu
from jax.sharding import Mesh
from jax.sharding import PartitionSpec as P

HEADS = 32
P_SIZE = 64
GROUPS = 2
STATE = 128
CONV = 4
LANES = 128
TP = ("tp_0", "tp_1")
EPSILON = 1e-06

F32 = jnp.float32
BF16 = jnp.bfloat16


def rounded(value):
    return value.astype(BF16).astype(F32)


def silu(value):
    return value / (1.0 + jnp.exp(-value))


def softplus(value):
    return jnp.maximum(value, 0.0) + jnp.log1p(jnp.exp(-jnp.abs(value)))


def dot(a, b, dims=((1,), (0,))):
    return lax.dot_general(a, b, (dims, ((), ())), preferred_element_type=F32)


def pieces(value):
    first = value.astype(BF16)
    rest = value - first.astype(F32)
    second = rest.astype(BF16)
    third = (rest - second.astype(F32)).astype(BF16)
    return first, second, third


def dot01(matrix, value):
    a, b, c = pieces(value)
    return dot(jnp.concatenate([matrix] * 3, axis=1), jnp.concatenate([a, b, c], axis=0))


def iota(shape, dim):
    return lax.broadcasted_iota(jnp.int32, shape, dim)


def own_half(row, head):
    return jnp.where(head % 2 == 0, row, pltpu.roll(row, 64, axis=1))


def pick(row, lane):
    return jnp.sum(jnp.where(iota(row.shape, 1) == lane, row, 0.0), axis=1, keepdims=True)


def pick_row(matrix, row):
    matrix = matrix.astype(F32)
    return jnp.sum(jnp.where(iota(matrix.shape, 0) == row, matrix, 0.0), axis=0, keepdims=True)


def local_body(
    x_hbm, value_ref, key_ref, step_ref, vt_ref, kt_ref, bias_ref, decay_ref, off_ref,
    state_ref, lead_ref, lead_weight_ref, logs_ref, taps_ref,
    x_ref, w_ref, sems, *, per,
):
    prompts, length, width = x_hbm.shape
    copies = []
    for i in range(prompts // per):
        part = pl.ds(i * per, per)
        copies.append(pltpu.make_async_copy(x_hbm.at[part], x_ref.at[part], sems.at[i]))
    for copy in copies:
        copy.start()
    head = lax.axis_index(TP)
    group = head // (HEADS // GROUPS)
    step_row = jnp.broadcast_to(pick_row(step_ref[...], head), (P_SIZE, width)).astype(BF16)
    w_ref[:, :LANES] = jnp.transpose(jnp.concatenate([value_ref[...], step_row], axis=0))
    logs_ref[...] = jnp.zeros_like(logs_ref)
    at = pl.multiple_of(group * STATE, STATE)
    w_ref[:, LANES:] = key_ref[:, pl.ds(at, STATE)]
    pair = pl.multiple_of((head // 2) * LANES, LANES)
    value_taps = own_half(vt_ref[:, pl.ds(pair, LANES)].astype(F32), head)
    taps = jnp.concatenate([value_taps, kt_ref[:, pl.ds(at, STATE)].astype(F32)], axis=1)
    taps_ref[:CONV] = taps
    bias = pick(bias_ref[...], head)
    speed = jnp.exp(pick(decay_ref[...], head))
    later = (iota((length, length), 1) > iota((length, length), 0)).astype(BF16)
    position = iota((length, LANES), 0)
    for i in range(prompts // per):
        copies[i].wait()
        rows = x_ref[i * per : (i + 1) * per].reshape(per * length, width)
        raw_all = rounded(dot(rows, w_ref[...]))
        steps, logs, mixes = [], [], []
        for j in range(per):
            b = i * per + j
            raw = raw_all[j * length : (j + 1) * length]
            for k in range(CONV - 1):
                lead_ref[k, b : b + 1, :] = raw[k : k + 1]
            step = softplus(pltpu.roll(raw[:, :LANES], 64, axis=1) + bias)
            offset = jnp.broadcast_to(pick_row(off_ref[b], head), (length, length))
            log = jnp.transpose(offset) - speed * step
            total = raw * taps[CONV - 1 : CONV]
            for k in range(CONV - 1):
                total = total + pltpu.roll(raw, CONV - 1 - k, axis=0) * taps[k : k + 1]
            steps.append(step)
            logs.append(log)
            mixes.append(rounded(silu(total)))
        after = dot01(later, jnp.concatenate(logs, axis=1))
        for j in range(per):
            b = i * per + j
            after_here = after[:, j * LANES : (j + 1) * LANES]
            weight = jnp.exp(after_here) * steps[j]
            logs_ref[b : b + 1, :] = after_here[:1] + logs[j][:1]
            for k in range(CONV - 1):
                lead_weight_ref[k, b : b + 1, :] = weight[k : k + 1]
            weighted = jnp.where(position >= CONV - 1, mixes[j][:, :LANES] * weight, 0.0)
            state = dot(
                weighted.astype(BF16), mixes[j][:, LANES:].astype(BF16), ((0,), (0,))
            )
            state_ref[b] = state[:P_SIZE]


def token_body(
    x_ref, next_ref, value_ref, gate_ref, key_ref, query_ref, step_ref, vt_ref, kt_ref, qt_ref,
    bias_ref, decay_ref, skip_ref,
    trail_ref, newest_ref, decay_out_ref, gate_out_ref,
    pad_ref, last_ref,
):
    prompts, block, width = x_ref.shape
    head = lax.axis_index(TP)
    group = head // (HEADS // GROUPS)
    padded = pad_ref.shape[0]
    at = pl.multiple_of(group * STATE, STATE)
    pair = pl.multiple_of((head // 2) * LANES, LANES)
    query = query_ref[:, pl.ds(at, STATE)]
    key = key_ref[:, pl.ds(at, STATE)]
    value_taps = own_half(vt_ref[:, pl.ds(pair, LANES)].astype(F32), head)[:, :P_SIZE]
    key_taps = kt_ref[:, pl.ds(at, STATE)].astype(F32)
    query_taps = qt_ref[:, pl.ds(at, STATE)].astype(F32)
    pad_ref[...] = jnp.zeros_like(pad_ref)
    pad_ref[:prompts] = next_ref[...].astype(F32)
    token = pad_ref[...].astype(BF16)
    rows = jnp.concatenate([x_ref[...].reshape(prompts * block, width), token], axis=0)
    count = prompts * block
    values = rounded(dot(rows, value_ref[...], ((1,), (1,))))
    keys = rounded(dot(rows, key))
    queries = rounded(dot(rows, query))
    new_step = pick(rounded(dot(token, step_ref[...], ((1,), (1,)))), head)
    new_gate = rounded(dot(token, gate_ref[...], ((1,), (1,))))
    last_ref[...] = jnp.zeros_like(last_ref)
    for b in range(prompts):
        at_row = (b + 1) * block - (CONV - 1)
        for k in range(CONV - 1):
            row = slice(at_row + k, at_row + k + 1)
            last_ref[k, b : b + 1, :P_SIZE] = values[row]
            last_ref[k, b : b + 1, LANES : 2 * LANES] = keys[row]
            last_ref[k, b : b + 1, 2 * LANES :] = queries[row]
    last = last_ref[...]
    trail_ref[...] = last[:, :, : 2 * LANES].astype(BF16)
    value_sum = last[0, :, :P_SIZE] * value_taps[:1]
    key_sum = last[0, :, LANES : 2 * LANES] * key_taps[:1]
    query_sum = last[0, :, 2 * LANES :] * query_taps[:1]
    for k in range(1, CONV - 1):
        value_sum = value_sum + last[k, :, :P_SIZE] * value_taps[k : k + 1]
        key_sum = key_sum + last[k, :, LANES : 2 * LANES] * key_taps[k : k + 1]
        query_sum = query_sum + last[k, :, 2 * LANES :] * query_taps[k : k + 1]
    new_input = rounded(silu(value_sum + values[count:] * value_taps[CONV - 1 : CONV]))
    new_in = rounded(silu(key_sum + keys[count:] * key_taps[CONV - 1 : CONV]))
    new_out = rounded(silu(query_sum + queries[count:] * query_taps[CONV - 1 : CONV]))
    step = softplus(new_step + pick(bias_ref[...], head))
    speed = jnp.exp(pick(decay_ref[...], head))
    decay_out_ref[...] = jnp.broadcast_to(jnp.exp(-speed * step), decay_out_ref.shape)
    agreement = jnp.sum(new_in * new_out, axis=1, keepdims=True)
    direct = new_input * (step * agreement + pick(skip_ref[...], head))
    high = rounded(direct)
    direct = jnp.concatenate([high, direct - high], axis=1)
    newest = jnp.concatenate([new_out, direct], axis=0).astype(BF16)
    for d in range(newest_ref.shape[0]):
        newest_ref[d] = newest
    gate_out_ref[...] = silu(new_gate)


def pack_body(
    halo_ref, lead_ref, lead_weight_ref, logs_ref, taps_ref, state_ref, newest_ref, out_ref,
):
    prompts, rows, _ = state_ref.shape
    dests = out_ref.shape[0]
    keep = rows // dests
    padded = logs_ref.shape[0]
    taps = taps_ref[...]
    new_out = newest_ref[dests - 1, :padded, :].astype(F32)
    window = [halo_ref[k].astype(F32) for k in range(CONV - 1)]
    window = window + [lead_ref[k] for k in range(CONV - 1)]
    weighted, maps = [], []
    for t in range(CONV - 1):
        total = window[t] * taps[:1]
        for k in range(1, CONV):
            total = total + window[t + k] * taps[k : k + 1]
        mixed = rounded(silu(total))
        weighted.append(jnp.transpose(rounded(mixed[:, :LANES] * lead_weight_ref[t])))
        maps.append(mixed[:, LANES:])
    states = []
    reads = jnp.zeros((rows, LANES), F32)
    lane = iota((rows, LANES), 1)
    for b in range(prompts):
        state = state_ref[b]
        for t in range(CONV - 1):
            state = state + weighted[t][:rows, b : b + 1] * maps[t][b : b + 1]
        states.append(state)
        read = jnp.sum(state * new_out[b : b + 1], axis=1, keepdims=True)
        reads = jnp.where(lane == b, read, reads)
    pair_rows = 2 * keep
    blocks = rows // pair_rows
    low = iota((blocks, pair_rows, STATE), 1) < keep
    for b in range(0, prompts, 2):
        one = states[b].reshape(blocks, pair_rows, STATE)
        two = states[b + 1].reshape(blocks, pair_rows, STATE)
        even = jnp.where(low, one, pltpu.roll(two, keep, axis=1))
        odd = jnp.where(low, pltpu.roll(one, keep, axis=1), two)
        at = b * keep
        for k in range(blocks):
            out_ref[2 * k, at : at + pair_rows, :] = even[k].astype(BF16)
            out_ref[2 * k + 1, at : at + pair_rows, :] = odd[k].astype(BF16)
    reads = jnp.transpose(reads)[:padded]
    high = rounded(reads)
    extra = jnp.concatenate([high, reads - high], axis=1)
    corner = (padded, LANES)
    logs = jnp.where(iota(corner, 0) == iota(corner, 1), logs_ref[...], 0.0)
    logs = jnp.sum(logs, axis=0, keepdims=True)
    for k, part in enumerate(pieces(logs)):
        extra = jnp.where(iota(corner, 0) == prompts + k, part.astype(F32), extra)
    extra = extra.astype(BF16)
    for d in range(dests):
        out_ref[d, prompts * keep :, :] = extra


def read_body(
    parts_ref, newest_ref, decay_ref, gate_ref, cache_ref, gated_ref, squares_ref, *, prompts,
):
    sources, _, _ = parts_ref.shape
    padded = decay_ref.shape[0]
    rows = parts_ref.shape[1] - padded
    keep = rows // prompts
    shard = lax.axis_index("sp")
    state_own = iota((rows, LANES), 1) == iota((rows, LANES), 0) // keep
    read_own = iota((padded, LANES), 1) == iota((padded, LANES), 0)
    total = jnp.zeros((rows, STATE), F32)
    reads = jnp.zeros((padded, P_SIZE), F32)
    for s in range(sources):
        extra = parts_ref[s, rows:, :].astype(F32)
        decay = jnp.sum(extra[prompts : prompts + 3], axis=0, keepdims=True)
        decay = jnp.exp(decay)
        per_row = jnp.sum(jnp.where(state_own, decay, 0.0), axis=1, keepdims=True)
        per_prompt = jnp.sum(jnp.where(read_own, decay, 0.0), axis=1, keepdims=True)
        total = total * per_row + parts_ref[s, :rows, :].astype(F32)
        reads = reads * per_prompt + (extra[:, :P_SIZE] + extra[:, P_SIZE:])
    cache_ref[...] = total.astype(BF16)
    direct = newest_ref[sources - 1, padded:, :].astype(F32)
    direct = direct[:, :P_SIZE] + direct[:, P_SIZE:]
    gated = (decay_ref[:, :P_SIZE] * reads + direct) * gate_ref[...]
    gated = jnp.where(iota(gated.shape, 0) < prompts, gated, 0.0)
    squares = jnp.sum(gated * gated, axis=1, keepdims=True)
    squares = jnp.sum(jnp.where(read_own, squares, 0.0), axis=0, keepdims=True)
    squares_ref[...] = jnp.broadcast_to(squares[None], squares_ref.shape)
    square = jnp.concatenate([gated, jnp.zeros((P_SIZE - padded, P_SIZE), F32)], axis=0)
    square = jnp.concatenate([square, jnp.zeros((P_SIZE, P_SIZE), F32)], axis=0)
    square = jnp.concatenate([square, jnp.zeros((LANES, P_SIZE), F32)], axis=1)
    own = (iota((8, LANES), 1) == shard * keep + iota((8, LANES), 0)).astype(BF16)
    gated_ref[...] = dot01(own, jnp.transpose(square))


def final_body(parts_ref, gated_ref, gain_ref, out_ref):
    _, keep, prompts = out_ref.shape
    heads, rows = gain_ref.shape
    head = lax.axis_index(TP)
    shard = lax.axis_index("sp")
    total = jnp.sum(parts_ref[...], axis=0)
    scale = lax.rsqrt(total / (heads * rows) + EPSILON)
    gain = jnp.broadcast_to(pick_row(gain_ref[...], head), (8, rows))
    own = iota((8, rows), 1) == shard * keep + iota((8, rows), 0)
    gain = jnp.sum(jnp.where(own, gain, 0.0), axis=1, keepdims=True)
    out = gated_ref[...] * scale * gain
    out_ref[0] = out[:keep, :prompts].astype(BF16)


def whole(count):
    return [pl.BlockSpec(memory_space=pltpu.VMEM) for _ in range(count)]


def call(body, outs, *operands, specs=None, scratch=(), name=None):
    return pl.pallas_call(
        body,
        in_specs=specs or whole(len(operands)),
        out_specs=whole(len(outs)),
        out_shape=outs,
        scratch_shapes=scratch,
        name=name,
    )(*operands)


def shards(
    prompt_layer_input,
    next_token_input,
    value_projection,
    output_gate_matrix,
    key_projection,
    query_projection,
    step_projection,
    value_filter_taps,
    key_filter_taps,
    query_filter_taps,
    step_size_bias,
    head_decay_logarithm,
    direct_path_weight,
    gated_norm_gain,
    position_decay_offset,
):
    prompts, length, width = prompt_layer_input.shape
    dests = lax.axis_size("sp")
    keep = P_SIZE // dests
    padded = -(-prompts // 8) * 8
    bias = step_size_bias[None]
    decay_rate = head_decay_logarithm[None]
    skip = direct_path_weight[None]
    out = jax.ShapeDtypeStruct
    value_rows = value_projection.T
    gate_rows = output_gate_matrix.T
    step_rows = step_projection.T
    offset_rows = jnp.swapaxes(position_decay_offset, 1, 2)

    block = 16
    tail = length // block - 1
    token_operands = (
        prompt_layer_input,
        next_token_input,
        value_rows,
        gate_rows,
        key_projection,
        query_projection,
        step_rows,
        value_filter_taps,
        key_filter_taps,
        query_filter_taps,
        bias,
        decay_rate,
        skip,
    )
    trail, newest, new_decay, new_gate = pl.pallas_call(
        token_body,
        grid=(1,),
        in_specs=[pl.BlockSpec((prompts, block, width), lambda i: (0, tail, 0))]
        + whole(len(token_operands) - 1),
        out_specs=whole(4),
        out_shape=[
            out((CONV - 1, padded, 2 * LANES), BF16),
            out((dests, 2 * padded, LANES), BF16),
            out((padded, LANES), F32),
            out((padded, P_SIZE), F32),
        ],
        scratch_shapes=[
            pltpu.VMEM((padded, width), F32),
            pltpu.VMEM((CONV - 1, padded, 3 * LANES), F32),
        ],
        name="token",
    )(*token_operands)
    newest = lax.all_to_all(newest, "sp", 0, 0, tiled=True)
    halo = lax.ppermute(trail, "sp", [(i, i + 1) for i in range(dests - 1)])
    per = 2
    state, lead, lead_weight, logs, taps = call(
        lambda *refs: local_body(*refs, per=per),
        [
            out((prompts, P_SIZE, STATE), F32),
            out((CONV - 1, padded, 2 * LANES), F32),
            out((CONV - 1, padded, LANES), F32),
            out((padded, LANES), F32),
            out((8, 2 * LANES), F32),
        ],
        prompt_layer_input,
        value_rows,
        key_projection,
        step_rows,
        value_filter_taps,
        key_filter_taps,
        bias,
        decay_rate,
        offset_rows,
        specs=[pl.BlockSpec(memory_space=pl.ANY)] + whole(8),
        scratch=[
            pltpu.VMEM((prompts, length, width), BF16),
            pltpu.VMEM((width, 2 * LANES), BF16),
            pltpu.SemaphoreType.DMA((prompts // per,)),
        ],
        name="local",
    )
    (payload,) = call(
        pack_body,
        [out((dests, prompts * keep + padded, STATE), BF16)],
        halo,
        lead,
        lead_weight,
        logs,
        taps,
        state,
        newest,
        name="pack",
    )
    received = lax.all_to_all(payload, "sp", 0, 0, tiled=True)
    tp_size = lax.axis_size(TP)
    cache, gated, squares = call(
        lambda *refs: read_body(*refs, prompts=prompts),
        [
            out((prompts * keep, STATE), BF16),
            out((8, LANES), F32),
            out((tp_size, 1, LANES), F32),
        ],
        received,
        newest,
        new_decay,
        new_gate,
        name="read",
    )
    squares = lax.all_to_all(squares, TP, 0, 0, tiled=True)
    (first_read,) = call(
        final_body, [out((1, keep, prompts), BF16)], squares, gated, gated_norm_gain, name="final"
    )
    return cache.reshape(prompts, 1, keep, STATE), jnp.transpose(first_read, (2, 0, 1))


def solution(mesh):
    split = Mesh(
        mesh.devices.reshape(mesh.shape["grp"], mesh.shape["sp"], mesh.shape["tp"] // 2, 2),
        ("grp", "sp", "tp_0", "tp_1"),
    )
    return jax.shard_map(
        shards,
        mesh=split,
        in_specs=(
            P("grp", "sp", None),
            P("grp", None),
            P(None, TP),
            P(None, TP),
            P(),
            P(),
            P(),
            P(),
            P(),
            P(),
            P(),
            P(),
            P(),
            P(),
            P("grp", "sp", None),
        ),
        out_specs=(P("grp", TP, "sp", None), P("grp", TP, "sp")),
        check_vma=False,
    )
```

time: 176 us -> 166 us (0.943)
  blocking collectives: 144 us -> 56.2 us
  starting transfers between devices: 9.19 us -> 86.7 us
    all_to_all x0 -> x1, starting transfers between devices: none -> 83.6 us  [shards(): newest = lax.all_to_all(newest, 'sp', 0, 0, tiled=True)]
    all_to_all x1, blocking collectives: 91.1 us -> 23.2 us  [shards(): received = lax.all_to_all(payload, 'sp', 0, 0, tiled=True)]
    all_to_all x1 -> x0, blocking collectives: 24.1 us -> none  [shards(): squares = lax.all_to_all(squares, 'sp', 0, 0, tiled=True)]
    ppermute x1, starting transfers between devices: 9.19 us -> 3.08 us  [shards(): halo = lax.ppermute(trail, 'sp', [(i, i + 1) for i in range(dests - 1)])]
    all_to_all x1, blocking collectives: 28.7 us -> 33 us  [shards(): squares = lax.all_to_all(squares, TP, 0, 0, tiled=True)]
    pallas_call x5 -> x4, Pallas kernels: 17.9 us -> 17.6 us  [call(): pl.pallas_call(body, in_specs=specs or whole(len(operands)), out_specs=wh...]
  transfers between devices with their start and end apart: 1 -> 2, of which waited for: 0 -> 0; matrix products, arithmetic and copies ran while one was open for 0% -> 0% of each run, Pallas kernels for 2% -> 7%
where the time goes in v2:
time: 166 us
  starting transfers between devices  86.7 us (52%)
  blocking collectives  56.2 us (34%)
  Pallas kernels  21.4 us (13%)
    all_to_all x1, starting transfers between devices, shards(): newest = lax.all_to_all(newest, 'sp', 0, 0, tiled=True)  83.6 us
    all_to_all x1, blocking collectives, shards(): squares = lax.all_to_all(squares, TP, 0, 0, tiled=True)  33 us
    all_to_all x1, blocking collectives, shards(): received = lax.all_to_all(payload, 'sp', 0, 0, tiled=True)  23.2 us
    pallas_call x4, Pallas kernels, call(): pl.pallas_call(body, in_specs=specs or whole(len(operands)), out_specs=wh...  17.6 us
    pallas_call x1, Pallas kernels, shards(): pl.pallas_call(token_body, grid=(1,), in_specs=[pl.BlockSpec((prompts, bl...  3.8 us
  transfers between devices with their start and end apart: 2, of which 0 were waited for; matrix products, arithmetic and copies ran while one was open for 0% of the time, Pallas kernels for 7%

profile of v2, /device:TPU:5, one launch (start us, length us, event | category | flops | bytes accessed | tf_op | source)
XLA Modules:
  0.0 165.7 jit_solution(693580175351891095)
XLA Ops:
  0.6 3.8 %token_.1 = (bf16[3,16,256]{2,1,0:T(8,128)(2,1)}, bf16[16,32,128]{2,1,0:T(8,128)(2,1)}, f32[16,128]{1,0:T(8,128)}, f32[16,64]{1,0:T(8,128)}) custom-call(bf16[12,128,2048]{2,1,0:T(8,128)(2,1)} %refs_0_.1, bf16[12,2048]{1,0:T(8,128)(2,1)} %next_ref.1, bf16[64,2048]{1,0:T(8,128)(2,1)} %bitcast.11, bf16[64,2048]{1,0:T(8,128)(2,1)} %bitcast.15, ...), custom_call_target="tpu_custom_call" | custom-call | tf_op jit(solution)/shard_map/token/pallas_call | solution.py:354
  4.4 83.6 %all-to-all-start = ((bf16[16,32,128]{2,1,0:T(8,128)(2,1)}), bf16[16,32,128]{2,1,0:T(8,128)(2,1)S(1)}, u32[]{:S(2)}, u32[]{:S(2)}) async-start(bf16[16,32,128]{2,1,0:T(8,128)(2,1)} %get-tuple-element.20), calls=%async_computation | async-start | bytes 262144 | tf_op jit(solution)/shard_map/all_to_all | solution.py:372
  88.1 3.1 %collective-permute-start = (bf16[3,16,256]{2,1,0:T(8,128)(2,1)}, bf16[3,16,256]{2,1,0:T(8,128)(2,1)S(1)}, u32[]{:S(2)}, u32[]{:S(2)}) collective-permute-start(bf16[3,16,256]{2,1,0:T(8,128)(2,1)} %get-tuple-element.14), channel_id=1, source_target_pairs={{0,32},{32,64},{64,96},{96,128},{128,160},{160,192},{192,224},{224... | collective-permute-start | bytes 73736 | tf_op jit(solution)/shard_map/ppermute | solution.py:373
  91.2 10.9 %local.1 = (f32[12,64,128]{2,1,0:T(8,128)}, f32[3,16,256]{2,1,0:T(8,128)}, f32[3,16,128]{2,1,0:T(8,128)}, f32[16,128]{1,0:T(8,128)}, f32[8,256]{1,0:T(8,128)}) custom-call(bf16[12,128,2048]{2,1,0:T(8,128)(2,1)} %refs_0_.1, bf16[64,2048]{1,0:T(8,128)(2,1)} %bitcast.12, bf16[2048,256]{1,0:T(8,128)(2,1)} %refs_2_.1, bf16[32,2048]{1,0:T(8,128)(2,1)} %bitcast.14, ...), custom_call_target="tpu_custom_call" | custom-call | tf_op jit(solution)/shard_map/local/pallas_call | solution.py:297
  102.0 0.0 collective-permute-done.halo_ref
  102.0 0.0 copy-start.1
  102.1 0.0 all-to-all-done.newest_ref.refs_1_
  102.1 0.0 copy-start
  102.1 0.6 copy-done.1
  102.7 0.1 copy-done
  102.7 3.1 %pack.1 = bf16[16,64,128]{2,1,0:T(8,128)(2,1)} custom-call(bf16[3,16,256]{2,1,0:T(8,128)(2,1)} %copy-done.1, f32[3,16,256]{2,1,0:T(8,128)} %get-tuple-element.15.lead_ref, f32[3,16,128]{2,1,0:T(8,128)} %get-tuple-element.16.lead_weight_ref, f32[16,128]{1,0:T(8,128)} %get-tuple-element.17.logs_ref, f32[8,256]{1,0:T(8,128)} %get-tuple-element.18.taps_ref, ...), custom_call_target="tpu_custom_call" | custom-call | tf_op jit(solution)/shard_map/pack/pallas_call | solution.py:297
  105.8 23.2 %all_to_all.15.refs_0_ = bf16[16,64,128]{2,1,0:T(8,128)(2,1)} all-to-all(bf16[16,64,128]{2,1,0:T(8,128)(2,1)} %pack.1), channel_id=1, replica_groups=mesh['grp'=2,'sp'=16,'tp_0'=16,'tp_1'=2] {'sp'}, dimensions={0} | all-to-all | bytes 524288 | tf_op jit(solution)/shard_map/all_to_all | solution.py:413
  129.0 2.2 %read.1 = (bf16[48,128]{1,0:T(8,128)(2,1)}, f32[8,128]{1,0:T(8,128)}, f32[32,1,128]{2,1,0:T(1,128)}) custom-call(bf16[16,64,128]{2,1,0:T(8,128)(2,1)} %all_to_all.15.refs_0_, bf16[16,32,128]{2,1,0:T(8,128)(2,1)} %copy-done, f32[16,128]{1,0:T(8,128)} %get-tuple-element.21.refs_2_, f32[16,64]{1,0:T(8,128)} %get-tuple-element.22.refs_3_), custom_call_target="tpu_custom_call" | custom-call | tf_op jit(solution)/shard_map/read/pallas_call | solution.py:297
  131.3 33.0 %all_to_all.16.parts_ref = f32[32,1,128]{2,1,0:T(1,128)} all-to-all(f32[32,1,128]{2,1,0:T(1,128)} %get-tuple-element.24), channel_id=1, replica_groups=mesh['grp'=2,'sp'=16,'tp_0'=16,'tp_1'=2] {'tp_0','tp_1'}, dimensions={0} | all-to-all | bytes 32768 | tf_op jit(solution)/shard_map/all_to_all | solution.py:428
  164.3 1.4 final.1
Async XLA Ops:
  4.4 97.6 %all-to-all-start = ((bf16[16,32,128]{2,1,0:T(8,128)(2,1)}), bf16[16,32,128]{2,1,0:T(8,128)(2,1)S(1)}, u32[]{:S(2)}, u32[]{:S(2)}) async-start(bf16[16,32,128]{2,1,0:T(8,128)(2,1)} %get-tuple-element.20), calls=%async_computation | async-start | bytes 262144 | tf_op jit(solution)/shard_map/all_to_all | solution.py:372
  88.1 14.0 %collective-permute-start = (bf16[3,16,256]{2,1,0:T(8,128)(2,1)}, bf16[3,16,256]{2,1,0:T(8,128)(2,1)S(1)}, u32[]{:S(2)}, u32[]{:S(2)}) collective-permute-start(bf16[3,16,256]{2,1,0:T(8,128)(2,1)} %get-tuple-element.14), channel_id=1, source_target_pairs={{0,32},{32,64},{64,96},{96,128},{128,160},{160,192},{192,224},{224... | collective-permute-start | bytes 73736 | tf_op jit(solution)/shard_map/ppermute | solution.py:373
  102.0 0.6 copy-start.1
  102.1 0.7 copy-start

commit v3 on v2

--- a/solution.py
+++ b/solution.py
@@ -135,7 +135,6 @@
     prompts, block, width = x_ref.shape
     head = lax.axis_index(TP)
     group = head // (HEADS // GROUPS)
-    padded = pad_ref.shape[0]
     at = pl.multiple_of(group * STATE, STATE)
     pair = pl.multiple_of((head // 2) * LANES, LANES)
     query = query_ref[:, pl.ds(at, STATE)]
@@ -180,9 +179,7 @@
     direct = new_input * (step * agreement + pick(skip_ref[...], head))
     high = rounded(direct)
     direct = jnp.concatenate([high, direct - high], axis=1)
-    newest = jnp.concatenate([new_out, direct], axis=0).astype(BF16)
-    for d in range(newest_ref.shape[0]):
-        newest_ref[d] = newest
+    newest_ref[...] = jnp.concatenate([new_out, direct], axis=0).astype(BF16)
     gate_out_ref[...] = silu(new_gate)
 
 
@@ -190,11 +187,8 @@
     halo_ref, lead_ref, lead_weight_ref, logs_ref, taps_ref, state_ref, newest_ref, out_ref,
 ):
     prompts, rows, _ = state_ref.shape
-    dests = out_ref.shape[0]
-    keep = rows // dests
     padded = logs_ref.shape[0]
     taps = taps_ref[...]
-    new_out = newest_ref[dests - 1, :padded, :].astype(F32)
     window = [halo_ref[k].astype(F32) for k in range(CONV - 1)]
     window = window + [lead_ref[k] for k in range(CONV - 1)]
     weighted, maps = [], []
@@ -205,74 +199,153 @@
         mixed = rounded(silu(total))
         weighted.append(jnp.transpose(rounded(mixed[:, :LANES] * lead_weight_ref[t])))
         maps.append(mixed[:, LANES:])
-    states = []
-    reads = jnp.zeros((rows, LANES), F32)
-    lane = iota((rows, LANES), 1)
     for b in range(prompts):
         state = state_ref[b]
         for t in range(CONV - 1):
             state = state + weighted[t][:rows, b : b + 1] * maps[t][b : b + 1]
-        states.append(state)
+        out_ref[b * rows : (b + 1) * rows] = state.astype(BF16)
+    base = prompts * rows
+    logs = jnp.zeros((padded, LANES), F32)
+    for k, part in enumerate(pieces(logs_ref[...])):
+        logs = jnp.where(iota(logs.shape, 1) == k, part.astype(F32), logs)
+    out_ref[base : base + padded] = logs.astype(BF16)
+    out_ref[base + padded :] = newest_ref[...]
+
+
+def log_of(part_ref, base, padded):
+    log = jnp.sum(part_ref[base : base + padded].astype(F32), axis=1, keepdims=True)
+    return jnp.broadcast_to(log, (padded, LANES))
+
+
+def followed(states, part_ref, log):
+    decay = jnp.exp(log)
+    rows = states[0].shape[0]
+    return [
+        state * decay[b : b + 1] + part_ref[b * rows : (b + 1) * rows].astype(F32)
+        for b, state in enumerate(states)
+    ]
+
+
+def joined_shards(refs, base, padded, prompts):
+    rows = base // prompts
+    states = [refs[0][b * rows : (b + 1) * rows].astype(F32) for b in range(prompts)]
+    logs = log_of(refs[0], base, padded)
+    for ref in refs[1:]:
+        log = log_of(ref, base, padded)
+        logs = logs + log
+        states = followed(states, ref, log)
+    return states, logs
+
+
+def early_body(*refs, prompts, padded, half):
+    parts, (one_ref, two_ref, logs_ref, newest_ref) = refs[:-4], refs[-4:]
+    base = prompts * P_SIZE
+    one, one_log = joined_shards(parts[:half], base, padded, prompts)
+    two, two_log = joined_shards(parts[half:], base, padded, prompts)
+    for b in range(prompts):
+        one_ref[b] = one[b]
+        two_ref[b] = two[b]
+    logs_ref[0] = one_log
+    logs_ref[1] = two_log
+    newest_ref[...] = parts[half - 1][base + padded :]
+
+
+def hub_body(
+    one_ref, two_ref, logs_ref, newest_ref, before_ref, last_ref, decay_ref, gate_ref,
+    own_ref, next_ref, pair_ref, rest_ref, *, half, keep,
+):
+    prompts, rows, _ = one_ref.shape
+    padded = decay_ref.shape[0]
+    base = prompts * rows
+    low = lax.axis_index("sp") < half
+    two_log = logs_ref[1]
+    two = [two_ref[b] for b in range(prompts)]
+    for ref in (before_ref, last_ref):
+        log = log_of(ref, base, padded)
+        two_log = two_log + log
+        two = followed(two, ref, log)
+    one_decay = jnp.exp(jnp.where(low, two_log, 0.0))
+    two_decay = jnp.exp(jnp.where(low, 0.0, logs_ref[0]))
+    newest = jnp.where(
+        low, last_ref[base + padded :].astype(F32), newest_ref[...].astype(F32)
+    )
+    new_out = newest[:padded]
+    lane = iota((rows, LANES), 1)
+    reads = jnp.zeros((rows, LANES), F32)
+    kept = []
+    for b in range(prompts):
+        state = rounded(one_ref[b] * one_decay[b : b + 1] + two[b] * two_decay[b : b + 1])
         read = jnp.sum(state * new_out[b : b + 1], axis=1, keepdims=True)
         reads = jnp.where(lane == b, read, reads)
+        kept.append(jnp.where(low, state[: rows // 2], state[rows // 2 :]))
+    corner = (padded, LANES)
+    decay = jnp.where(iota(corner, 0) == iota(corner, 1), decay_ref[...], 0.0)
+    decay = jnp.sum(decay, axis=0, keepdims=True)
+    below = jnp.zeros((LANES - padded, LANES), F32)
+    direct = jnp.transpose(jnp.concatenate([newest[padded:], below], axis=0))
+    direct = direct[:rows] + direct[rows:]
+    gate = jnp.concatenate([gate_ref[...], gate_ref[...]], axis=1)
+    gate = jnp.transpose(jnp.concatenate([gate, below], axis=0))[:rows]
+    gated = jnp.where(lane < prompts, (decay * reads + direct) * gate, 0.0)
+    squares = jnp.sum(gated * gated, axis=0, keepdims=True)
+    gated = jnp.where(low, gated[: rows // 2], gated[rows // 2 :])
+    count = rows // 2
+    square_rows = jnp.zeros(corner, F32)
+    for k, part in enumerate(pieces(squares)):
+        square_rows = jnp.where(iota(corner, 0) == k, part.astype(F32), square_rows)
+    stack = jnp.concatenate([*pieces(gated), square_rows.astype(BF16)], axis=0)
+    chosen = (16 * half, stack.shape[0])
+    dest, at, col = iota(chosen, 0) // 16, iota(chosen, 0) % 16, iota(chosen, 1)
+    source = jnp.where(
+        at < 3 * keep,
+        (at // keep) * count + dest * keep + at % keep,
+        3 * count + at - 3 * keep,
+    )
+    extra = dot((col == source).astype(BF16), stack).astype(BF16)
+
+    def place(dest):
+        if dest == 0:
+            return own_ref, 0
+        if dest == 1:
+            return next_ref, 0
+        return (pair_ref, dest - 2) if dest < 4 else (rest_ref, dest - 4)
+
     pair_rows = 2 * keep
-    blocks = rows // pair_rows
-    low = iota((blocks, pair_rows, STATE), 1) < keep
+    blocks = count // pair_rows
+    first = iota((blocks, pair_rows, STATE), 1) < keep
     for b in range(0, prompts, 2):
-        one = states[b].reshape(blocks, pair_rows, STATE)
-        two = states[b + 1].reshape(blocks, pair_rows, STATE)
-        even = jnp.where(low, one, pltpu.roll(two, keep, axis=1))
-        odd = jnp.where(low, pltpu.roll(one, keep, axis=1), two)
-        at = b * keep
+        one = kept[b].reshape(blocks, pair_rows, STATE)
+        two = kept[b + 1].reshape(blocks, pair_rows, STATE)
+        even = jnp.where(first, one, pltpu.roll(two, keep, axis=1)).astype(BF16)
+        odd = jnp.where(first, pltpu.roll(one, keep, axis=1), two).astype(BF16)
         for k in range(blocks):
-            out_ref[2 * k, at : at + pair_rows, :] = even[k].astype(BF16)
-            out_ref[2 * k + 1, at : at + pair_rows, :] = odd[k].astype(BF16)
-    reads = jnp.transpose(reads)[:padded]
-    high = rounded(reads)
-    extra = jnp.concatenate([high, reads - high], axis=1)
-    corner = (padded, LANES)
-    logs = jnp.where(iota(corner, 0) == iota(corner, 1), logs_ref[...], 0.0)
-    logs = jnp.sum(logs, axis=0, keepdims=True)
-    for k, part in enumerate(pieces(logs)):
-        extra = jnp.where(iota(corner, 0) == prompts + k, part.astype(F32), extra)
-    extra = extra.astype(BF16)
-    for d in range(dests):
-        out_ref[d, prompts * keep :, :] = extra
-
-
-def read_body(
-    parts_ref, newest_ref, decay_ref, gate_ref, cache_ref, gated_ref, squares_ref, *, prompts,
+            for dest, value in ((2 * k, even[k]), (2 * k + 1, odd[k])):
+                ref, i = place(dest)
+                ref[i, b * keep : (b + 2) * keep, :] = value
+    for d in range(half):
+        ref, i = place(d)
+        ref[i, prompts * keep :, :] = extra[d * 16 : (d + 1) * 16]
+
+
+def pick_body(
+    own_ref, next_ref, pair_ref, rest_ref, sixth_ref, odd_ref,
+    cache_ref, gated_ref, squares_ref, *, half, keep,
 ):
-    sources, _, _ = parts_ref.shape
-    padded = decay_ref.shape[0]
-    rows = parts_ref.shape[1] - padded
-    keep = rows // prompts
-    shard = lax.axis_index("sp")
-    state_own = iota((rows, LANES), 1) == iota((rows, LANES), 0) // keep
-    read_own = iota((padded, LANES), 1) == iota((padded, LANES), 0)
-    total = jnp.zeros((rows, STATE), F32)
-    reads = jnp.zeros((padded, P_SIZE), F32)
-    for s in range(sources):
-        extra = parts_ref[s, rows:, :].astype(F32)
-        decay = jnp.sum(extra[prompts : prompts + 3], axis=0, keepdims=True)
-        decay = jnp.exp(decay)
-        per_row = jnp.sum(jnp.where(state_own, decay, 0.0), axis=1, keepdims=True)
-        per_prompt = jnp.sum(jnp.where(read_own, decay, 0.0), axis=1, keepdims=True)
-        total = total * per_row + parts_ref[s, :rows, :].astype(F32)
-        reads = reads * per_prompt + (extra[:, :P_SIZE] + extra[:, P_SIZE:])
-    cache_ref[...] = total.astype(BF16)
-    direct = newest_ref[sources - 1, padded:, :].astype(F32)
-    direct = direct[:, :P_SIZE] + direct[:, P_SIZE:]
-    gated = (decay_ref[:, :P_SIZE] * reads + direct) * gate_ref[...]
-    gated = jnp.where(iota(gated.shape, 0) < prompts, gated, 0.0)
-    squares = jnp.sum(gated * gated, axis=1, keepdims=True)
-    squares = jnp.sum(jnp.where(read_own, squares, 0.0), axis=0, keepdims=True)
-    squares_ref[...] = jnp.broadcast_to(squares[None], squares_ref.shape)
-    square = jnp.concatenate([gated, jnp.zeros((P_SIZE - padded, P_SIZE), F32)], axis=0)
-    square = jnp.concatenate([square, jnp.zeros((P_SIZE, P_SIZE), F32)], axis=0)
-    square = jnp.concatenate([square, jnp.zeros((LANES, P_SIZE), F32)], axis=1)
-    own = (iota((8, LANES), 1) == shard * keep + iota((8, LANES), 0)).astype(BF16)
-    gated_ref[...] = dot01(own, jnp.transpose(square))
+    rows = cache_ref.shape[0]
+    at_hub = lax.axis_index("sp") % half == 0
+    mine = jnp.where(at_hub, own_ref[0].astype(F32), 0.0)
+    for value in (next_ref[0], pair_ref[0], rest_ref[0], sixth_ref[2], odd_ref[0]):
+        mine = mine + value.astype(F32)
+    mine = mine.astype(BF16)
+    cache_ref[...] = mine[:rows]
+    shape = (8, 16)
+    row, col = iota(shape, 0), iota(shape, 1)
+    chosen = ((row < keep) & (col < 3 * keep) & (col % keep == row)) | (
+        (row == keep) & (col >= 3 * keep) & (col < 3 * keep + 3)
+    )
+    values = dot(chosen.astype(BF16), mine[rows:])
+    gated_ref[...] = values
+    squares_ref[...] = jnp.broadcast_to(values[keep : keep + 1][None], squares_ref.shape)
 
 
 def final_body(parts_ref, gated_ref, gain_ref, out_ref):
@@ -293,14 +366,13 @@
     return [pl.BlockSpec(memory_space=pltpu.VMEM) for _ in range(count)]
 
 
-def call(body, outs, *operands, specs=None, scratch=(), name=None):
+def call(body, outs, *operands, specs=None, scratch=()):
     return pl.pallas_call(
         body,
         in_specs=specs or whole(len(operands)),
         out_specs=whole(len(outs)),
         out_shape=outs,
         scratch_shapes=scratch,
-        name=name,
     )(*operands)
 
 
@@ -359,7 +431,7 @@
         out_specs=whole(4),
         out_shape=[
             out((CONV - 1, padded, 2 * LANES), BF16),
-            out((dests, 2 * padded, LANES), BF16),
+            out((2 * padded, LANES), BF16),
             out((padded, LANES), F32),
             out((padded, P_SIZE), F32),
         ],
@@ -369,7 +441,6 @@
         ],
         name="token",
     )(*token_operands)
-    newest = lax.all_to_all(newest, "sp", 0, 0, tiled=True)
     halo = lax.ppermute(trail, "sp", [(i, i + 1) for i in range(dests - 1)])
     per = 2
     state, lead, lead_weight, logs, taps = call(
@@ -396,11 +467,10 @@
             pltpu.VMEM((width, 2 * LANES), BF16),
             pltpu.SemaphoreType.DMA((prompts // per,)),
         ],
-        name="local",
     )
     (payload,) = call(
         pack_body,
-        [out((dests, prompts * keep + padded, STATE), BF16)],
+        [out((prompts * P_SIZE + 3 * padded, STATE), BF16)],
         halo,
         lead,
         lead_weight,
@@ -408,26 +478,59 @@
         taps,
         state,
         newest,
-        name="pack",
-    )
-    received = lax.all_to_all(payload, "sp", 0, 0, tiled=True)
+    )
+    half = dests // 2
+    parts = {0: payload}
+    for k in range(dests - 1, 0, -1):
+        pairs = [(k, 0), ((half + k) % dests, half)]
+        parts[k] = lax.ppermute(payload, "sp", pairs)
+    states = out((prompts, P_SIZE, STATE), F32)
+    one, two, early_logs, early_newest = call(
+        lambda *refs: early_body(*refs, prompts=prompts, padded=padded, half=half),
+        [states, states, out((2, padded, LANES), F32), out((2 * padded, LANES), BF16)],
+        *[parts[k] for k in range(dests - 2)],
+    )
+    entry = prompts * keep + 16
+    own, to_next, to_pair, to_rest = call(
+        lambda *refs: hub_body(*refs, half=half, keep=keep),
+        [out((n, entry, STATE), BF16) for n in (1, 1, 2, 4)],
+        one,
+        two,
+        early_logs,
+        early_newest,
+        parts[dests - 2],
+        parts[dests - 1],
+        new_decay,
+        new_gate,
+    )
+
+    def hop(value, *moves):
+        pairs = [(h + i, h + j) for h in (0, half) for i, j in moves]
+        return lax.ppermute(value, "sp", pairs)
+
+    to_next = hop(to_next, (0, 1))
+    to_pair = hop(to_pair, (0, 2))
+    to_rest = hop(to_rest, (0, 4))
+    to_sixth = hop(to_rest, (4, 6))
+    to_odd = hop(to_pair[1:] + to_rest[1:2] + to_sixth[3:], (2, 3), (4, 5), (6, 7))
     tp_size = lax.axis_size(TP)
     cache, gated, squares = call(
-        lambda *refs: read_body(*refs, prompts=prompts),
+        lambda *refs: pick_body(*refs, half=half, keep=keep),
         [
             out((prompts * keep, STATE), BF16),
             out((8, LANES), F32),
             out((tp_size, 1, LANES), F32),
         ],
-        received,
-        newest,
-        new_decay,
-        new_gate,
-        name="read",
+        own,
+        to_next,
+        to_pair,
+        to_rest,
+        to_sixth,
+        to_odd,
     )
     squares = lax.all_to_all(squares, TP, 0, 0, tiled=True)
     (first_read,) = call(
-        final_body, [out((1, keep, prompts), BF16)], squares, gated, gated_norm_gain, name="final"
+        final_body, [out((1, keep, prompts), BF16)], squares, gated, gated_norm_gain
     )
     return cache.reshape(prompts, 1, keep, STATE), jnp.transpose(first_read, (2, 0, 1))
 

time: 166 us -> 191 us (1.15)
  waiting for transfers between devices: 0.01 us -> 81.3 us
  starting transfers between devices: 86.7 us -> 37.1 us
  blocking collectives: 56.2 us -> 42.6 us
  Pallas kernels: 21.4 us -> 25.5 us
  local copies, waits for them, and re-layouts: 0.64 us -> 2.56 us
    all_to_all x1 -> x0, starting transfers between devices: 83.6 us -> none  [shards(): newest = lax.all_to_all(newest, 'sp', 0, 0, tiled=True)]
    ppermute x0 -> x20, waiting for transfers between devices: none -> 81.3 us  [the longest x15 79.4 us: shards(): parts[k] = lax.ppermute(payload, 'sp', pairs)]
    ppermute x0 -> x20, starting transfers between devices: none -> 27.9 us  [the longest x15 22.7 us: shards(): parts[k] = lax.ppermute(payload, 'sp', pairs)]
    all_to_all x1 -> x0, blocking collectives: 23.2 us -> none  [shards(): received = lax.all_to_all(payload, 'sp', 0, 0, tiled=True)]
    all_to_all x1, blocking collectives: 33 us -> 42.6 us  [shards(): squares = lax.all_to_all(squares, TP, 0, 0, tiled=True)]
    ppermute x1, starting transfers between devices: 3.08 us -> 9.18 us  [shards(): halo = lax.ppermute(trail, 'sp', [(i, i + 1) for i in range(dests - 1)])]
    pallas_call x4 -> x6, Pallas kernels: 17.6 us -> 21.8 us  [call(): pl.pallas_call(body, in_specs=specs or whole(len(operands)), out_specs=wh...]
    unnamed x4 -> x42, local copies, waits for them, and re-layouts: 0.64 us -> 2.56 us
  transfers between devices with their start and end apart: 2 -> 21, of which waited for: 0 -> 12; matrix products, arithmetic and copies ran while one was open for 0% -> 0% of each run, Pallas kernels for 7% -> 7%
where the time goes in v3:
time: 191 us; the launch traced here: 190 us
  waiting for transfers between devices  81.3 us (43%)
  blocking collectives  42.6 us (22%)
  starting transfers between devices  37.1 us (19%)
  Pallas kernels  25.5 us (13%)
  local copies, waits for them, and re-layouts  2.56 us (1%)
    ppermute x15, waiting for transfers between devices, shards(): parts[k] = lax.ppermute(payload, 'sp', pairs)  79.4 us
    all_to_all x1, blocking collectives, shards(): squares = lax.all_to_all(squares, TP, 0, 0, tiled=True)  42.6 us
    ppermute x15, starting transfers between devices, shards(): parts[k] = lax.ppermute(payload, 'sp', pairs)  22.7 us
    pallas_call x6, Pallas kernels, call(): pl.pallas_call(body, in_specs=specs or whole(len(operands)), out_specs=wh...  21.8 us
    ppermute x1, starting transfers between devices, shards(): halo = lax.ppermute(trail, 'sp', [(i, i + 1) for i in range(dests - 1)])  9.18 us
    ppermute x5, starting transfers between devices, hop(): return lax.ppermute(value, 'sp', pairs)  5.22 us
  transfers between devices with their start and end apart: 21, of which 12 were waited for; matrix products, arithmetic and copies ran while one was open for 0% of the time, Pallas kernels for 7%

profile of v3, /device:TPU:5, one launch (start us, length us, event | category | flops | bytes accessed | tf_op | source)
XLA Modules:
  0.0 190.2 jit_solution(2115792128296615513)
XLA Ops:
  0.6 3.7 %token_.1 = (bf16[3,16,256]{2,1,0:T(8,128)(2,1)}, bf16[32,128]{1,0:T(8,128)(2,1)}, f32[16,128]{1,0:T(8,128)}, f32[16,64]{1,0:T(8,128)}) custom-call(bf16[12,128,2048]{2,1,0:T(8,128)(2,1)} %refs_0_.1, bf16[12,2048]{1,0:T(8,128)(2,1)} %next_ref.1, bf16[64,2048]{1,0:T(8,128)(2,1)} %bitcast.11, bf16[64,2048]{1,0:T(8,128)(2,1)} %bitcast.15, ...), custom_call_target="tpu_custom_call" | custom-call | tf_op jit(solution)/shard_map/token/pallas_call | solution.py:426
  4.4 9.2 %collective-permute-start = (bf16[3,16,256]{2,1,0:T(8,128)(2,1)}, bf16[3,16,256]{2,1,0:T(8,128)(2,1)S(1)}, u32[]{:S(2)}, u32[]{:S(2)}) collective-permute-start(bf16[3,16,256]{2,1,0:T(8,128)(2,1)} %get-tuple-element.22), channel_id=1, source_target_pairs={{0,32},{32,64},{64,96},{96,128},{128,160},{160,192},{192,224},{224... | collective-permute-start | bytes 73736 | tf_op jit(solution)/shard_map/ppermute | solution.py:444
  13.5 10.9 %shard_map.158 = (f32[12,64,128]{2,1,0:T(8,128)}, f32[3,16,256]{2,1,0:T(8,128)}, f32[3,16,128]{2,1,0:T(8,128)}, f32[16,128]{1,0:T(8,128)}, f32[8,256]{1,0:T(8,128)}) custom-call(bf16[12,128,2048]{2,1,0:T(8,128)(2,1)} %refs_0_.1, bf16[64,2048]{1,0:T(8,128)(2,1)} %bitcast.12, bf16[2048,256]{1,0:T(8,128)(2,1)} %refs_2_.1, bf16[32,2048]{1,0:T(8,128)(2,1)} %bitcast.14, ...), custom_call_target="tpu_custom_call" | custom-call | tf_op jit(solution)/shard_map/pallas_call | solution.py:370
  24.4 0.0 collective-permute-done.halo_ref
  24.4 0.6 copy-done.18
  25.0 2.1 %shard_map.159.refs_0_ = bf16[816,128]{1,0:T(8,128)(2,1)} custom-call(bf16[3,16,256]{2,1,0:T(8,128)(2,1)} %copy-done.18, f32[3,16,256]{2,1,0:T(8,128)} %get-tuple-element.23.lead_ref, f32[3,16,128]{2,1,0:T(8,128)} %get-tuple-element.24.lead_weight_ref, f32[16,128]{1,0:T(8,128)} %get-tuple-element.25.logs_ref, f32[8,256]{1,0:T(8,128)} %get-tuple-element.26.taps_ref, ...), custom_call_target="tpu_custom_call" | custom-call | tf_op jit(solution)/shard_map/pallas_call | solution.py:370
  27.1 1.3 collective-permute-start.1
  28.4 1.3 collective-permute-start.10
  29.7 1.3 collective-permute-start.11
  31.0 1.3 collective-permute-start.12
  32.3 1.3 collective-permute-start.13
  33.7 4.6 %collective-permute-done.1.refs_1_ = bf16[816,128]{1,0:T(8,128)(2,1)S(1)} collective-permute-done((bf16[816,128]{1,0:T(8,128)(2,1)}, bf16[816,128]{1,0:T(8,128)(2,1)S(1)}, u32[]{:S(2)}, u32[]{:S(2)}) %collective-permute-start.1) | collective-permute-done | bytes 208928 | tf_op jit(solution)/shard_map/ppermute | solution.py:486
  38.2 1.3 collective-permute-start.2
  39.5 52.8 %collective-permute-done.10.refs_10_ = bf16[816,128]{1,0:T(8,128)(2,1)S(1)} collective-permute-done((bf16[816,128]{1,0:T(8,128)(2,1)}, bf16[816,128]{1,0:T(8,128)(2,1)S(1)}, u32[]{:S(2)}, u32[]{:S(2)}) %collective-permute-start.10) | collective-permute-done | bytes 208928 | tf_op jit(solution)/shard_map/ppermute | solution.py:486
  92.3 1.3 collective-permute-start.3
  93.6 3.6 %collective-permute-done.11.refs_11_ = bf16[816,128]{1,0:T(8,128)(2,1)S(1)} collective-permute-done((bf16[816,128]{1,0:T(8,128)(2,1)}, bf16[816,128]{1,0:T(8,128)(2,1)S(1)}, u32[]{:S(2)}, u32[]{:S(2)}) %collective-permute-start.11) | collective-permute-done | bytes 208928 | tf_op jit(solution)/shard_map/ppermute | solution.py:486
  97.2 1.3 collective-permute-start.4
  98.5 2.5 %collective-permute-done.12.refs_12_ = bf16[816,128]{1,0:T(8,128)(2,1)S(1)} collective-permute-done((bf16[816,128]{1,0:T(8,128)(2,1)}, bf16[816,128]{1,0:T(8,128)(2,1)S(1)}, u32[]{:S(2)}, u32[]{:S(2)}) %collective-permute-start.12) | collective-permute-done | bytes 208928 | tf_op jit(solution)/shard_map/ppermute | solution.py:486
  101.1 1.3 collective-permute-start.5
  102.4 3.7 %collective-permute-done.13.refs_13_ = bf16[816,128]{1,0:T(8,128)(2,1)S(1)} collective-permute-done((bf16[816,128]{1,0:T(8,128)(2,1)}, bf16[816,128]{1,0:T(8,128)(2,1)S(1)}, u32[]{:S(2)}, u32[]{:S(2)}) %collective-permute-start.13) | collective-permute-done | bytes 208928 | tf_op jit(solution)/shard_map/ppermute | solution.py:486
  106.1 1.3 collective-permute-start.6
  107.4 1.3 collective-permute-start.7
  108.8 4.5 %collective-permute-start.8 = (bf16[816,128]{1,0:T(8,128)(2,1)}, bf16[816,128]{1,0:T(8,128)(2,1)S(1)}, u32[]{:S(2)}, u32[]{:S(2)}) collective-permute-start(bf16[816,128]{1,0:T(8,128)(2,1)} %shard_map.159.refs_0_), channel_id=1, source_target_pairs={{256,0},{0,256},{257,1},{1,257},{258,2},{2,258},{259,3},{3,259},{2... | collective-permute-start | bytes 626696 | tf_op jit(solution)/shard_map/ppermute | solution.py:486
  113.2 1.3 collective-permute-start.9
  114.6 1.3 collective-permute-start.14
  115.9 3.0 %collective-permute-done.6.refs_6_ = bf16[816,128]{1,0:T(8,128)(2,1)S(1)} collective-permute-done((bf16[816,128]{1,0:T(8,128)(2,1)}, bf16[816,128]{1,0:T(8,128)(2,1)S(1)}, u32[]{:S(2)}, u32[]{:S(2)}) %collective-permute-start.6) | collective-permute-done | bytes 208928 | tf_op jit(solution)/shard_map/ppermute | solution.py:486
  118.9 1.3 collective-permute-start.15
  120.2 0.7 collective-permute-done.7.refs_7_
  120.9 3.6 %collective-permute-done.8.refs_8_ = bf16[816,128]{1,0:T(8,128)(2,1)S(1)} collective-permute-done((bf16[816,128]{1,0:T(8,128)(2,1)}, bf16[816,128]{1,0:T(8,128)(2,1)S(1)}, u32[]{:S(2)}, u32[]{:S(2)}) %collective-permute-start.8) | collective-permute-done | bytes 208928 | tf_op jit(solution)/shard_map/ppermute | solution.py:486
  124.5 3.6 %collective-permute-done.9.refs_9_ = bf16[816,128]{1,0:T(8,128)(2,1)S(1)} collective-permute-done((bf16[816,128]{1,0:T(8,128)(2,1)}, bf16[816,128]{1,0:T(8,128)(2,1)S(1)}, u32[]{:S(2)}, u32[]{:S(2)}) %collective-permute-start.9) | collective-permute-done | bytes 208928 | tf_op jit(solution)/shard_map/ppermute | solution.py:486
  128.2 0.7 copy-done.14
  128.9 3.3 %shard_map.160 = (f32[12,64,128]{2,1,0:T(8,128)}, f32[12,64,128]{2,1,0:T(8,128)}, f32[2,16,128]{2,1,0:T(8,128)}, bf16[32,128]{1,0:T(8,128)(2,1)}) custom-call(bf16[816,128]{1,0:T(8,128)(2,1)} %shard_map.159.refs_0_, bf16[816,128]{1,0:T(8,128)(2,1)} %copy-done, bf16[816,128]{1,0:T(8,128)(2,1)} %copy-done.5, bf16[816,128]{1,0:T(8,128)(2,1)} %copy-done.6, ...), custom_call_target="tpu_custom_call" | custom-call | tf_op jit(solution)/shard_map/pallas_call | solution.py:370
  132.2 1.2 collective-permute-done.15.refs_5_
  133.4 0.7 copy-done.13
  134.1 2.5 %shard_map.161 = (bf16[1,64,128]{2,1,0:T(8,128)(2,1)}, bf16[1,64,128]{2,1,0:T(8,128)(2,1)}, bf16[2,64,128]{2,1,0:T(8,128)(2,1)}, bf16[4,64,128]{2,1,0:T(8,128)(2,1)}) custom-call(f32[12,64,128]{2,1,0:T(8,128)} %get-tuple-element.29.refs_0_, f32[12,64,128]{2,1,0:T(8,128)} %get-tuple-element.30.refs_1_, f32[2,16,128]{2,1,0:T(8,128)} %get-tuple-element.31.refs_2_, ...), custom_call_target="tpu_custom_call" | custom-call | tf_op jit(solution)/shard_map/pallas_call | solution.py:370
  136.6 1.3 collective-permute-start.18
  137.9 1.6 collective-permute-done.18.refs_3_
  139.5 0.7 collective-permute-start.19
  140.2 1.3 collective-permute-start.17
  141.5 1.3 collective-permute-start.16
  142.8 0.0 collective-permute-done.17.refs_2_
  142.9 0.7 collective-permute-start.20
  143.6 0.3 collective-permute-done.16.refs_1_
  143.9 0.6 copy-done.19
  144.5 0.0 copy-done.20
  144.5 1.7 shard_map.162
  146.2 42.6 %all_to_all.5.parts_ref = f32[32,1,128]{2,1,0:T(1,128)} all-to-all(f32[32,1,128]{2,1,0:T(1,128)} %get-tuple-element.40), channel_id=1, replica_groups=mesh['grp'=2,'sp'=16,'tp_0'=16,'tp_1'=2] {'tp_0','tp_1'}, dimensions={0} | all-to-all | bytes 32768 | tf_op jit(solution)/shard_map/all_to_all | solution.py:531
  188.8 1.4 shard_map.163
  (45 shorter events, 0.1 us)
Async XLA Ops:
  4.4 20.1 %collective-permute-start = (bf16[3,16,256]{2,1,0:T(8,128)(2,1)}, bf16[3,16,256]{2,1,0:T(8,128)(2,1)S(1)}, u32[]{:S(2)}, u32[]{:S(2)}) collective-permute-start(bf16[3,16,256]{2,1,0:T(8,128)(2,1)} %get-tuple-element.22), channel_id=1, source_target_pairs={{0,32},{32,64},{64,96},{96,128},{128,160},{160,192},{192,224},{224... | collective-permute-start | bytes 73736 | tf_op jit(solution)/shard_map/ppermute | solution.py:444
  24.4 0.6 copy-start.18
  27.1 11.1 %collective-permute-start.1 = (bf16[816,128]{1,0:T(8,128)(2,1)}, bf16[816,128]{1,0:T(8,128)(2,1)S(1)}, u32[]{:S(2)}, u32[]{:S(2)}) collective-permute-start(bf16[816,128]{1,0:T(8,128)(2,1)} %shard_map.159.refs_0_), channel_id=1, source_target_pairs={{32,0},{288,256},{33,1},{289,257},{34,2},{290,258},{35,3},{291,259... | collective-permute-start | bytes 626696 | tf_op jit(solution)/shard_map/ppermute | solution.py:486
  28.4 63.9 %collective-permute-start.10 = (bf16[816,128]{1,0:T(8,128)(2,1)}, bf16[816,128]{1,0:T(8,128)(2,1)S(1)}, u32[]{:S(2)}, u32[]{:S(2)}) collective-permute-start(bf16[816,128]{1,0:T(8,128)(2,1)} %shard_map.159.refs_0_), channel_id=1, source_target_pairs={{320,0},{64,256},{321,1},{65,257},{322,2},{66,258},{323,3},{67,259... | collective-permute-start | bytes 626696 | tf_op jit(solution)/shard_map/ppermute | solution.py:486
  29.7 67.5 %collective-permute-start.11 = (bf16[816,128]{1,0:T(8,128)(2,1)}, bf16[816,128]{1,0:T(8,128)(2,1)S(1)}, u32[]{:S(2)}, u32[]{:S(2)}) collective-permute-start(bf16[816,128]{1,0:T(8,128)(2,1)} %shard_map.159.refs_0_), channel_id=1, source_target_pairs={{352,0},{96,256},{353,1},{97,257},{354,2},{98,258},{355,3},{99,259... | collective-permute-start | bytes 626696 | tf_op jit(solution)/shard_map/ppermute | solution.py:486
  31.0 70.0 %collective-permute-start.12 = (bf16[816,128]{1,0:T(8,128)(2,1)}, bf16[816,128]{1,0:T(8,128)(2,1)S(1)}, u32[]{:S(2)}, u32[]{:S(2)}) collective-permute-start(bf16[816,128]{1,0:T(8,128)(2,1)} %shard_map.159.refs_0_), channel_id=1, source_target_pairs={{384,0},{128,256},{385,1},{129,257},{386,2},{130,258},{387,3},{131... | collective-permute-start | bytes 626696 | tf_op jit(solution)/shard_map/ppermute | solution.py:486
  32.3 73.8 %collective-permute-start.13 = (bf16[816,128]{1,0:T(8,128)(2,1)}, bf16[816,128]{1,0:T(8,128)(2,1)S(1)}, u32[]{:S(2)}, u32[]{:S(2)}) collective-permute-start(bf16[816,128]{1,0:T(8,128)(2,1)} %shard_map.159.refs_0_), channel_id=1, source_target_pairs={{416,0},{160,256},{417,1},{161,257},{418,2},{162,258},{419,3},{163... | collective-permute-start | bytes 626696 | tf_op jit(solution)/shard_map/ppermute | solution.py:486
  38.2 89.9 %copy-start = (bf16[816,128]{1,0:T(8,128)(2,1)}, bf16[816,128]{1,0:T(8,128)(2,1)S(1)}, u32[]{:S(2)}) copy-start(bf16[816,128]{1,0:T(8,128)(2,1)S(1)} %collective-permute-done.1.refs_1_) | copy-start | bytes 626692
  38.2 69.2 %collective-permute-start.2 = (bf16[816,128]{1,0:T(8,128)(2,1)}, bf16[816,128]{1,0:T(8,128)(2,1)S(1)}, u32[]{:S(2)}, u32[]{:S(2)}) collective-permute-start(bf16[816,128]{1,0:T(8,128)(2,1)} %shard_map.159.refs_0_), channel_id=1, source_target_pairs={{64,0},{320,256},{65,1},{321,257},{66,2},{322,258},{67,3},{323,259... | collective-permute-start | bytes 626696 | tf_op jit(solution)/shard_map/ppermute | solution.py:486
  92.3 35.8 %copy-start.1 = (bf16[816,128]{1,0:T(8,128)(2,1)}, bf16[816,128]{1,0:T(8,128)(2,1)S(1)}, u32[]{:S(2)}) copy-start(bf16[816,128]{1,0:T(8,128)(2,1)S(1)} %collective-permute-done.10.refs_10_) | copy-start | bytes 626692
  92.3 16.4 %collective-permute-start.3 = (bf16[816,128]{1,0:T(8,128)(2,1)}, bf16[816,128]{1,0:T(8,128)(2,1)S(1)}, u32[]{:S(2)}, u32[]{:S(2)}) collective-permute-start(bf16[816,128]{1,0:T(8,128)(2,1)} %shard_map.159.refs_0_), channel_id=1, source_target_pairs={{96,0},{352,256},{97,1},{353,257},{98,2},{354,258},{99,3},{355,259... | collective-permute-start | bytes 626696 | tf_op jit(solution)/shard_map/ppermute | solution.py:486
  97.2 30.9 %copy-start.2 = (bf16[816,128]{1,0:T(8,128)(2,1)}, bf16[816,128]{1,0:T(8,128)(2,1)S(1)}, u32[]{:S(2)}) copy-start(bf16[816,128]{1,0:T(8,128)(2,1)S(1)} %collective-permute-done.11.refs_11_) | copy-start | bytes 626692
  97.2 16.0 %collective-permute-start.4 = (bf16[816,128]{1,0:T(8,128)(2,1)}, bf16[816,128]{1,0:T(8,128)(2,1)S(1)}, u32[]{:S(2)}, u32[]{:S(2)}) collective-permute-start(bf16[816,128]{1,0:T(8,128)(2,1)} %shard_map.159.refs_0_), channel_id=1, source_target_pairs={{128,0},{384,256},{129,1},{385,257},{130,2},{386,258},{131,3},{387... | collective-permute-start | bytes 626696 | tf_op jit(solution)/shard_map/ppermute | solution.py:486
  101.1 27.1 %copy-start.3 = (bf16[816,128]{1,0:T(8,128)(2,1)}, bf16[816,128]{1,0:T(8,128)(2,1)S(1)}, u32[]{:S(2)}) copy-start(bf16[816,128]{1,0:T(8,128)(2,1)S(1)} %collective-permute-done.12.refs_12_) | copy-start | bytes 626692
  101.1 13.5 %collective-permute-start.5 = (bf16[816,128]{1,0:T(8,128)(2,1)}, bf16[816,128]{1,0:T(8,128)(2,1)S(1)}, u32[]{:S(2)}, u32[]{:S(2)}) collective-permute-start(bf16[816,128]{1,0:T(8,128)(2,1)} %shard_map.159.refs_0_), channel_id=1, source_target_pairs={{160,0},{416,256},{161,1},{417,257},{162,2},{418,258},{163,3},{419... | collective-permute-start | bytes 626696 | tf_op jit(solution)/shard_map/ppermute | solution.py:486
  106.1 22.0 %copy-start.4 = (bf16[816,128]{1,0:T(8,128)(2,1)}, bf16[816,128]{1,0:T(8,128)(2,1)S(1)}, u32[]{:S(2)}) copy-start(bf16[816,128]{1,0:T(8,128)(2,1)S(1)} %collective-permute-done.13.refs_13_) | copy-start | bytes 626692
  106.1 12.8 %collective-permute-start.6 = (bf16[816,128]{1,0:T(8,128)(2,1)}, bf16[816,128]{1,0:T(8,128)(2,1)S(1)}, u32[]{:S(2)}, u32[]{:S(2)}) collective-permute-start(bf16[816,128]{1,0:T(8,128)(2,1)} %shard_map.159.refs_0_), channel_id=1, source_target_pairs={{192,0},{448,256},{193,1},{449,257},{194,2},{450,258},{195,3},{451... | collective-permute-start | bytes 626696 | tf_op jit(solution)/shard_map/ppermute | solution.py:486
  107.4 20.7 %copy-start.5 = (bf16[816,128]{1,0:T(8,128)(2,1)}, bf16[816,128]{1,0:T(8,128)(2,1)S(1)}, u32[]{:S(2)}) copy-start(bf16[816,128]{1,0:T(8,128)(2,1)S(1)} %collective-permute-done.2.refs_2_) | copy-start | bytes 626692
  107.4 13.5 %collective-permute-start.7 = (bf16[816,128]{1,0:T(8,128)(2,1)}, bf16[816,128]{1,0:T(8,128)(2,1)S(1)}, u32[]{:S(2)}, u32[]{:S(2)}) collective-permute-start(bf16[816,128]{1,0:T(8,128)(2,1)} %shard_map.159.refs_0_), channel_id=1, source_target_pairs={{224,0},{480,256},{225,1},{481,257},{226,2},{482,258},{227,3},{483... | collective-permute-start | bytes 626696 | tf_op jit(solution)/shard_map/ppermute | solution.py:486
  108.8 19.4 %copy-start.6 = (bf16[816,128]{1,0:T(8,128)(2,1)}, bf16[816,128]{1,0:T(8,128)(2,1)S(1)}, u32[]{:S(2)}) copy-start(bf16[816,128]{1,0:T(8,128)(2,1)S(1)} %collective-permute-done.3.refs_3_) | copy-start | bytes 626692
  108.8 15.8 %collective-permute-start.8 = (bf16[816,128]{1,0:T(8,128)(2,1)}, bf16[816,128]{1,0:T(8,128)(2,1)S(1)}, u32[]{:S(2)}, u32[]{:S(2)}) collective-permute-start(bf16[816,128]{1,0:T(8,128)(2,1)} %shard_map.159.refs_0_), channel_id=1, source_target_pairs={{256,0},{0,256},{257,1},{1,257},{258,2},{2,258},{259,3},{3,259},{2... | collective-permute-start | bytes 626696 | tf_op jit(solution)/shard_map/ppermute | solution.py:486
  113.2 14.9 %copy-start.7 = (bf16[816,128]{1,0:T(8,128)(2,1)}, bf16[816,128]{1,0:T(8,128)(2,1)S(1)}, u32[]{:S(2)}) copy-start(bf16[816,128]{1,0:T(8,128)(2,1)S(1)} %collective-permute-done.4.refs_4_) | copy-start | bytes 626692
  113.2 14.9 %collective-permute-start.9 = (bf16[816,128]{1,0:T(8,128)(2,1)}, bf16[816,128]{1,0:T(8,128)(2,1)S(1)}, u32[]{:S(2)}, u32[]{:S(2)}) collective-permute-start(bf16[816,128]{1,0:T(8,128)(2,1)} %shard_map.159.refs_0_), channel_id=1, source_target_pairs={{288,0},{32,256},{289,1},{33,257},{290,2},{34,258},{291,3},{35,259... | collective-permute-start | bytes 626696 | tf_op jit(solution)/shard_map/ppermute | solution.py:486
  114.6 13.6 %copy-start.8 = (bf16[816,128]{1,0:T(8,128)(2,1)}, bf16[816,128]{1,0:T(8,128)(2,1)S(1)}, u32[]{:S(2)}) copy-start(bf16[816,128]{1,0:T(8,128)(2,1)S(1)} %collective-permute-done.5.refs_5_) | copy-start | bytes 626692
  114.6 17.6 %collective-permute-start.14 = (bf16[816,128]{1,0:T(8,128)(2,1)}, bf16[816,128]{1,0:T(8,128)(2,1)S(1)}, u32[]{:S(2)}, u32[]{:S(2)}) collective-permute-start(bf16[816,128]{1,0:T(8,128)(2,1)} %shard_map.159.refs_0_), channel_id=1, source_target_pairs={{448,0},{192,256},{449,1},{193,257},{450,2},{194,258},{451,3},{195... | collective-permute-start | bytes 626696 | tf_op jit(solution)/shard_map/ppermute | solution.py:486
  118.9 9.3 %copy-start.9 = (bf16[816,128]{1,0:T(8,128)(2,1)}, bf16[816,128]{1,0:T(8,128)(2,1)S(1)}, u32[]{:S(2)}) copy-start(bf16[816,128]{1,0:T(8,128)(2,1)S(1)} %collective-permute-done.6.refs_6_) | copy-start | bytes 626692
  118.9 14.5 %collective-permute-start.15 = (bf16[816,128]{1,0:T(8,128)(2,1)}, bf16[816,128]{1,0:T(8,128)(2,1)S(1)}, u32[]{:S(2)}, u32[]{:S(2)}) collective-permute-start(bf16[816,128]{1,0:T(8,128)(2,1)} %shard_map.159.refs_0_), channel_id=1, source_target_pairs={{480,0},{224,256},{481,1},{225,257},{482,2},{226,258},{483,3},{227... | collective-permute-start | bytes 626696 | tf_op jit(solution)/shard_map/ppermute | solution.py:486
  120.9 7.3 %copy-start.10 = (bf16[816,128]{1,0:T(8,128)(2,1)}, bf16[816,128]{1,0:T(8,128)(2,1)S(1)}, u32[]{:S(2)}) copy-start(bf16[816,128]{1,0:T(8,128)(2,1)S(1)} %collective-permute-done.7.refs_7_) | copy-start | bytes 626692
  124.5 3.7 %copy-start.12 = (bf16[816,128]{1,0:T(8,128)(2,1)}, bf16[816,128]{1,0:T(8,128)(2,1)S(1)}, u32[]{:S(2)}) copy-start(bf16[816,128]{1,0:T(8,128)(2,1)S(1)} %collective-permute-done.8.refs_8_) | copy-start | bytes 626692
  128.2 0.7 copy-start.14
  132.2 1.2 copy-start.11
  133.4 0.7 copy-start.13
  136.6 2.9 %collective-permute-start.18 = (bf16[4,64,128]{2,1,0:T(8,128)(2,1)}, bf16[4,64,128]{2,1,0:T(8,128)(2,1)S(1)}, u32[]{:S(2)}, u32[]{:S(2)}) collective-permute-start(bf16[4,64,128]{2,1,0:T(8,128)(2,1)} %get-tuple-element.38), channel_id=1, source_target_pairs={{0,128},{256,384},{1,129},{257,385},{2,130},{258,386},{3,131},{259... | collective-permute-start | bytes 196616 | tf_op jit(solution)/shard_map/ppermute | solution.py:509
  139.5 4.4 %copy-start.15 = (bf16[4,64,128]{2,1,0:T(8,128)(2,1)}, bf16[4,64,128]{2,1,0:T(8,128)(2,1)S(1)}, u32[]{:S(2)}) copy-start(bf16[4,64,128]{2,1,0:T(8,128)(2,1)S(1)} %collective-permute-done.18.refs_3_) | copy-start | bytes 196612
  139.5 3.3 %collective-permute-start.19 = (bf16[4,64,128]{2,1,0:T(8,128)(2,1)S(1)}, bf16[4,64,128]{2,1,0:T(8,128)(2,1)S(1)}, u32[]{:S(2)}, u32[]{:S(2)}) collective-permute-start(bf16[4,64,128]{2,1,0:T(8,128)(2,1)S(1)} %collective-permute-done.18.refs_3_), channel_id=1, source_target_pairs={{128,192},{384,448},{129,193},{385,449},{130,194},{386,450},{131,1... | collective-permute-start | bytes 196616 | tf_op jit(solution)/shard_map/ppermute | solution.py:509
  140.2 2.6 %collective-permute-start.17 = (bf16[2,64,128]{2,1,0:T(8,128)(2,1)}, bf16[2,64,128]{2,1,0:T(8,128)(2,1)S(1)}, u32[]{:S(2)}, u32[]{:S(2)}) collective-permute-start(bf16[2,64,128]{2,1,0:T(8,128)(2,1)} %get-tuple-element.37), channel_id=1, source_target_pairs={{0,64},{256,320},{1,65},{257,321},{2,66},{258,322},{3,67},{259,323... | collective-permute-start | bytes 98312 | tf_op jit(solution)/shard_map/ppermute | solution.py:509
  141.5 2.4 %collective-permute-start.16 = (bf16[1,64,128]{2,1,0:T(8,128)(2,1)}, bf16[1,64,128]{2,1,0:T(8,128)(2,1)S(1)}, u32[]{:S(2)}, u32[]{:S(2)}) collective-permute-start(bf16[1,64,128]{2,1,0:T(8,128)(2,1)} %get-tuple-element.36), channel_id=1, source_target_pairs={{0,32},{256,288},{1,33},{257,289},{2,34},{258,290},{3,35},{259,291... | collective-permute-start | bytes 49160 | tf_op jit(solution)/shard_map/ppermute | solution.py:509
  142.8 1.1 copy-start.17
  142.9 1.1 copy-start.16
  142.9 1.0 collective-permute-start.20
  143.9 0.6 copy-start.19
  143.9 0.6 copy-start.20

commit v4 on v3

--- a/solution.py
+++ b/solution.py
@@ -43,11 +43,6 @@
     return first, second, third
 
 
-def dot01(matrix, value):
-    a, b, c = pieces(value)
-    return dot(jnp.concatenate([matrix] * 3, axis=1), jnp.concatenate([a, b, c], axis=0))
-
-
 def iota(shape, dim):
     return lax.broadcasted_iota(jnp.int32, shape, dim)
 
@@ -66,79 +61,84 @@
 
 
 def local_body(
-    x_hbm, value_ref, key_ref, step_ref, vt_ref, kt_ref, bias_ref, decay_ref, off_ref,
-    state_ref, lead_ref, lead_weight_ref, logs_ref, taps_ref,
-    x_ref, w_ref, sems, *, per,
+    x_hbm, key_hbm, value_ref, step_ref, vt_ref, kt_ref, bias_ref, decay_ref, off_ref,
+    state_ref, lead_ref, weight_ref, logs_ref, taps_ref,
+    x_ref, w_ref, wide_ref, map_ref, rows_ref, key_sem, sems, *, per,
 ):
     prompts, length, width = x_hbm.shape
+    head = lax.axis_index(TP)
+    group = head // (HEADS // GROUPS)
+    at = pl.multiple_of(group * STATE, STATE)
+    key_copy = pltpu.make_async_copy(
+        key_hbm.at[:, pl.ds(at, STATE)], w_ref.at[:, pl.ds(LANES, STATE)], key_sem
+    )
+    key_copy.start()
     copies = []
     for i in range(prompts // per):
         part = pl.ds(i * per, per)
         copies.append(pltpu.make_async_copy(x_hbm.at[part], x_ref.at[part], sems.at[i]))
     for copy in copies:
         copy.start()
-    head = lax.axis_index(TP)
-    group = head // (HEADS // GROUPS)
     step_row = jnp.broadcast_to(pick_row(step_ref[...], head), (P_SIZE, width)).astype(BF16)
     w_ref[:, :LANES] = jnp.transpose(jnp.concatenate([value_ref[...], step_row], axis=0))
-    logs_ref[...] = jnp.zeros_like(logs_ref)
-    at = pl.multiple_of(group * STATE, STATE)
-    w_ref[:, LANES:] = key_ref[:, pl.ds(at, STATE)]
     pair = pl.multiple_of((head // 2) * LANES, LANES)
     value_taps = own_half(vt_ref[:, pl.ds(pair, LANES)].astype(F32), head)
     taps = jnp.concatenate([value_taps, kt_ref[:, pl.ds(at, STATE)].astype(F32)], axis=1)
     taps_ref[:CONV] = taps
-    bias = pick(bias_ref[...], head)
-    speed = jnp.exp(pick(decay_ref[...], head))
-    later = (iota((length, length), 1) > iota((length, length), 0)).astype(BF16)
-    position = iota((length, LANES), 0)
+    rows_ref[...] = jnp.zeros_like(rows_ref)
+    offset = off_ref[...]
+    offset = jnp.where(iota(offset.shape, 1) == head, offset, 0.0)
+    rows_ref[1, :prompts] = jnp.sum(offset, axis=1)
+    feature = iota((length, LANES), 1) < P_SIZE
+    key_copy.wait()
     for i in range(prompts // per):
         copies[i].wait()
         rows = x_ref[i * per : (i + 1) * per].reshape(per * length, width)
         raw_all = rounded(dot(rows, w_ref[...]))
-        steps, logs, mixes = [], [], []
         for j in range(per):
             b = i * per + j
             raw = raw_all[j * length : (j + 1) * length]
             for k in range(CONV - 1):
                 lead_ref[k, b : b + 1, :] = raw[k : k + 1]
-            step = softplus(pltpu.roll(raw[:, :LANES], 64, axis=1) + bias)
-            offset = jnp.broadcast_to(pick_row(off_ref[b], head), (length, length))
-            log = jnp.transpose(offset) - speed * step
             total = raw * taps[CONV - 1 : CONV]
             for k in range(CONV - 1):
                 total = total + pltpu.roll(raw, CONV - 1 - k, axis=0) * taps[k : k + 1]
-            steps.append(step)
-            logs.append(log)
-            mixes.append(rounded(silu(total)))
-        after = dot01(later, jnp.concatenate(logs, axis=1))
-        for j in range(per):
-            b = i * per + j
-            after_here = after[:, j * LANES : (j + 1) * LANES]
-            weight = jnp.exp(after_here) * steps[j]
-            logs_ref[b : b + 1, :] = after_here[:1] + logs[j][:1]
-            for k in range(CONV - 1):
-                lead_weight_ref[k, b : b + 1, :] = weight[k : k + 1]
-            weighted = jnp.where(position >= CONV - 1, mixes[j][:, :LANES] * weight, 0.0)
-            state = dot(
-                weighted.astype(BF16), mixes[j][:, LANES:].astype(BF16), ((0,), (0,))
-            )
-            state_ref[b] = state[:P_SIZE]
+            mixed = silu(total)
+            map_ref[b] = mixed[:, LANES:].astype(BF16)
+            turned = jnp.where(feature, rounded(mixed[:, :LANES]), raw[:, :LANES])
+            turned = jnp.transpose(turned)
+            wide_ref[b] = turned[:P_SIZE]
+            rows_ref[0, b : b + 1, :] = turned[P_SIZE : P_SIZE + 1]
+    step = softplus(rows_ref[0] + pick(bias_ref[...], head))
+    log = rows_ref[1] - jnp.exp(pick(decay_ref[...], head)) * step
+    later = (iota((length, length), 0) > iota((length, length), 1)).astype(BF16)
+    after = dot(jnp.concatenate(pieces(log), axis=1), jnp.concatenate([later] * 3, axis=0))
+    weight = jnp.exp(after) * step
+    weight_ref[...] = weight
+    logs_ref[...] = jnp.broadcast_to(jnp.sum(log, axis=1, keepdims=True), logs_ref.shape)
+    weight = jnp.where(iota(weight.shape, 1) >= CONV - 1, weight, 0.0)
+    for b in range(prompts):
+        weighted = (wide_ref[b] * weight[b : b + 1]).astype(BF16)
+        state_ref[b] = dot(weighted, map_ref[b])
 
 
 def token_body(
-    x_ref, next_ref, value_ref, gate_ref, key_ref, query_ref, step_ref, vt_ref, kt_ref, qt_ref,
+    key_hbm, query_hbm, x_ref, next_ref, value_ref, gate_ref, step_ref, vt_ref, kt_ref, qt_ref,
     bias_ref, decay_ref, skip_ref,
     trail_ref, newest_ref, decay_out_ref, gate_out_ref,
-    pad_ref, last_ref,
+    pad_ref, last_ref, key_ref, query_ref, sems,
 ):
     prompts, block, width = x_ref.shape
     head = lax.axis_index(TP)
     group = head // (HEADS // GROUPS)
     at = pl.multiple_of(group * STATE, STATE)
     pair = pl.multiple_of((head // 2) * LANES, LANES)
-    query = query_ref[:, pl.ds(at, STATE)]
-    key = key_ref[:, pl.ds(at, STATE)]
+    copies = [
+        pltpu.make_async_copy(source.at[:, pl.ds(at, STATE)], target, sems.at[i])
+        for i, (source, target) in enumerate(((key_hbm, key_ref), (query_hbm, query_ref)))
+    ]
+    for copy in copies:
+        copy.start()
     value_taps = own_half(vt_ref[:, pl.ds(pair, LANES)].astype(F32), head)[:, :P_SIZE]
     key_taps = kt_ref[:, pl.ds(at, STATE)].astype(F32)
     query_taps = qt_ref[:, pl.ds(at, STATE)].astype(F32)
@@ -148,10 +148,12 @@
     rows = jnp.concatenate([x_ref[...].reshape(prompts * block, width), token], axis=0)
     count = prompts * block
     values = rounded(dot(rows, value_ref[...], ((1,), (1,))))
-    keys = rounded(dot(rows, key))
-    queries = rounded(dot(rows, query))
     new_step = pick(rounded(dot(token, step_ref[...], ((1,), (1,)))), head)
     new_gate = rounded(dot(token, gate_ref[...], ((1,), (1,))))
+    copies[0].wait()
+    keys = rounded(dot(rows, key_ref[...]))
+    copies[1].wait()
+    queries = rounded(dot(rows, query_ref[...]))
     last_ref[...] = jnp.zeros_like(last_ref)
     for b in range(prompts):
         at_row = (b + 1) * block - (CONV - 1)
@@ -184,7 +186,7 @@
 
 
 def pack_body(
-    halo_ref, lead_ref, lead_weight_ref, logs_ref, taps_ref, state_ref, newest_ref, out_ref,
+    halo_ref, lead_ref, weight_ref, logs_ref, taps_ref, state_ref, newest_ref, out_ref,
 ):
     prompts, rows, _ = state_ref.shape
     padded = logs_ref.shape[0]
@@ -197,7 +199,8 @@
         for k in range(1, CONV):
             total = total + window[t + k] * taps[k : k + 1]
         mixed = rounded(silu(total))
-        weighted.append(jnp.transpose(rounded(mixed[:, :LANES] * lead_weight_ref[t])))
+        weight = pick(weight_ref[...], t)
+        weighted.append(jnp.transpose(rounded(mixed[:, :LANES] * weight)))
         maps.append(mixed[:, LANES:])
     for b in range(prompts):
         state = state_ref[b]
@@ -229,55 +232,38 @@
 def joined_shards(refs, base, padded, prompts):
     rows = base // prompts
     states = [refs[0][b * rows : (b + 1) * rows].astype(F32) for b in range(prompts)]
-    logs = log_of(refs[0], base, padded)
     for ref in refs[1:]:
-        log = log_of(ref, base, padded)
-        logs = logs + log
-        states = followed(states, ref, log)
-    return states, logs
-
-
-def early_body(*refs, prompts, padded, half):
-    parts, (one_ref, two_ref, logs_ref, newest_ref) = refs[:-4], refs[-4:]
-    base = prompts * P_SIZE
-    one, one_log = joined_shards(parts[:half], base, padded, prompts)
-    two, two_log = joined_shards(parts[half:], base, padded, prompts)
+        states = followed(states, ref, log_of(ref, base, padded))
+    return states
+
+
+def early_body(*refs, prompts, padded):
+    parts, state_ref = refs[:-1], refs[-1]
+    states = joined_shards(parts, prompts * P_SIZE, padded, prompts)
     for b in range(prompts):
-        one_ref[b] = one[b]
-        two_ref[b] = two[b]
-    logs_ref[0] = one_log
-    logs_ref[1] = two_log
-    newest_ref[...] = parts[half - 1][base + padded :]
+        state_ref[b] = states[b]
 
 
 def hub_body(
-    one_ref, two_ref, logs_ref, newest_ref, before_ref, last_ref, decay_ref, gate_ref,
-    own_ref, next_ref, pair_ref, rest_ref, *, half, keep,
+    state_ref, before_ref, last_ref, decay_ref, gate_ref, own_ref, *next_refs, keep,
 ):
-    prompts, rows, _ = one_ref.shape
+    prompts, rows, _ = state_ref.shape
     padded = decay_ref.shape[0]
+    dests = rows // keep
     base = prompts * rows
-    low = lax.axis_index("sp") < half
-    two_log = logs_ref[1]
-    two = [two_ref[b] for b in range(prompts)]
+    states = [state_ref[b] for b in range(prompts)]
     for ref in (before_ref, last_ref):
-        log = log_of(ref, base, padded)
-        two_log = two_log + log
-        two = followed(two, ref, log)
-    one_decay = jnp.exp(jnp.where(low, two_log, 0.0))
-    two_decay = jnp.exp(jnp.where(low, 0.0, logs_ref[0]))
-    newest = jnp.where(
-        low, last_ref[base + padded :].astype(F32), newest_ref[...].astype(F32)
-    )
+        states = followed(states, ref, log_of(ref, base, padded))
+    newest = last_ref[base + padded :].astype(F32)
     new_out = newest[:padded]
     lane = iota((rows, LANES), 1)
     reads = jnp.zeros((rows, LANES), F32)
     kept = []
     for b in range(prompts):
-        state = rounded(one_ref[b] * one_decay[b : b + 1] + two[b] * two_decay[b : b + 1])
+        state = rounded(states[b])
         read = jnp.sum(state * new_out[b : b + 1], axis=1, keepdims=True)
         reads = jnp.where(lane == b, read, reads)
-        kept.append(jnp.where(low, state[: rows // 2], state[rows // 2 :]))
+        kept.append(state)
     corner = (padded, LANES)
     decay = jnp.where(iota(corner, 0) == iota(corner, 1), decay_ref[...], 0.0)
     decay = jnp.sum(decay, axis=0, keepdims=True)
@@ -288,13 +274,12 @@
     gate = jnp.transpose(jnp.concatenate([gate, below], axis=0))[:rows]
     gated = jnp.where(lane < prompts, (decay * reads + direct) * gate, 0.0)
     squares = jnp.sum(gated * gated, axis=0, keepdims=True)
-    gated = jnp.where(low, gated[: rows // 2], gated[rows // 2 :])
-    count = rows // 2
+    count = rows
     square_rows = jnp.zeros(corner, F32)
     for k, part in enumerate(pieces(squares)):
         square_rows = jnp.where(iota(corner, 0) == k, part.astype(F32), square_rows)
     stack = jnp.concatenate([*pieces(gated), square_rows.astype(BF16)], axis=0)
-    chosen = (16 * half, stack.shape[0])
+    chosen = (16 * dests, stack.shape[0])
     dest, at, col = iota(chosen, 0) // 16, iota(chosen, 0) % 16, iota(chosen, 1)
     source = jnp.where(
         at < 3 * keep,
@@ -304,11 +289,8 @@
     extra = dot((col == source).astype(BF16), stack).astype(BF16)
 
     def place(dest):
-        if dest == 0:
-            return own_ref, 0
-        if dest == 1:
-            return next_ref, 0
-        return (pair_ref, dest - 2) if dest < 4 else (rest_ref, dest - 4)
+        level = dest.bit_length()
+        return ((own_ref, *next_refs)[level], dest - (1 << level >> 1))
 
     pair_rows = 2 * keep
     blocks = count // pair_rows
@@ -322,20 +304,18 @@
             for dest, value in ((2 * k, even[k]), (2 * k + 1, odd[k])):
                 ref, i = place(dest)
                 ref[i, b * keep : (b + 2) * keep, :] = value
-    for d in range(half):
+    for d in range(dests):
         ref, i = place(d)
         ref[i, prompts * keep :, :] = extra[d * 16 : (d + 1) * 16]
 
 
-def pick_body(
-    own_ref, next_ref, pair_ref, rest_ref, sixth_ref, odd_ref,
-    cache_ref, gated_ref, squares_ref, *, half, keep,
-):
+def pick_body(own_ref, *refs, places, keep):
+    parts, (cache_ref, gated_ref, squares_ref) = refs[:-3], refs[-3:]
     rows = cache_ref.shape[0]
-    at_hub = lax.axis_index("sp") % half == 0
+    at_hub = lax.axis_index("sp") == 0
     mine = jnp.where(at_hub, own_ref[0].astype(F32), 0.0)
-    for value in (next_ref[0], pair_ref[0], rest_ref[0], sixth_ref[2], odd_ref[0]):
-        mine = mine + value.astype(F32)
+    for part, place in zip(parts, places):
+        mine = mine + part[place].astype(F32)
     mine = mine.astype(BF16)
     cache_ref[...] = mine[:rows]
     shape = (8, 16)
@@ -409,12 +389,12 @@
     block = 16
     tail = length // block - 1
     token_operands = (
+        key_projection,
+        query_projection,
         prompt_layer_input,
         next_token_input,
         value_rows,
         gate_rows,
-        key_projection,
-        query_projection,
         step_rows,
         value_filter_taps,
         key_filter_taps,
@@ -426,8 +406,9 @@
     trail, newest, new_decay, new_gate = pl.pallas_call(
         token_body,
         grid=(1,),
-        in_specs=[pl.BlockSpec((prompts, block, width), lambda i: (0, tail, 0))]
-        + whole(len(token_operands) - 1),
+        in_specs=[pl.BlockSpec(memory_space=pl.ANY)] * 2
+        + [pl.BlockSpec((prompts, block, width), lambda i: (0, tail, 0))]
+        + whole(len(token_operands) - 3),
         out_specs=whole(4),
         out_shape=[
             out((CONV - 1, padded, 2 * LANES), BF16),
@@ -438,33 +419,40 @@
         scratch_shapes=[
             pltpu.VMEM((padded, width), F32),
             pltpu.VMEM((CONV - 1, padded, 3 * LANES), F32),
+            pltpu.VMEM((width, STATE), BF16),
+            pltpu.VMEM((width, STATE), BF16),
+            pltpu.SemaphoreType.DMA((2,)),
         ],
         name="token",
     )(*token_operands)
     halo = lax.ppermute(trail, "sp", [(i, i + 1) for i in range(dests - 1)])
     per = 2
-    state, lead, lead_weight, logs, taps = call(
+    state, lead, weight, logs, taps = call(
         lambda *refs: local_body(*refs, per=per),
         [
             out((prompts, P_SIZE, STATE), F32),
             out((CONV - 1, padded, 2 * LANES), F32),
-            out((CONV - 1, padded, LANES), F32),
+            out((padded, length), F32),
             out((padded, LANES), F32),
             out((8, 2 * LANES), F32),
         ],
         prompt_layer_input,
+        key_projection,
         value_rows,
-        key_projection,
         step_rows,
         value_filter_taps,
         key_filter_taps,
         bias,
         decay_rate,
         offset_rows,
-        specs=[pl.BlockSpec(memory_space=pl.ANY)] + whole(8),
+        specs=[pl.BlockSpec(memory_space=pl.ANY)] * 2 + whole(7),
         scratch=[
             pltpu.VMEM((prompts, length, width), BF16),
             pltpu.VMEM((width, 2 * LANES), BF16),
+            pltpu.VMEM((prompts, P_SIZE, length), F32),
+            pltpu.VMEM((prompts, length, STATE), BF16),
+            pltpu.VMEM((2, padded, length), F32),
+            pltpu.SemaphoreType.DMA,
             pltpu.SemaphoreType.DMA((prompts // per,)),
         ],
     )
@@ -473,60 +461,59 @@
         [out((prompts * P_SIZE + 3 * padded, STATE), BF16)],
         halo,
         lead,
-        lead_weight,
+        weight,
         logs,
         taps,
         state,
         newest,
     )
-    half = dests // 2
-    parts = {0: payload}
+    parts = [payload]
     for k in range(dests - 1, 0, -1):
-        pairs = [(k, 0), ((half + k) % dests, half)]
-        parts[k] = lax.ppermute(payload, "sp", pairs)
-    states = out((prompts, P_SIZE, STATE), F32)
-    one, two, early_logs, early_newest = call(
-        lambda *refs: early_body(*refs, prompts=prompts, padded=padded, half=half),
-        [states, states, out((2, padded, LANES), F32), out((2 * padded, LANES), BF16)],
-        *[parts[k] for k in range(dests - 2)],
+        parts.insert(1, lax.ppermute(payload, "sp", [(k, 0)]))
+    (early,) = call(
+        lambda *refs: early_body(*refs, prompts=prompts, padded=padded),
+        [out((prompts, P_SIZE, STATE), F32)],
+        *parts[: dests - 2],
     )
     entry = prompts * keep + 16
-    own, to_next, to_pair, to_rest = call(
-        lambda *refs: hub_body(*refs, half=half, keep=keep),
-        [out((n, entry, STATE), BF16) for n in (1, 1, 2, 4)],
-        one,
-        two,
-        early_logs,
-        early_newest,
+    own, to1, to2, to4, to8 = call(
+        lambda *refs: hub_body(*refs, keep=keep),
+        [out((n, entry, STATE), BF16) for n in (1, 1, 2, 4, 8)],
+        early,
         parts[dests - 2],
         parts[dests - 1],
         new_decay,
         new_gate,
     )
 
-    def hop(value, *moves):
-        pairs = [(h + i, h + j) for h in (0, half) for i, j in moves]
+    def hop(value, *pairs):
         return lax.ppermute(value, "sp", pairs)
 
-    to_next = hop(to_next, (0, 1))
-    to_pair = hop(to_pair, (0, 2))
-    to_rest = hop(to_rest, (0, 4))
-    to_sixth = hop(to_rest, (4, 6))
-    to_odd = hop(to_pair[1:] + to_rest[1:2] + to_sixth[3:], (2, 3), (4, 5), (6, 7))
+    to1 = hop(to1, (0, 1))
+    to2 = hop(to2, (0, 2))
+    to4 = hop(to4, (0, 4))
+    to8 = hop(to8, (0, 8))
+    to12 = hop(to8, (8, 12))
+    to6 = hop(to4[2:] + to8[2:4] + to12[6:], (4, 6), (8, 10), (12, 14))
+    odd = to2[1:] + to4[1:2] + to8[1:2] + to12[5:6] + to6[1:]
+    odd = hop(odd, *[(i, i + 1) for i in range(2, dests, 2)])
+    places = (0, 0, 0, 0, 4, 0, 0)
     tp_size = lax.axis_size(TP)
     cache, gated, squares = call(
-        lambda *refs: pick_body(*refs, half=half, keep=keep),
+        lambda *refs: pick_body(*refs, places=places, keep=keep),
         [
             out((prompts * keep, STATE), BF16),
             out((8, LANES), F32),
             out((tp_size, 1, LANES), F32),
         ],
         own,
-        to_next,
-        to_pair,
-        to_rest,
-        to_sixth,
-        to_odd,
+        to1,
+        to2,
+        to4,
+        to8,
+        to12,
+        to6,
+        odd,
     )
     squares = lax.all_to_all(squares, TP, 0, 0, tiled=True)
     (first_read,) = call(

time: 191 us -> 191 us (level)
  waiting for transfers between devices: 81.3 us -> 85.4 us
  blocking collectives: 42.6 us -> 40.4 us
    ppermute x15, waiting for transfers between devices: 79.4 us -> 82.5 us  [shards(): parts.insert(1, lax.ppermute(payload, 'sp', [(k, 0)]))]
    ppermute x15, starting transfers between devices: 22.7 us -> 19.5 us  [shards(): parts.insert(1, lax.ppermute(payload, 'sp', [(k, 0)]))]
    all_to_all x1, blocking collectives: 42.6 us -> 40.4 us  [shards(): squares = lax.all_to_all(squares, TP, 0, 0, tiled=True)]
    ppermute x5 -> x7, starting transfers between devices: 5.22 us -> 7.2 us  [hop(): return lax.ppermute(value, 'sp', pairs)]
  transfers between devices with their start and end apart: 21 -> 23, of which waited for: 12 -> 15; matrix products, arithmetic and copies ran while one was open for 0% -> 0% of each run, Pallas kernels for 7% -> 7%
where the time goes in v4:
time: 191 us; the launch traced here: 190 us
  waiting for transfers between devices  85.4 us (45%)
  blocking collectives  40.4 us (21%)
  starting transfers between devices  35.9 us (19%)
  Pallas kernels  24.3 us (13%)
  local copies, waits for them, and re-layouts  2.6 us (1%)
    ppermute x15, waiting for transfers between devices, shards(): parts.insert(1, lax.ppermute(payload, 'sp', [(k, 0)]))  82.5 us
    all_to_all x1, blocking collectives, shards(): squares = lax.all_to_all(squares, TP, 0, 0, tiled=True)  40.4 us
    pallas_call x6, Pallas kernels, call(): pl.pallas_call(body, in_specs=specs or whole(len(operands)), out_specs=wh...  20.2 us
    ppermute x15, starting transfers between devices, shards(): parts.insert(1, lax.ppermute(payload, 'sp', [(k, 0)]))  19.5 us
    ppermute x1, starting transfers between devices, shards(): halo = lax.ppermute(trail, 'sp', [(i, i + 1) for i in range(dests - 1)])  9.19 us
    ppermute x7, starting transfers between devices, hop(): return lax.ppermute(value, 'sp', pairs)  7.2 us
    pallas_call x1, Pallas kernels, shards(): pl.pallas_call(token_body, grid=(1,), in_specs=[pl.BlockSpec(memory_space...  4.11 us
  transfers between devices with their start and end apart: 23, of which 15 were waited for; matrix products, arithmetic and copies ran while one was open for 0% of the time, Pallas kernels for 7%

profile of v4, /device:TPU:5, one launch (start us, length us, event | category | flops | bytes accessed | tf_op | source)
XLA Modules:
  0.0 189.7 jit_solution(12840866296793668703)
XLA Ops:
  0.6 4.1 %token_.1 = (bf16[3,16,256]{2,1,0:T(8,128)(2,1)}, bf16[32,128]{1,0:T(8,128)(2,1)}, f32[16,128]{1,0:T(8,128)}, f32[16,64]{1,0:T(8,128)}) custom-call(bf16[2048,256]{1,0:T(8,128)(2,1)} %refs_1_.1, bf16[2048,256]{1,0:T(8,128)(2,1)} %query_hbm.1, bf16[12,128,2048]{2,1,0:T(8,128)(2,1)} %refs_0_.1, bf16[12,2048]{1,0:T(8,128)(2,1)} %next_ref.1, ...), custom_call_target="tpu_custom_call" | custom-call | tf_op jit(solution)/shard_map/token/pallas_call | solution.py:406
  4.7 9.2 %collective-permute-start = (bf16[3,16,256]{2,1,0:T(8,128)(2,1)}, bf16[3,16,256]{2,1,0:T(8,128)(2,1)S(1)}, u32[]{:S(2)}, u32[]{:S(2)}) collective-permute-start(bf16[3,16,256]{2,1,0:T(8,128)(2,1)} %get-tuple-element.19), channel_id=1, source_target_pairs={{0,32},{32,64},{64,96},{96,128},{128,160},{160,192},{192,224},{224... | collective-permute-start | bytes 73736 | tf_op jit(solution)/shard_map/ppermute | solution.py:428
  13.9 9.1 %shard_map.158 = (f32[12,64,128]{2,1,0:T(8,128)}, f32[3,16,256]{2,1,0:T(8,128)}, f32[16,128]{1,0:T(8,128)}, f32[16,128]{1,0:T(8,128)}, f32[8,256]{1,0:T(8,128)}) custom-call(bf16[12,128,2048]{2,1,0:T(8,128)(2,1)} %refs_0_.1, bf16[2048,256]{1,0:T(8,128)(2,1)} %refs_1_.1, bf16[64,2048]{1,0:T(8,128)(2,1)} %bitcast.12, bf16[32,2048]{1,0:T(8,128)(2,1)} %bitcast.14, ...), custom_call_target="tpu_custom_call" | custom-call | tf_op jit(solution)/shard_map/pallas_call | solution.py:350
  23.1 0.6 copy-done.20
  23.7 2.1 %shard_map.159.refs_0_ = bf16[816,128]{1,0:T(8,128)(2,1)} custom-call(bf16[3,16,256]{2,1,0:T(8,128)(2,1)} %copy-done.20, f32[3,16,256]{2,1,0:T(8,128)} %get-tuple-element.20.lead_ref, f32[16,128]{1,0:T(8,128)} %get-tuple-element.21.weight_ref, f32[16,128]{1,0:T(8,128)} %get-tuple-element.22.logs_ref, f32[8,256]{1,0:T(8,128)} %get-tuple-element.23.taps_ref, ...), custom_call_target="tpu_custom_call" | custom-call | tf_op jit(solution)/shard_map/pallas_call | solution.py:350
  25.8 1.3 collective-permute-start.1
  27.1 1.3 collective-permute-start.10
  28.5 1.3 collective-permute-start.11
  29.8 1.3 collective-permute-start.12
  31.1 1.3 collective-permute-start.13
  32.4 4.6 %collective-permute-done.1.refs_1_ = bf16[816,128]{1,0:T(8,128)(2,1)S(1)} collective-permute-done((bf16[816,128]{1,0:T(8,128)(2,1)}, bf16[816,128]{1,0:T(8,128)(2,1)S(1)}, u32[]{:S(2)}, u32[]{:S(2)}) %collective-permute-start.1) | collective-permute-done | bytes 208928 | tf_op jit(solution)/shard_map/ppermute | solution.py:472
  37.0 1.3 collective-permute-start.2
  38.3 52.7 %collective-permute-done.10.refs_10_ = bf16[816,128]{1,0:T(8,128)(2,1)S(1)} collective-permute-done((bf16[816,128]{1,0:T(8,128)(2,1)}, bf16[816,128]{1,0:T(8,128)(2,1)S(1)}, u32[]{:S(2)}, u32[]{:S(2)}) %collective-permute-start.10) | collective-permute-done | bytes 208928 | tf_op jit(solution)/shard_map/ppermute | solution.py:472
  91.0 1.3 collective-permute-start.3
  92.3 3.7 %collective-permute-done.11.refs_11_ = bf16[816,128]{1,0:T(8,128)(2,1)S(1)} collective-permute-done((bf16[816,128]{1,0:T(8,128)(2,1)}, bf16[816,128]{1,0:T(8,128)(2,1)S(1)}, u32[]{:S(2)}, u32[]{:S(2)}) %collective-permute-start.11) | collective-permute-done | bytes 208928 | tf_op jit(solution)/shard_map/ppermute | solution.py:472
  96.0 1.3 collective-permute-start.4
  97.3 2.5 %collective-permute-done.12.refs_12_ = bf16[816,128]{1,0:T(8,128)(2,1)S(1)} collective-permute-done((bf16[816,128]{1,0:T(8,128)(2,1)}, bf16[816,128]{1,0:T(8,128)(2,1)S(1)}, u32[]{:S(2)}, u32[]{:S(2)}) %collective-permute-start.12) | collective-permute-done | bytes 208928 | tf_op jit(solution)/shard_map/ppermute | solution.py:472
  99.8 1.3 collective-permute-start.5
  101.1 3.7 %collective-permute-done.13.refs_13_ = bf16[816,128]{1,0:T(8,128)(2,1)S(1)} collective-permute-done((bf16[816,128]{1,0:T(8,128)(2,1)}, bf16[816,128]{1,0:T(8,128)(2,1)S(1)}, u32[]{:S(2)}, u32[]{:S(2)}) %collective-permute-start.13) | collective-permute-done | bytes 208928 | tf_op jit(solution)/shard_map/ppermute | solution.py:472
  104.9 1.3 collective-permute-start.6
  106.2 1.3 collective-permute-start.7
  107.5 1.3 collective-permute-start.8
  108.9 1.3 collective-permute-start.9
  110.2 1.2 collective-permute-done.5.refs_5_
  111.4 1.3 collective-permute-start.14
  112.7 4.9 %collective-permute-done.6.refs_6_ = bf16[816,128]{1,0:T(8,128)(2,1)S(1)} collective-permute-done((bf16[816,128]{1,0:T(8,128)(2,1)}, bf16[816,128]{1,0:T(8,128)(2,1)S(1)}, u32[]{:S(2)}, u32[]{:S(2)}) %collective-permute-start.6) | collective-permute-done | bytes 208928 | tf_op jit(solution)/shard_map/ppermute | solution.py:472
  117.6 1.3 collective-permute-start.15
  118.9 0.7 collective-permute-done.7.refs_7_
  119.7 3.7 %collective-permute-done.8.refs_8_ = bf16[816,128]{1,0:T(8,128)(2,1)S(1)} collective-permute-done((bf16[816,128]{1,0:T(8,128)(2,1)}, bf16[816,128]{1,0:T(8,128)(2,1)S(1)}, u32[]{:S(2)}, u32[]{:S(2)}) %collective-permute-start.8) | collective-permute-done | bytes 208928 | tf_op jit(solution)/shard_map/ppermute | solution.py:472
  123.3 2.2 %collective-permute-done.9.refs_9_ = bf16[816,128]{1,0:T(8,128)(2,1)S(1)} collective-permute-done((bf16[816,128]{1,0:T(8,128)(2,1)}, bf16[816,128]{1,0:T(8,128)(2,1)S(1)}, u32[]{:S(2)}, u32[]{:S(2)}) %collective-permute-start.9) | collective-permute-done | bytes 208928 | tf_op jit(solution)/shard_map/ppermute | solution.py:472
  125.7 0.7 copy-done.14
  126.4 3.3 %shard_map.160.refs_0_ = f32[12,64,128]{2,1,0:T(8,128)} custom-call(bf16[816,128]{1,0:T(8,128)(2,1)} %shard_map.159.refs_0_, bf16[816,128]{1,0:T(8,128)(2,1)} %copy-done.2, bf16[816,128]{1,0:T(8,128)(2,1)} %copy-done.7, bf16[816,128]{1,0:T(8,128)(2,1)} %copy-done.8, bf16[816,128]{1,0:T(8,128)(2,1)} %copy-done.9, bf16[816,128]{1,0:T(8,128)(2,1)} %copy-done.10, ...), custom_call_target="tpu_custom_call" | custom-call | tf_op jit(solution)/shard_map/pallas_call | solution.py:350
  129.7 0.6 collective-permute-done.14.refs_1_
  130.3 1.9 %collective-permute-done.15.refs_2_ = bf16[816,128]{1,0:T(8,128)(2,1)S(1)} collective-permute-done((bf16[816,128]{1,0:T(8,128)(2,1)}, bf16[816,128]{1,0:T(8,128)(2,1)S(1)}, u32[]{:S(2)}, u32[]{:S(2)}) %collective-permute-start.15) | collective-permute-done | bytes 208928 | tf_op jit(solution)/shard_map/ppermute | solution.py:472
  132.2 0.7 copy-done.16
  132.9 2.4 %shard_map.161 = (bf16[1,64,128]{2,1,0:T(8,128)(2,1)}, bf16[1,64,128]{2,1,0:T(8,128)(2,1)}, bf16[2,64,128]{2,1,0:T(8,128)(2,1)}, bf16[4,64,128]{2,1,0:T(8,128)(2,1)}, bf16[8,64,128]{2,1,0:T(8,128)(2,1)}) custom-call(f32[12,64,128]{2,1,0:T(8,128)} %shard_map.160.refs_0_, bf16[816,128]{1,0:T(8,128)(2,1)} %copy-done.15, bf16[816,128]{1,0:T(8,128)(2,1)} %copy-done.16, ...), custom_call_target="tpu_custom_call" | custom-call | tf_op jit(solution)/shard_map/pallas_call | solution.py:350
  135.3 1.3 collective-permute-start.19
  136.6 2.2 %collective-permute-done.19.refs_4_ = bf16[8,64,128]{2,1,0:T(8,128)(2,1)S(1)} collective-permute-done((bf16[8,64,128]{2,1,0:T(8,128)(2,1)}, bf16[8,64,128]{2,1,0:T(8,128)(2,1)S(1)}, u32[]{:S(2)}, u32[]{:S(2)}) %collective-permute-start.19) | collective-permute-done | bytes 131104 | tf_op jit(solution)/shard_map/ppermute | solution.py:490
  138.8 0.7 collective-permute-start.20
  139.5 1.3 collective-permute-start.18
  140.8 1.3 collective-permute-start.17
  142.5 0.7 collective-permute-start.21
  143.1 1.3 collective-permute-start.16
  144.5 0.7 collective-permute-start.22
  145.6 0.6 copy-done.21
  146.1 1.8 shard_map.162
  147.9 40.4 %all_to_all.5.parts_ref = f32[32,1,128]{2,1,0:T(1,128)} all-to-all(f32[32,1,128]{2,1,0:T(1,128)} %get-tuple-element.34), channel_id=1, replica_groups=mesh['grp'=2,'sp'=16,'tp_0'=16,'tp_1'=2] {'tp_0','tp_1'}, dimensions={0} | all-to-all | bytes 32768 | tf_op jit(solution)/shard_map/all_to_all | solution.py:518
  188.3 1.4 shard_map.163
  (54 shorter events, 0.8 us)
Async XLA Ops:
  4.7 18.4 %collective-permute-start = (bf16[3,16,256]{2,1,0:T(8,128)(2,1)}, bf16[3,16,256]{2,1,0:T(8,128)(2,1)S(1)}, u32[]{:S(2)}, u32[]{:S(2)}) collective-permute-start(bf16[3,16,256]{2,1,0:T(8,128)(2,1)} %get-tuple-element.19), channel_id=1, source_target_pairs={{0,32},{32,64},{64,96},{96,128},{128,160},{160,192},{192,224},{224... | collective-permute-start | bytes 73736 | tf_op jit(solution)/shard_map/ppermute | solution.py:428
  23.1 0.6 copy-start.20
  25.8 11.1 %collective-permute-start.1 = (bf16[816,128]{1,0:T(8,128)(2,1)}, bf16[816,128]{1,0:T(8,128)(2,1)S(1)}, u32[]{:S(2)}, u32[]{:S(2)}) collective-permute-start(bf16[816,128]{1,0:T(8,128)(2,1)} %shard_map.159.refs_0_), channel_id=1, source_target_pairs={{32,0},{33,1},{34,2},{35,3},{36,4},{37,5},{38,6},{39,7},{40,8},{41... | collective-permute-start | bytes 626696 | tf_op jit(solution)/shard_map/ppermute | solution.py:472
  27.1 63.8 %collective-permute-start.10 = (bf16[816,128]{1,0:T(8,128)(2,1)}, bf16[816,128]{1,0:T(8,128)(2,1)S(1)}, u32[]{:S(2)}, u32[]{:S(2)}) collective-permute-start(bf16[816,128]{1,0:T(8,128)(2,1)} %shard_map.159.refs_0_), channel_id=1, source_target_pairs={{320,0},{321,1},{322,2},{323,3},{324,4},{325,5},{326,6},{327,7},{3... | collective-permute-start | bytes 626696 | tf_op jit(solution)/shard_map/ppermute | solution.py:472
  28.5 67.5 %collective-permute-start.11 = (bf16[816,128]{1,0:T(8,128)(2,1)}, bf16[816,128]{1,0:T(8,128)(2,1)S(1)}, u32[]{:S(2)}, u32[]{:S(2)}) collective-permute-start(bf16[816,128]{1,0:T(8,128)(2,1)} %shard_map.159.refs_0_), channel_id=1, source_target_pairs={{352,0},{353,1},{354,2},{355,3},{356,4},{357,5},{358,6},{359,7},{3... | collective-permute-start | bytes 626696 | tf_op jit(solution)/shard_map/ppermute | solution.py:472
  29.8 70.0 %collective-permute-start.12 = (bf16[816,128]{1,0:T(8,128)(2,1)}, bf16[816,128]{1,0:T(8,128)(2,1)S(1)}, u32[]{:S(2)}, u32[]{:S(2)}) collective-permute-start(bf16[816,128]{1,0:T(8,128)(2,1)} %shard_map.159.refs_0_), channel_id=1, source_target_pairs={{384,0},{385,1},{386,2},{387,3},{388,4},{389,5},{390,6},{391,7},{3... | collective-permute-start | bytes 626696 | tf_op jit(solution)/shard_map/ppermute | solution.py:472
  31.1 73.8 %collective-permute-start.13 = (bf16[816,128]{1,0:T(8,128)(2,1)}, bf16[816,128]{1,0:T(8,128)(2,1)S(1)}, u32[]{:S(2)}, u32[]{:S(2)}) collective-permute-start(bf16[816,128]{1,0:T(8,128)(2,1)} %shard_map.159.refs_0_), channel_id=1, source_target_pairs={{416,0},{417,1},{418,2},{419,3},{420,4},{421,5},{422,6},{423,7},{4... | collective-permute-start | bytes 626696 | tf_op jit(solution)/shard_map/ppermute | solution.py:472
  37.0 88.6 %copy-start.2 = (bf16[816,128]{1,0:T(8,128)(2,1)}, bf16[816,128]{1,0:T(8,128)(2,1)S(1)}, u32[]{:S(2)}) copy-start(bf16[816,128]{1,0:T(8,128)(2,1)S(1)} %collective-permute-done.1.refs_1_) | copy-start | bytes 626692
  37.0 69.2 %collective-permute-start.2 = (bf16[816,128]{1,0:T(8,128)(2,1)}, bf16[816,128]{1,0:T(8,128)(2,1)S(1)}, u32[]{:S(2)}, u32[]{:S(2)}) collective-permute-start(bf16[816,128]{1,0:T(8,128)(2,1)} %shard_map.159.refs_0_), channel_id=1, source_target_pairs={{64,0},{65,1},{66,2},{67,3},{68,4},{69,5},{70,6},{71,7},{72,8},{73... | collective-permute-start | bytes 626696 | tf_op jit(solution)/shard_map/ppermute | solution.py:472
  91.0 34.6 %copy-start.3 = (bf16[816,128]{1,0:T(8,128)(2,1)}, bf16[816,128]{1,0:T(8,128)(2,1)S(1)}, u32[]{:S(2)}) copy-start(bf16[816,128]{1,0:T(8,128)(2,1)S(1)} %collective-permute-done.10.refs_10_) | copy-start | bytes 626692
  91.0 16.5 %collective-permute-start.3 = (bf16[816,128]{1,0:T(8,128)(2,1)}, bf16[816,128]{1,0:T(8,128)(2,1)S(1)}, u32[]{:S(2)}, u32[]{:S(2)}) collective-permute-start(bf16[816,128]{1,0:T(8,128)(2,1)} %shard_map.159.refs_0_), channel_id=1, source_target_pairs={{96,0},{97,1},{98,2},{99,3},{100,4},{101,5},{102,6},{103,7},{104,8... | collective-permute-start | bytes 626696 | tf_op jit(solution)/shard_map/ppermute | solution.py:472
  96.0 29.6 %copy-start.4 = (bf16[816,128]{1,0:T(8,128)(2,1)}, bf16[816,128]{1,0:T(8,128)(2,1)S(1)}, u32[]{:S(2)}) copy-start(bf16[816,128]{1,0:T(8,128)(2,1)S(1)} %collective-permute-done.11.refs_11_) | copy-start | bytes 626692
  96.0 12.8 %collective-permute-start.4 = (bf16[816,128]{1,0:T(8,128)(2,1)}, bf16[816,128]{1,0:T(8,128)(2,1)S(1)}, u32[]{:S(2)}, u32[]{:S(2)}) collective-permute-start(bf16[816,128]{1,0:T(8,128)(2,1)} %shard_map.159.refs_0_), channel_id=1, source_target_pairs={{128,0},{129,1},{130,2},{131,3},{132,4},{133,5},{134,6},{135,7},{1... | collective-permute-start | bytes 626696 | tf_op jit(solution)/shard_map/ppermute | solution.py:472
  99.8 25.8 %copy-start.5 = (bf16[816,128]{1,0:T(8,128)(2,1)}, bf16[816,128]{1,0:T(8,128)(2,1)S(1)}, u32[]{:S(2)}) copy-start(bf16[816,128]{1,0:T(8,128)(2,1)S(1)} %collective-permute-done.12.refs_12_) | copy-start | bytes 626692
  99.8 11.6 %collective-permute-start.5 = (bf16[816,128]{1,0:T(8,128)(2,1)}, bf16[816,128]{1,0:T(8,128)(2,1)S(1)}, u32[]{:S(2)}, u32[]{:S(2)}) collective-permute-start(bf16[816,128]{1,0:T(8,128)(2,1)} %shard_map.159.refs_0_), channel_id=1, source_target_pairs={{160,0},{161,1},{162,2},{163,3},{164,4},{165,5},{166,6},{167,7},{1... | collective-permute-start | bytes 626696 | tf_op jit(solution)/shard_map/ppermute | solution.py:472
  104.9 20.7 %copy-start.6 = (bf16[816,128]{1,0:T(8,128)(2,1)}, bf16[816,128]{1,0:T(8,128)(2,1)S(1)}, u32[]{:S(2)}) copy-start(bf16[816,128]{1,0:T(8,128)(2,1)S(1)} %collective-permute-done.13.refs_13_) | copy-start | bytes 626692
  104.9 12.8 %collective-permute-start.6 = (bf16[816,128]{1,0:T(8,128)(2,1)}, bf16[816,128]{1,0:T(8,128)(2,1)S(1)}, u32[]{:S(2)}, u32[]{:S(2)}) collective-permute-start(bf16[816,128]{1,0:T(8,128)(2,1)} %shard_map.159.refs_0_), channel_id=1, source_target_pairs={{192,0},{193,1},{194,2},{195,3},{196,4},{197,5},{198,6},{199,7},{2... | collective-permute-start | bytes 626696 | tf_op jit(solution)/shard_map/ppermute | solution.py:472
  106.2 19.4 %copy-start.7 = (bf16[816,128]{1,0:T(8,128)(2,1)}, bf16[816,128]{1,0:T(8,128)(2,1)S(1)}, u32[]{:S(2)}) copy-start(bf16[816,128]{1,0:T(8,128)(2,1)S(1)} %collective-permute-done.2.refs_2_) | copy-start | bytes 626692
  106.2 13.5 %collective-permute-start.7 = (bf16[816,128]{1,0:T(8,128)(2,1)}, bf16[816,128]{1,0:T(8,128)(2,1)S(1)}, u32[]{:S(2)}, u32[]{:S(2)}) collective-permute-start(bf16[816,128]{1,0:T(8,128)(2,1)} %shard_map.159.refs_0_), channel_id=1, source_target_pairs={{224,0},{225,1},{226,2},{227,3},{228,4},{229,5},{230,6},{231,7},{2... | collective-permute-start | bytes 626696 | tf_op jit(solution)/shard_map/ppermute | solution.py:472
  107.5 18.1 %copy-start.8 = (bf16[816,128]{1,0:T(8,128)(2,1)}, bf16[816,128]{1,0:T(8,128)(2,1)S(1)}, u32[]{:S(2)}) copy-start(bf16[816,128]{1,0:T(8,128)(2,1)S(1)} %collective-permute-done.3.refs_3_) | copy-start | bytes 626692
  107.5 15.8 %collective-permute-start.8 = (bf16[816,128]{1,0:T(8,128)(2,1)}, bf16[816,128]{1,0:T(8,128)(2,1)S(1)}, u32[]{:S(2)}, u32[]{:S(2)}) collective-permute-start(bf16[816,128]{1,0:T(8,128)(2,1)} %shard_map.159.refs_0_), channel_id=1, source_target_pairs={{256,0},{257,1},{258,2},{259,3},{260,4},{261,5},{262,6},{263,7},{2... | collective-permute-start | bytes 626696 | tf_op jit(solution)/shard_map/ppermute | solution.py:472
  108.9 16.8 %copy-start.9 = (bf16[816,128]{1,0:T(8,128)(2,1)}, bf16[816,128]{1,0:T(8,128)(2,1)S(1)}, u32[]{:S(2)}) copy-start(bf16[816,128]{1,0:T(8,128)(2,1)S(1)} %collective-permute-done.4.refs_4_) | copy-start | bytes 626692
  108.9 16.7 %collective-permute-start.9 = (bf16[816,128]{1,0:T(8,128)(2,1)}, bf16[816,128]{1,0:T(8,128)(2,1)S(1)}, u32[]{:S(2)}, u32[]{:S(2)}) collective-permute-start(bf16[816,128]{1,0:T(8,128)(2,1)} %shard_map.159.refs_0_), channel_id=1, source_target_pairs={{288,0},{289,1},{290,2},{291,3},{292,4},{293,5},{294,6},{295,7},{2... | collective-permute-start | bytes 626696 | tf_op jit(solution)/shard_map/ppermute | solution.py:472
  111.4 14.2 %copy-start.10 = (bf16[816,128]{1,0:T(8,128)(2,1)}, bf16[816,128]{1,0:T(8,128)(2,1)S(1)}, u32[]{:S(2)}) copy-start(bf16[816,128]{1,0:T(8,128)(2,1)S(1)} %collective-permute-done.5.refs_5_) | copy-start | bytes 626692
  111.4 18.9 %collective-permute-start.14 = (bf16[816,128]{1,0:T(8,128)(2,1)}, bf16[816,128]{1,0:T(8,128)(2,1)S(1)}, u32[]{:S(2)}, u32[]{:S(2)}) collective-permute-start(bf16[816,128]{1,0:T(8,128)(2,1)} %shard_map.159.refs_0_), channel_id=1, source_target_pairs={{448,0},{449,1},{450,2},{451,3},{452,4},{453,5},{454,6},{455,7},{4... | collective-permute-start | bytes 626696 | tf_op jit(solution)/shard_map/ppermute | solution.py:472
  117.6 8.0 %copy-start.11 = (bf16[816,128]{1,0:T(8,128)(2,1)}, bf16[816,128]{1,0:T(8,128)(2,1)S(1)}, u32[]{:S(2)}) copy-start(bf16[816,128]{1,0:T(8,128)(2,1)S(1)} %collective-permute-done.6.refs_6_) | copy-start | bytes 626692
  117.6 14.5 %collective-permute-start.15 = (bf16[816,128]{1,0:T(8,128)(2,1)}, bf16[816,128]{1,0:T(8,128)(2,1)S(1)}, u32[]{:S(2)}, u32[]{:S(2)}) collective-permute-start(bf16[816,128]{1,0:T(8,128)(2,1)} %shard_map.159.refs_0_), channel_id=1, source_target_pairs={{480,0},{481,1},{482,2},{483,3},{484,4},{485,5},{486,6},{487,7},{4... | collective-permute-start | bytes 626696 | tf_op jit(solution)/shard_map/ppermute | solution.py:472
  119.7 6.0 %copy-start.12 = (bf16[816,128]{1,0:T(8,128)(2,1)}, bf16[816,128]{1,0:T(8,128)(2,1)S(1)}, u32[]{:S(2)}) copy-start(bf16[816,128]{1,0:T(8,128)(2,1)S(1)} %collective-permute-done.7.refs_7_) | copy-start | bytes 626692
  123.3 2.3 %copy-start.13 = (bf16[816,128]{1,0:T(8,128)(2,1)}, bf16[816,128]{1,0:T(8,128)(2,1)S(1)}, u32[]{:S(2)}) copy-start(bf16[816,128]{1,0:T(8,128)(2,1)S(1)} %collective-permute-done.8.refs_8_) | copy-start | bytes 626692
  125.7 0.7 copy-start.14
  130.3 1.9 %copy-start.15 = (bf16[816,128]{1,0:T(8,128)(2,1)}, bf16[816,128]{1,0:T(8,128)(2,1)S(1)}, u32[]{:S(2)}) copy-start(bf16[816,128]{1,0:T(8,128)(2,1)S(1)} %collective-permute-done.14.refs_1_) | copy-start | bytes 626692
  132.2 0.7 copy-start.16
  135.3 3.5 %collective-permute-start.19 = (bf16[8,64,128]{2,1,0:T(8,128)(2,1)}, bf16[8,64,128]{2,1,0:T(8,128)(2,1)S(1)}, u32[]{:S(2)}, u32[]{:S(2)}) collective-permute-start(bf16[8,64,128]{2,1,0:T(8,128)(2,1)} %get-tuple-element.32), channel_id=1, source_target_pairs={{0,256},{1,257},{2,258},{3,259},{4,260},{5,261},{6,262},{7,263},{8... | collective-permute-start | bytes 393224 | tf_op jit(solution)/shard_map/ppermute | solution.py:490
  138.8 6.7 %copy-start = (bf16[8,64,128]{2,1,0:T(8,128)(2,1)}, bf16[8,64,128]{2,1,0:T(8,128)(2,1)S(1)}, u32[]{:S(2)}) copy-start(bf16[8,64,128]{2,1,0:T(8,128)(2,1)S(1)} %collective-permute-done.19.refs_4_) | copy-start | bytes 393220
  138.8 3.6 %collective-permute-start.20 = (bf16[8,64,128]{2,1,0:T(8,128)(2,1)S(1)}, bf16[8,64,128]{2,1,0:T(8,128)(2,1)S(1)}, u32[]{:S(2)}, u32[]{:S(2)}) collective-permute-start(bf16[8,64,128]{2,1,0:T(8,128)(2,1)S(1)} %collective-permute-done.19.refs_4_), channel_id=1, source_target_pairs={{256,384},{257,385},{258,386},{259,387},{260,388},{261,389},{262,3... | collective-permute-start | bytes 393224 | tf_op jit(solution)/shard_map/ppermute | solution.py:490
  139.5 2.9 %collective-permute-start.18 = (bf16[4,64,128]{2,1,0:T(8,128)(2,1)}, bf16[4,64,128]{2,1,0:T(8,128)(2,1)S(1)}, u32[]{:S(2)}, u32[]{:S(2)}) collective-permute-start(bf16[4,64,128]{2,1,0:T(8,128)(2,1)} %get-tuple-element.31), channel_id=1, source_target_pairs={{0,128},{1,129},{2,130},{3,131},{4,132},{5,133},{6,134},{7,135},{8... | collective-permute-start | bytes 196616 | tf_op jit(solution)/shard_map/ppermute | solution.py:490
  140.8 3.6 %collective-permute-start.17 = (bf16[2,64,128]{2,1,0:T(8,128)(2,1)}, bf16[2,64,128]{2,1,0:T(8,128)(2,1)S(1)}, u32[]{:S(2)}, u32[]{:S(2)}) collective-permute-start(bf16[2,64,128]{2,1,0:T(8,128)(2,1)} %get-tuple-element.30), channel_id=1, source_target_pairs={{0,64},{1,65},{2,66},{3,67},{4,68},{5,69},{6,70},{7,71},{8,72},{9,... | collective-permute-start | bytes 98312 | tf_op jit(solution)/shard_map/ppermute | solution.py:490
  142.4 3.1 %copy-start.17 = (bf16[4,64,128]{2,1,0:T(8,128)(2,1)}, bf16[4,64,128]{2,1,0:T(8,128)(2,1)S(1)}, u32[]{:S(2)}) copy-start(bf16[4,64,128]{2,1,0:T(8,128)(2,1)S(1)} %collective-permute-done.18.refs_3_) | copy-start | bytes 196612
  142.4 3.1 %copy-start.1 = (bf16[8,64,128]{2,1,0:T(8,128)(2,1)}, bf16[8,64,128]{2,1,0:T(8,128)(2,1)S(1)}, u32[]{:S(2)}) copy-start(bf16[8,64,128]{2,1,0:T(8,128)(2,1)S(1)} %collective-permute-done.20.refs_5_) | copy-start | bytes 393220
  142.5 2.0 %collective-permute-start.21 = (bf16[2,64,128]{2,1,0:T(8,128)(2,1)S(1)}, bf16[2,64,128]{2,1,0:T(8,128)(2,1)S(1)}, u32[]{:S(2)}, u32[]{:S(2)}) collective-permute-start(bf16[2,64,128]{2,1,0:T(8,128)(2,1)S(1)} %slice_add_fusion), channel_id=1, source_target_pairs={{128,192},{256,320},{384,448},{129,193},{257,321},{385,449},{130,1... | collective-permute-start | bytes 98312 | tf_op jit(solution)/shard_map/ppermute | solution.py:490
  143.1 2.4 %collective-permute-start.16 = (bf16[1,64,128]{2,1,0:T(8,128)(2,1)}, bf16[1,64,128]{2,1,0:T(8,128)(2,1)S(1)}, u32[]{:S(2)}, u32[]{:S(2)}) collective-permute-start(bf16[1,64,128]{2,1,0:T(8,128)(2,1)} %get-tuple-element.29), channel_id=1, source_target_pairs={{0,32},{1,33},{2,34},{3,35},{4,36},{5,37},{6,38},{7,39},{8,40},{9,... | collective-permute-start | bytes 49160 | tf_op jit(solution)/shard_map/ppermute | solution.py:490
  144.5 1.1 copy-start.18
  144.5 1.1 copy-start.19
  144.5 1.0 collective-permute-start.22
  145.5 0.6 copy-start.21
  145.5 0.6 copy-start.22

commit v5 on v2

--- a/solution.py
+++ b/solution.py
@@ -66,68 +66,126 @@
 
 
 def local_body(
-    x_hbm, value_ref, key_ref, step_ref, vt_ref, kt_ref, bias_ref, decay_ref, off_ref,
-    state_ref, lead_ref, lead_weight_ref, logs_ref, taps_ref,
-    x_ref, w_ref, sems, *, per,
+    x_hbm, key_hbm, value_hbm, step_hbm, off_hbm, taps_ref, bias_ref, decay_ref,
+    state_ref, lead_ref, weight_ref, logs_ref,
+    x_ref, w_ref, value_ref, step_ref, off_ref, wide_ref, map_ref, rows_ref, small_sems, sems,
+    *, per,
 ):
     prompts, length, width = x_hbm.shape
+    head = lax.axis_index(TP)
+    group = head // (HEADS // GROUPS)
+    at = pl.multiple_of(group * STATE, STATE)
+    small = (
+        (value_hbm, value_ref),
+        (step_hbm, step_ref),
+        (key_hbm.at[:, pl.ds(at, STATE)], w_ref.at[:, pl.ds(LANES, STATE)]),
+        (off_hbm, off_ref),
+    )
+    small = [pltpu.make_async_copy(*pair, small_sems.at[i]) for i, pair in enumerate(small)]
+    for copy in small:
+        copy.start()
     copies = []
     for i in range(prompts // per):
         part = pl.ds(i * per, per)
         copies.append(pltpu.make_async_copy(x_hbm.at[part], x_ref.at[part], sems.at[i]))
     for copy in copies:
         copy.start()
-    head = lax.axis_index(TP)
-    group = head // (HEADS // GROUPS)
+    small[0].wait()
+    small[1].wait()
     step_row = jnp.broadcast_to(pick_row(step_ref[...], head), (P_SIZE, width)).astype(BF16)
     w_ref[:, :LANES] = jnp.transpose(jnp.concatenate([value_ref[...], step_row], axis=0))
-    logs_ref[...] = jnp.zeros_like(logs_ref)
-    at = pl.multiple_of(group * STATE, STATE)
-    w_ref[:, LANES:] = key_ref[:, pl.ds(at, STATE)]
-    pair = pl.multiple_of((head // 2) * LANES, LANES)
-    value_taps = own_half(vt_ref[:, pl.ds(pair, LANES)].astype(F32), head)
-    taps = jnp.concatenate([value_taps, kt_ref[:, pl.ds(at, STATE)].astype(F32)], axis=1)
-    taps_ref[:CONV] = taps
-    bias = pick(bias_ref[...], head)
-    speed = jnp.exp(pick(decay_ref[...], head))
-    later = (iota((length, length), 1) > iota((length, length), 0)).astype(BF16)
-    position = iota((length, LANES), 0)
+    taps = taps_ref[:CONV]
+    rows_ref[...] = jnp.zeros_like(rows_ref)
+    small[3].wait()
+    offset = off_ref[...]
+    offset = jnp.where(iota(offset.shape, 1) == head, offset, 0.0)
+    rows_ref[1, :prompts] = jnp.sum(offset, axis=1)
+    feature = iota((length, LANES), 1) < P_SIZE
+    small[2].wait()
     for i in range(prompts // per):
         copies[i].wait()
         rows = x_ref[i * per : (i + 1) * per].reshape(per * length, width)
         raw_all = rounded(dot(rows, w_ref[...]))
-        steps, logs, mixes = [], [], []
         for j in range(per):
             b = i * per + j
             raw = raw_all[j * length : (j + 1) * length]
             for k in range(CONV - 1):
                 lead_ref[k, b : b + 1, :] = raw[k : k + 1]
-            step = softplus(pltpu.roll(raw[:, :LANES], 64, axis=1) + bias)
-            offset = jnp.broadcast_to(pick_row(off_ref[b], head), (length, length))
-            log = jnp.transpose(offset) - speed * step
             total = raw * taps[CONV - 1 : CONV]
             for k in range(CONV - 1):
                 total = total + pltpu.roll(raw, CONV - 1 - k, axis=0) * taps[k : k + 1]
-            steps.append(step)
-            logs.append(log)
-            mixes.append(rounded(silu(total)))
-        after = dot01(later, jnp.concatenate(logs, axis=1))
-        for j in range(per):
-            b = i * per + j
-            after_here = after[:, j * LANES : (j + 1) * LANES]
-            weight = jnp.exp(after_here) * steps[j]
-            logs_ref[b : b + 1, :] = after_here[:1] + logs[j][:1]
-            for k in range(CONV - 1):
-                lead_weight_ref[k, b : b + 1, :] = weight[k : k + 1]
-            weighted = jnp.where(position >= CONV - 1, mixes[j][:, :LANES] * weight, 0.0)
-            state = dot(
-                weighted.astype(BF16), mixes[j][:, LANES:].astype(BF16), ((0,), (0,))
-            )
-            state_ref[b] = state[:P_SIZE]
+            mixed = silu(total)
+            map_ref[b] = mixed[:, LANES:].astype(BF16)
+            turned = jnp.where(feature, rounded(mixed[:, :LANES]), raw[:, :LANES])
+            turned = jnp.transpose(turned)
+            wide_ref[b] = turned[:P_SIZE]
+            rows_ref[0, b : b + 1, :] = turned[P_SIZE : P_SIZE + 1]
+    step = softplus(rows_ref[0] + pick(bias_ref[...], head))
+    log = rows_ref[1] - jnp.exp(pick(decay_ref[...], head)) * step
+    later = (iota((length, length), 0) > iota((length, length), 1)).astype(BF16)
+    after = dot(jnp.concatenate(pieces(log), axis=1), jnp.concatenate([later] * 3, axis=0))
+    weight = jnp.exp(after) * step
+    weight_ref[...] = weight
+    logs_ref[...] = jnp.broadcast_to(jnp.sum(log, axis=1, keepdims=True), logs_ref.shape)
+    weight = jnp.where(iota(weight.shape, 1) >= CONV - 1, weight, 0.0)
+    for b in range(prompts):
+        weighted = (wide_ref[b] * weight[b : b + 1]).astype(BF16)
+        state_ref[b] = dot(weighted, map_ref[b])
+
+
+def taps_of(vt_ref, kt_ref):
+    head = lax.axis_index(TP)
+    at = pl.multiple_of((head // (HEADS // GROUPS)) * STATE, STATE)
+    pair = pl.multiple_of((head // 2) * LANES, LANES)
+    value_taps = own_half(vt_ref[:, pl.ds(pair, LANES)].astype(F32), head)
+    return jnp.concatenate([value_taps, kt_ref[:, pl.ds(at, STATE)].astype(F32)], axis=1)
+
+
+def on_last():
+    return lax.axis_index("sp") == lax.axis_size("sp") - 1
+
+
+def early_body(
+    x_hbm, key_hbm, value_hbm, step_hbm, off_hbm, vt_ref, kt_ref, bias_ref, decay_ref,
+    state_ref, lead_ref, weight_ref, logs_ref, taps_ref, *scratch, per,
+):
+    taps_ref[:CONV] = taps_of(vt_ref, kt_ref)
+
+    @pl.when(jnp.logical_not(on_last()))
+    def _():
+        local_body(
+            x_hbm, key_hbm, value_hbm, step_hbm, off_hbm, taps_ref, bias_ref, decay_ref,
+            state_ref, lead_ref, weight_ref, logs_ref, *scratch, per=per,
+        )
+
+
+def late_body(
+    x_hbm, key_hbm, value_hbm, step_hbm, off_hbm, taps_ref, bias_ref, decay_ref, after_ref,
+    state_in, lead_in, weight_in, logs_in,
+    state_ref, lead_ref, weight_ref, logs_ref, *scratch, per,
+):
+    @pl.when(on_last())
+    def _():
+        local_body(
+            x_hbm, key_hbm, value_hbm, step_hbm, off_hbm, taps_ref, bias_ref, decay_ref,
+            state_ref, lead_ref, weight_ref, logs_ref, *scratch, per=per,
+        )
+
+    @pl.when(jnp.logical_not(on_last()))
+    def _():
+        copies = []
+        inputs = (state_in, lead_in, weight_in, logs_in)
+        outputs = (state_ref, lead_ref, weight_ref, logs_ref)
+        for i, (source, target) in enumerate(zip(inputs, outputs)):
+            copies.append(pltpu.make_async_copy(source, target, scratch[-2].at[i]))
+        for copy in copies:
+            copy.start()
+        for copy in copies:
+            copy.wait()
 
 
 def token_body(
-    x_ref, next_ref, value_ref, gate_ref, key_ref, query_ref, step_ref, vt_ref, kt_ref, qt_ref,
+    x_ref, next_ref, value_ref, gate_ref, key_ref, query_ref, step_ref, taps_ref, qt_ref,
     bias_ref, decay_ref, skip_ref,
     trail_ref, newest_ref, decay_out_ref, gate_out_ref,
     pad_ref, last_ref,
@@ -137,11 +195,10 @@
     group = head // (HEADS // GROUPS)
     padded = pad_ref.shape[0]
     at = pl.multiple_of(group * STATE, STATE)
-    pair = pl.multiple_of((head // 2) * LANES, LANES)
     query = query_ref[:, pl.ds(at, STATE)]
     key = key_ref[:, pl.ds(at, STATE)]
-    value_taps = own_half(vt_ref[:, pl.ds(pair, LANES)].astype(F32), head)[:, :P_SIZE]
-    key_taps = kt_ref[:, pl.ds(at, STATE)].astype(F32)
+    value_taps = taps_ref[:CONV, :P_SIZE]
+    key_taps = taps_ref[:CONV, LANES:]
     query_taps = qt_ref[:, pl.ds(at, STATE)].astype(F32)
     pad_ref[...] = jnp.zeros_like(pad_ref)
     pad_ref[:prompts] = next_ref[...].astype(F32)
@@ -187,7 +244,7 @@
 
 
 def pack_body(
-    halo_ref, lead_ref, lead_weight_ref, logs_ref, taps_ref, state_ref, newest_ref, out_ref,
+    halo_ref, lead_ref, weight_ref, logs_ref, taps_ref, state_ref, newest_ref, out_ref,
 ):
     prompts, rows, _ = state_ref.shape
     dests = out_ref.shape[0]
@@ -203,7 +260,8 @@
         for k in range(1, CONV):
             total = total + window[t + k] * taps[k : k + 1]
         mixed = rounded(silu(total))
-        weighted.append(jnp.transpose(rounded(mixed[:, :LANES] * lead_weight_ref[t])))
+        weight = pick(weight_ref[...], t)
+        weighted.append(jnp.transpose(rounded(mixed[:, :LANES] * weight)))
         maps.append(mixed[:, LANES:])
     states = []
     reads = jnp.zeros((rows, LANES), F32)
@@ -334,6 +392,45 @@
     step_rows = step_projection.T
     offset_rows = jnp.swapaxes(position_decay_offset, 1, 2)
 
+    per = 2
+    local_outs = [
+        out((prompts, P_SIZE, STATE), F32),
+        out((CONV - 1, padded, 2 * LANES), F32),
+        out((padded, length), F32),
+        out((padded, LANES), F32),
+    ]
+    local_operands = (
+        prompt_layer_input,
+        key_projection,
+        value_rows,
+        step_rows,
+        offset_rows,
+    )
+    away = [pl.BlockSpec(memory_space=pl.ANY)]
+    local_scratch = [
+        pltpu.VMEM((prompts, length, width), BF16),
+        pltpu.VMEM((width, 2 * LANES), BF16),
+        pltpu.VMEM(value_rows.shape, BF16),
+        pltpu.VMEM(step_rows.shape, BF16),
+        pltpu.VMEM(offset_rows.shape, F32),
+        pltpu.VMEM((prompts, P_SIZE, length), F32),
+        pltpu.VMEM((prompts, length, STATE), BF16),
+        pltpu.VMEM((2, padded, length), F32),
+        pltpu.SemaphoreType.DMA((4,)),
+        pltpu.SemaphoreType.DMA((prompts // per,)),
+    ]
+    *early, taps = call(
+        lambda *refs: early_body(*refs, per=per),
+        [*local_outs, out((8, 2 * LANES), F32)],
+        *local_operands,
+        value_filter_taps,
+        key_filter_taps,
+        bias,
+        decay_rate,
+        specs=away * 5 + whole(4),
+        scratch=local_scratch,
+        name="early",
+    )
     block = 16
     tail = length // block - 1
     token_operands = (
@@ -344,8 +441,7 @@
         key_projection,
         query_projection,
         step_rows,
-        value_filter_taps,
-        key_filter_taps,
+        taps,
         query_filter_taps,
         bias,
         decay_rate,
@@ -371,39 +467,25 @@
     )(*token_operands)
     newest = lax.all_to_all(newest, "sp", 0, 0, tiled=True)
     halo = lax.ppermute(trail, "sp", [(i, i + 1) for i in range(dests - 1)])
-    per = 2
-    state, lead, lead_weight, logs, taps = call(
-        lambda *refs: local_body(*refs, per=per),
-        [
-            out((prompts, P_SIZE, STATE), F32),
-            out((CONV - 1, padded, 2 * LANES), F32),
-            out((CONV - 1, padded, LANES), F32),
-            out((padded, LANES), F32),
-            out((8, 2 * LANES), F32),
-        ],
-        prompt_layer_input,
-        value_rows,
-        key_projection,
-        step_rows,
-        value_filter_taps,
-        key_filter_taps,
+    state, lead, weight, logs = call(
+        lambda *refs: late_body(*refs, per=per),
+        local_outs,
+        *local_operands,
+        taps,
         bias,
         decay_rate,
-        offset_rows,
-        specs=[pl.BlockSpec(memory_space=pl.ANY)] + whole(8),
-        scratch=[
-            pltpu.VMEM((prompts, length, width), BF16),
-            pltpu.VMEM((width, 2 * LANES), BF16),
-            pltpu.SemaphoreType.DMA((prompts // per,)),
-        ],
-        name="local",
+        new_decay,
+        *early,
+        specs=away * 5 + whole(3) + away * 5,
+        scratch=local_scratch,
+        name="late",
     )
     (payload,) = call(
         pack_body,
         [out((dests, prompts * keep + padded, STATE), BF16)],
         halo,
         lead,
-        lead_weight,
+        weight,
         logs,
         taps,
         state,

time: 166 us -> 166 us (level)
  waiting for transfers between devices: 0.01 us -> 6.1 us
  starting transfers between devices: 86.7 us -> 82.4 us
  blocking collectives: 56.2 us -> 52.7 us
  Pallas kernels: 21.4 us -> 23.4 us
    all_to_all x1, waiting for transfers between devices: 0.01 us -> 6.1 us  [shards(): newest = lax.all_to_all(newest, 'sp', 0, 0, tiled=True)]
    all_to_all x1, blocking collectives: 23.2 us -> 18.3 us  [shards(): received = lax.all_to_all(payload, 'sp', 0, 0, tiled=True)]
    all_to_all x1, starting transfers between devices: 83.6 us -> 79.3 us  [shards(): newest = lax.all_to_all(newest, 'sp', 0, 0, tiled=True)]
    pallas_call x4 -> x5, Pallas kernels: 17.6 us -> 19.6 us  [call(): pl.pallas_call(body, in_specs=specs or whole(len(operands)), out_specs=wh...]
  transfers between devices with their start and end apart: 2 -> 2, of which waited for: 0 -> 1; matrix products, arithmetic and copies ran while one was open for 0% -> 0% of each run, Pallas kernels for 7% -> 2%
where the time goes in v5:
time: 166 us
  starting transfers between devices  82.4 us (50%)
  blocking collectives  52.7 us (32%)
  Pallas kernels  23.4 us (14%)
  waiting for transfers between devices  6.1 us (4%)
    all_to_all x1, starting transfers between devices, shards(): newest = lax.all_to_all(newest, 'sp', 0, 0, tiled=True)  79.3 us
    all_to_all x1, blocking collectives, shards(): squares = lax.all_to_all(squares, TP, 0, 0, tiled=True)  34.4 us
    pallas_call x5, Pallas kernels, call(): pl.pallas_call(body, in_specs=specs or whole(len(operands)), out_specs=wh...  19.6 us
    all_to_all x1, blocking collectives, shards(): received = lax.all_to_all(payload, 'sp', 0, 0, tiled=True)  18.3 us
    all_to_all x1, waiting for transfers between devices, shards(): newest = lax.all_to_all(newest, 'sp', 0, 0, tiled=True)  6.1 us
    pallas_call x1, Pallas kernels, shards(): pl.pallas_call(token_body, grid=(1,), in_specs=[pl.BlockSpec((prompts, bl...  3.77 us
  transfers between devices with their start and end apart: 2, of which 1 were waited for; matrix products, arithmetic and copies ran while one was open for 0% of the time, Pallas kernels for 2%

profile of v5, /device:TPU:5, one launch (start us, length us, event | category | flops | bytes accessed | tf_op | source)
XLA Modules:
  0.0 165.9 jit_solution(6516180651988542219)
XLA Ops:
  0.6 10.3 %early.1 = (f32[12,64,128]{2,1,0:T(8,128)}, f32[3,16,256]{2,1,0:T(8,128)}, f32[16,128]{1,0:T(8,128)}, f32[16,128]{1,0:T(8,128)}, f32[8,256]{1,0:T(8,128)}) custom-call(bf16[12,128,2048]{2,1,0:T(8,128)(2,1)} %refs_0_.3, bf16[2048,256]{1,0:T(8,128)(2,1)} %refs_1_.3, bf16[64,2048]{1,0:T(8,128)(2,1)} %bitcast.11, bf16[32,2048]{1,0:T(8,128)(2,1)} %bitcast.14, ...), custom_call_target="tpu_custom_call" | custom-call | tf_op jit(solution)/shard_map/early/pallas_call | solution.py:355
  10.9 3.8 %token_.1 = (bf16[3,16,256]{2,1,0:T(8,128)(2,1)}, bf16[16,32,128]{2,1,0:T(8,128)(2,1)}, f32[16,128]{1,0:T(8,128)}, f32[16,64]{1,0:T(8,128)}) custom-call(bf16[12,128,2048]{2,1,0:T(8,128)(2,1)} %refs_0_.3, bf16[12,2048]{1,0:T(8,128)(2,1)} %next_ref.1, bf16[64,2048]{1,0:T(8,128)(2,1)} %bitcast.12, bf16[64,2048]{1,0:T(8,128)(2,1)} %bitcast.19, ...), custom_call_target="tpu_custom_call" | custom-call | tf_op jit(solution)/shard_map/token/pallas_call | solution.py:450
  14.7 79.3 %all-to-all-start = ((bf16[16,32,128]{2,1,0:T(8,128)(2,1)}), bf16[16,32,128]{2,1,0:T(8,128)(2,1)S(1)}, u32[]{:S(2)}, u32[]{:S(2)}) async-start(bf16[16,32,128]{2,1,0:T(8,128)(2,1)} %get-tuple-element.29), calls=%async_computation | async-start | bytes 262144 | tf_op jit(solution)/shard_map/all_to_all | solution.py:468
  93.9 3.1 %collective-permute-start = (bf16[3,16,256]{2,1,0:T(8,128)(2,1)}, bf16[3,16,256]{2,1,0:T(8,128)(2,1)S(1)}, u32[]{:S(2)}, u32[]{:S(2)}) collective-permute-start(bf16[3,16,256]{2,1,0:T(8,128)(2,1)} %get-tuple-element.19), channel_id=1, source_target_pairs={{0,32},{32,64},{64,96},{96,128},{128,160},{160,192},{192,224},{224... | collective-permute-start | bytes 73736 | tf_op jit(solution)/shard_map/ppermute | solution.py:469
  97.0 2.6 %late.1 = (f32[12,64,128]{2,1,0:T(8,128)}, f32[3,16,256]{2,1,0:T(8,128)}, f32[16,128]{1,0:T(8,128)}, f32[16,128]{1,0:T(8,128)}) custom-call(bf16[12,128,2048]{2,1,0:T(8,128)(2,1)} %refs_0_.3, bf16[2048,256]{1,0:T(8,128)(2,1)} %refs_1_.3, bf16[64,2048]{1,0:T(8,128)(2,1)} %bitcast.13, bf16[32,2048]{1,0:T(8,128)(2,1)} %bitcast.16, f32[12,32,128]{2,1,0:T(8,128)} %bitcast.18, ...), custom_call_target="tpu_custom_call" | custom-call | tf_op jit(solution)/shard_map/late/pallas_call | solution.py:355
  99.6 0.0 collective-permute-done.halo_ref
  99.6 0.0 copy-start.1
  99.6 6.1 %all-to-all-done.newest_ref.refs_1_ = bf16[16,32,128]{2,1,0:T(8,128)(2,1)S(1)} async-done(((bf16[16,32,128]{2,1,0:T(8,128)(2,1)}), bf16[16,32,128]{2,1,0:T(8,128)(2,1)S(1)}, u32[]{:S(2)}, u32[]{:S(2)}) %all-to-all-start) | async-done | bytes 131104 | tf_op jit(solution)/shard_map/all_to_all | solution.py:468
  105.7 0.0 copy-start
  105.7 0.0 copy-done.1
  105.7 0.7 copy-done
  106.4 3.1 %pack.1 = bf16[16,64,128]{2,1,0:T(8,128)(2,1)} custom-call(bf16[3,16,256]{2,1,0:T(8,128)(2,1)} %copy-done.1, f32[3,16,256]{2,1,0:T(8,128)} %get-tuple-element.25.lead_ref, f32[16,128]{1,0:T(8,128)} %get-tuple-element.26.weight_ref, f32[16,128]{1,0:T(8,128)} %get-tuple-element.27.logs_ref, f32[8,256]{1,0:T(8,128)} %get-tuple-element.18.taps_ref.refs_5_, ...), custom_call_target="tpu_custom_call" | custom-call | tf_op jit(solution)/shard_map/pack/pallas_call | solution.py:355
  109.5 18.3 %all_to_all.15.refs_0_ = bf16[16,64,128]{2,1,0:T(8,128)(2,1)} all-to-all(bf16[16,64,128]{2,1,0:T(8,128)(2,1)} %pack.1), channel_id=1, replica_groups=mesh['grp'=2,'sp'=16,'tp_0'=16,'tp_1'=2] {'sp'}, dimensions={0} | all-to-all | bytes 524288 | tf_op jit(solution)/shard_map/all_to_all | solution.py:495
  127.9 2.2 %read.1 = (bf16[48,128]{1,0:T(8,128)(2,1)}, f32[8,128]{1,0:T(8,128)}, f32[32,1,128]{2,1,0:T(1,128)}) custom-call(bf16[16,64,128]{2,1,0:T(8,128)(2,1)} %all_to_all.15.refs_0_, bf16[16,32,128]{2,1,0:T(8,128)(2,1)} %copy-done, f32[16,128]{1,0:T(8,128)} %get-tuple-element.20.refs_8_.refs_2_, f32[16,64]{1,0:T(8,128)} %get-tuple-element.30.refs_3_), custom_call_target="tpu_custom_call" | custom-call | tf_op jit(solution)/shard_map/read/pallas_call | solution.py:355
  130.1 34.4 %all_to_all.16.parts_ref = f32[32,1,128]{2,1,0:T(1,128)} all-to-all(f32[32,1,128]{2,1,0:T(1,128)} %get-tuple-element.32), channel_id=1, replica_groups=mesh['grp'=2,'sp'=16,'tp_0'=16,'tp_1'=2] {'tp_0','tp_1'}, dimensions={0} | all-to-all | bytes 32768 | tf_op jit(solution)/shard_map/all_to_all | solution.py:510
  164.5 1.4 final.1
Async XLA Ops:
  14.7 91.1 %all-to-all-start = ((bf16[16,32,128]{2,1,0:T(8,128)(2,1)}), bf16[16,32,128]{2,1,0:T(8,128)(2,1)S(1)}, u32[]{:S(2)}, u32[]{:S(2)}) async-start(bf16[16,32,128]{2,1,0:T(8,128)(2,1)} %get-tuple-element.29), calls=%async_computation | async-start | bytes 262144 | tf_op jit(solution)/shard_map/all_to_all | solution.py:468
  93.9 5.7 %collective-permute-start = (bf16[3,16,256]{2,1,0:T(8,128)(2,1)}, bf16[3,16,256]{2,1,0:T(8,128)(2,1)S(1)}, u32[]{:S(2)}, u32[]{:S(2)}) collective-permute-start(bf16[3,16,256]{2,1,0:T(8,128)(2,1)} %get-tuple-element.19), channel_id=1, source_target_pairs={{0,32},{32,64},{64,96},{96,128},{128,160},{160,192},{192,224},{224... | collective-permute-start | bytes 73736 | tf_op jit(solution)/shard_map/ppermute | solution.py:469
  99.6 6.1 %copy-start.1 = (bf16[3,16,256]{2,1,0:T(8,128)(2,1)}, bf16[3,16,256]{2,1,0:T(8,128)(2,1)S(1)}, u32[]{:S(2)}) copy-start(bf16[3,16,256]{2,1,0:T(8,128)(2,1)S(1)} %collective-permute-done.halo_ref) | copy-start | bytes 73732
  105.7 0.7 copy-start

commit v6 on v5

--- a/solution.py
+++ b/solution.py
@@ -67,8 +67,9 @@
 
 def local_body(
     x_hbm, key_hbm, value_hbm, step_hbm, off_hbm, taps_ref, bias_ref, decay_ref,
-    state_ref, lead_ref, weight_ref, logs_ref,
-    x_ref, w_ref, value_ref, step_ref, off_ref, wide_ref, map_ref, rows_ref, small_sems, sems,
+    state_hbm, lead_hbm, weight_hbm, logs_hbm,
+    x_ref, w_ref, value_ref, step_ref, off_ref, wide_ref, map_ref, rows_ref,
+    state_ref, lead_ref, weight_ref, logs_ref, small_sems, sems,
     *, per,
 ):
     prompts, length, width = x_hbm.shape
@@ -131,6 +132,17 @@
     for b in range(prompts):
         weighted = (wide_ref[b] * weight[b : b + 1]).astype(BF16)
         state_ref[b] = dot(weighted, map_ref[b])
+    results = (
+        (state_ref, state_hbm),
+        (lead_ref, lead_hbm),
+        (weight_ref, weight_hbm),
+        (logs_ref, logs_hbm),
+    )
+    results = [pltpu.make_async_copy(*pair, small_sems.at[i]) for i, pair in enumerate(results)]
+    for copy in results:
+        copy.start()
+    for copy in results:
+        copy.wait()
 
 
 def taps_of(vt_ref, kt_ref):
@@ -141,8 +153,8 @@
     return jnp.concatenate([value_taps, kt_ref[:, pl.ds(at, STATE)].astype(F32)], axis=1)
 
 
-def on_last():
-    return lax.axis_index("sp") == lax.axis_size("sp") - 1
+def is_late():
+    return lax.axis_index("sp") >= lax.axis_size("sp") - 2
 
 
 def early_body(
@@ -151,7 +163,7 @@
 ):
     taps_ref[:CONV] = taps_of(vt_ref, kt_ref)
 
-    @pl.when(jnp.logical_not(on_last()))
+    @pl.when(jnp.logical_not(is_late()))
     def _():
         local_body(
             x_hbm, key_hbm, value_hbm, step_hbm, off_hbm, taps_ref, bias_ref, decay_ref,
@@ -164,52 +176,53 @@
     state_in, lead_in, weight_in, logs_in,
     state_ref, lead_ref, weight_ref, logs_ref, *scratch, per,
 ):
-    @pl.when(on_last())
+    @pl.when(is_late())
     def _():
         local_body(
             x_hbm, key_hbm, value_hbm, step_hbm, off_hbm, taps_ref, bias_ref, decay_ref,
             state_ref, lead_ref, weight_ref, logs_ref, *scratch, per=per,
         )
 
-    @pl.when(jnp.logical_not(on_last()))
-    def _():
-        copies = []
-        inputs = (state_in, lead_in, weight_in, logs_in)
-        outputs = (state_ref, lead_ref, weight_ref, logs_ref)
-        for i, (source, target) in enumerate(zip(inputs, outputs)):
-            copies.append(pltpu.make_async_copy(source, target, scratch[-2].at[i]))
-        for copy in copies:
-            copy.start()
-        for copy in copies:
-            copy.wait()
-
 
 def token_body(
-    x_ref, next_ref, value_ref, gate_ref, key_ref, query_ref, step_ref, taps_ref, qt_ref,
+    x_hbm, value_hbm, gate_hbm, step_hbm, key_hbm, query_hbm, next_ref, taps_ref, qt_ref,
     bias_ref, decay_ref, skip_ref,
     trail_ref, newest_ref, decay_out_ref, gate_out_ref,
-    pad_ref, last_ref,
+    x_ref, rows_ref, maps_ref, pad_ref, last_ref, sems,
 ):
     prompts, block, width = x_ref.shape
     head = lax.axis_index(TP)
-    group = head // (HEADS // GROUPS)
     padded = pad_ref.shape[0]
-    at = pl.multiple_of(group * STATE, STATE)
-    query = query_ref[:, pl.ds(at, STATE)]
-    key = key_ref[:, pl.ds(at, STATE)]
+    heads = step_hbm.shape[0]
+    at = pl.multiple_of((head // (HEADS // GROUPS)) * STATE, STATE)
+    tail = x_hbm.shape[1] - block
+    copies = (
+        (key_hbm.at[:, pl.ds(at, STATE)], maps_ref.at[:, pl.ds(0, STATE)]),
+        (query_hbm.at[:, pl.ds(at, STATE)], maps_ref.at[:, pl.ds(STATE, STATE)]),
+        (value_hbm, rows_ref.at[pl.ds(0, P_SIZE)]),
+        (gate_hbm, rows_ref.at[pl.ds(P_SIZE, P_SIZE)]),
+        (step_hbm, rows_ref.at[pl.ds(2 * P_SIZE, heads)]),
+        (x_hbm.at[:, pl.ds(tail, block)], x_ref),
+    )
+    copies = [pltpu.make_async_copy(*pair, sems.at[i]) for i, pair in enumerate(copies)]
+    for copy in copies:
+        copy.start()
     value_taps = taps_ref[:CONV, :P_SIZE]
     key_taps = taps_ref[:CONV, LANES:]
     query_taps = qt_ref[:, pl.ds(at, STATE)].astype(F32)
     pad_ref[...] = jnp.zeros_like(pad_ref)
     pad_ref[:prompts] = next_ref[...].astype(F32)
     token = pad_ref[...].astype(BF16)
+    for copy in copies:
+        copy.wait()
     rows = jnp.concatenate([x_ref[...].reshape(prompts * block, width), token], axis=0)
     count = prompts * block
-    values = rounded(dot(rows, value_ref[...], ((1,), (1,))))
-    keys = rounded(dot(rows, key))
-    queries = rounded(dot(rows, query))
-    new_step = pick(rounded(dot(token, step_ref[...], ((1,), (1,)))), head)
-    new_gate = rounded(dot(token, gate_ref[...], ((1,), (1,))))
+    maps = rounded(dot(rows, maps_ref[...]))
+    keys, queries = maps[:, :STATE], maps[:, STATE:]
+    others = rounded(dot(rows, rows_ref[...], ((1,), (1,))))
+    values = others[:, :P_SIZE]
+    new_gate = others[count:, P_SIZE : 2 * P_SIZE]
+    new_step = pick(others[count:, 2 * P_SIZE :], head)
     last_ref[...] = jnp.zeros_like(last_ref)
     for b in range(prompts):
         at_row = (b + 1) * block - (CONV - 1)
@@ -351,11 +364,12 @@
     return [pl.BlockSpec(memory_space=pltpu.VMEM) for _ in range(count)]
 
 
-def call(body, outs, *operands, specs=None, scratch=(), name=None):
+def call(body, outs, *operands, specs=None, out_specs=None, scratch=(), aliases=(), name=None):
     return pl.pallas_call(
         body,
         in_specs=specs or whole(len(operands)),
-        out_specs=whole(len(outs)),
+        out_specs=out_specs or whole(len(outs)),
+        input_output_aliases=dict(aliases),
         out_shape=outs,
         scratch_shapes=scratch,
         name=name,
@@ -416,6 +430,7 @@
         pltpu.VMEM((prompts, P_SIZE, length), F32),
         pltpu.VMEM((prompts, length, STATE), BF16),
         pltpu.VMEM((2, padded, length), F32),
+        *[pltpu.VMEM(result.shape, result.dtype) for result in local_outs],
         pltpu.SemaphoreType.DMA((4,)),
         pltpu.SemaphoreType.DMA((prompts // per,)),
     ]
@@ -428,43 +443,42 @@
         bias,
         decay_rate,
         specs=away * 5 + whole(4),
+        out_specs=away * 4 + whole(1),
         scratch=local_scratch,
         name="early",
     )
     block = 16
-    tail = length // block - 1
-    token_operands = (
+    trail, newest, new_decay, new_gate = call(
+        token_body,
+        [
+            out((CONV - 1, padded, 2 * LANES), BF16),
+            out((dests, 2 * padded, LANES), BF16),
+            out((padded, LANES), F32),
+            out((padded, P_SIZE), F32),
+        ],
         prompt_layer_input,
-        next_token_input,
         value_rows,
         gate_rows,
+        step_rows,
         key_projection,
         query_projection,
-        step_rows,
+        next_token_input,
         taps,
         query_filter_taps,
         bias,
         decay_rate,
         skip,
-    )
-    trail, newest, new_decay, new_gate = pl.pallas_call(
-        token_body,
-        grid=(1,),
-        in_specs=[pl.BlockSpec((prompts, block, width), lambda i: (0, tail, 0))]
-        + whole(len(token_operands) - 1),
-        out_specs=whole(4),
-        out_shape=[
-            out((CONV - 1, padded, 2 * LANES), BF16),
-            out((dests, 2 * padded, LANES), BF16),
-            out((padded, LANES), F32),
-            out((padded, P_SIZE), F32),
-        ],
-        scratch_shapes=[
+        specs=away * 6 + whole(6),
+        scratch=[
+            pltpu.VMEM((prompts, block, width), BF16),
+            pltpu.VMEM((2 * P_SIZE + step_rows.shape[0], width), BF16),
+            pltpu.VMEM((width, 2 * STATE), BF16),
             pltpu.VMEM((padded, width), F32),
             pltpu.VMEM((CONV - 1, padded, 3 * LANES), F32),
+            pltpu.SemaphoreType.DMA((6,)),
         ],
         name="token",
-    )(*token_operands)
+    )
     newest = lax.all_to_all(newest, "sp", 0, 0, tiled=True)
     halo = lax.ppermute(trail, "sp", [(i, i + 1) for i in range(dests - 1)])
     state, lead, weight, logs = call(
@@ -477,7 +491,9 @@
         new_decay,
         *early,
         specs=away * 5 + whole(3) + away * 5,
+        out_specs=away * 4,
         scratch=local_scratch,
+        aliases=((9 + i, i) for i in range(4)),
         name="late",
     )
     (payload,) = call(

time: 166 us -> 163 us (0.982)
  starting transfers between devices: 82.4 us -> 78 us
  waiting for transfers between devices: 6.1 us -> 7.88 us
    all_to_all x1, starting transfers between devices: 79.3 us -> 74.9 us  [shards(): newest = lax.all_to_all(newest, 'sp', 0, 0, tiled=True)]
  transfers between devices with their start and end apart: 2 -> 2, of which waited for: 1 -> 2; matrix products, arithmetic and copies ran while one was open for 0% -> 0% of each run, Pallas kernels for 2% -> 1%
where the time goes in v6:
time: 163 us; the launch traced here: 162 us
  starting transfers between devices  78 us (48%)
  blocking collectives  52.7 us (32%)
  Pallas kernels  22.5 us (14%)
  waiting for transfers between devices  7.88 us (5%)
    all_to_all x1, starting transfers between devices, shards(): newest = lax.all_to_all(newest, 'sp', 0, 0, tiled=True)  74.9 us
    all_to_all x1, blocking collectives, shards(): squares = lax.all_to_all(squares, TP, 0, 0, tiled=True)  34.3 us
    pallas_call x6, Pallas kernels, call(): pl.pallas_call(body, in_specs=specs or whole(len(operands)), out_specs=ou...  22.5 us
    all_to_all x1, blocking collectives, shards(): received = lax.all_to_all(payload, 'sp', 0, 0, tiled=True)  18.4 us
    all_to_all x1, waiting for transfers between devices, shards(): newest = lax.all_to_all(newest, 'sp', 0, 0, tiled=True)  7.56 us
  transfers between devices with their start and end apart: 2, of which 2 were waited for; matrix products, arithmetic and copies ran while one was open for 0% of the time, Pallas kernels for 1%

profile of v6, /device:TPU:5, one launch (start us, length us, event | category | flops | bytes accessed | tf_op | source)
XLA Modules:
  0.0 162.4 jit_solution(14155325843181981069)
XLA Ops:
  0.6 10.8 %early.1 = (f32[12,64,128]{2,1,0:T(8,128)}, f32[3,16,256]{2,1,0:T(8,128)}, f32[16,128]{1,0:T(8,128)}, f32[16,128]{1,0:T(8,128)}, f32[8,256]{1,0:T(8,128)}) custom-call(bf16[12,128,2048]{2,1,0:T(8,128)(2,1)} %refs_0_.3, bf16[2048,256]{1,0:T(8,128)(2,1)} %refs_1_.3, bf16[64,2048]{1,0:T(8,128)(2,1)} %bitcast.11, bf16[32,2048]{1,0:T(8,128)(2,1)} %bitcast.14, ...), custom_call_target="tpu_custom_call" | custom-call | tf_op jit(solution)/shard_map/early/pallas_call | solution.py:368
  11.5 4.1 %token_.1 = (bf16[3,16,256]{2,1,0:T(8,128)(2,1)}, bf16[16,32,128]{2,1,0:T(8,128)(2,1)}, f32[16,128]{1,0:T(8,128)}, f32[16,64]{1,0:T(8,128)}) custom-call(bf16[12,128,2048]{2,1,0:T(8,128)(2,1)} %refs_0_.3, bf16[64,2048]{1,0:T(8,128)(2,1)} %bitcast.12, bf16[64,2048]{1,0:T(8,128)(2,1)} %bitcast.19, bf16[32,2048]{1,0:T(8,128)(2,1)} %bitcast.15, ...), custom_call_target="tpu_custom_call" | custom-call | tf_op jit(solution)/shard_map/token/pallas_call | solution.py:368
  15.5 74.9 %all-to-all-start = ((bf16[16,32,128]{2,1,0:T(8,128)(2,1)}), bf16[16,32,128]{2,1,0:T(8,128)(2,1)S(1)}, u32[]{:S(2)}, u32[]{:S(2)}) async-start(bf16[16,32,128]{2,1,0:T(8,128)(2,1)} %get-tuple-element.29), calls=%async_computation | async-start | bytes 262144 | tf_op jit(solution)/shard_map/all_to_all | solution.py:482
  90.5 3.1 %collective-permute-start = (bf16[3,16,256]{2,1,0:T(8,128)(2,1)}, bf16[3,16,256]{2,1,0:T(8,128)(2,1)S(1)}, u32[]{:S(2)}, u32[]{:S(2)}) collective-permute-start(bf16[3,16,256]{2,1,0:T(8,128)(2,1)} %get-tuple-element.19), channel_id=1, source_target_pairs={{0,32},{32,64},{64,96},{96,128},{128,160},{160,192},{192,224},{224... | collective-permute-start | bytes 73736 | tf_op jit(solution)/shard_map/ppermute | solution.py:483
  93.6 0.8 late.1
  94.4 0.3 collective-permute-done.halo_ref
  94.7 0.0 copy-start.1
  94.7 7.6 %all-to-all-done.newest_ref.refs_1_ = bf16[16,32,128]{2,1,0:T(8,128)(2,1)S(1)} async-done(((bf16[16,32,128]{2,1,0:T(8,128)(2,1)}), bf16[16,32,128]{2,1,0:T(8,128)(2,1)S(1)}, u32[]{:S(2)}, u32[]{:S(2)}) %all-to-all-start) | async-done | bytes 131104 | tf_op jit(solution)/shard_map/all_to_all | solution.py:482
  102.3 0.0 copy-start
  102.3 0.0 copy-done.1
  102.3 0.7 copy-done
  102.9 3.1 %pack.1 = bf16[16,64,128]{2,1,0:T(8,128)(2,1)} custom-call(bf16[3,16,256]{2,1,0:T(8,128)(2,1)} %copy-done.1, f32[3,16,256]{2,1,0:T(8,128)} %get-tuple-element.25.lead_ref, f32[16,128]{1,0:T(8,128)} %get-tuple-element.26.weight_ref, f32[16,128]{1,0:T(8,128)} %get-tuple-element.27.logs_ref, f32[8,256]{1,0:T(8,128)} %get-tuple-element.18.taps_ref.refs_5_, ...), custom_call_target="tpu_custom_call" | custom-call | tf_op jit(solution)/shard_map/pack/pallas_call | solution.py:368
  106.1 18.4 %all_to_all.15.refs_0_ = bf16[16,64,128]{2,1,0:T(8,128)(2,1)} all-to-all(bf16[16,64,128]{2,1,0:T(8,128)(2,1)} %pack.1), channel_id=1, replica_groups=mesh['grp'=2,'sp'=16,'tp_0'=16,'tp_1'=2] {'sp'}, dimensions={0} | all-to-all | bytes 524288 | tf_op jit(solution)/shard_map/all_to_all | solution.py:511
  124.5 2.2 %read.1 = (bf16[48,128]{1,0:T(8,128)(2,1)}, f32[8,128]{1,0:T(8,128)}, f32[32,1,128]{2,1,0:T(1,128)}) custom-call(bf16[16,64,128]{2,1,0:T(8,128)(2,1)} %all_to_all.15.refs_0_, bf16[16,32,128]{2,1,0:T(8,128)(2,1)} %copy-done, f32[16,128]{1,0:T(8,128)} %get-tuple-element.20.refs_8_.refs_2_, f32[16,64]{1,0:T(8,128)} %get-tuple-element.30.refs_3_), custom_call_target="tpu_custom_call" | custom-call | tf_op jit(solution)/shard_map/read/pallas_call | solution.py:368
  126.7 34.3 %all_to_all.16.parts_ref = f32[32,1,128]{2,1,0:T(1,128)} all-to-all(f32[32,1,128]{2,1,0:T(1,128)} %get-tuple-element.32), channel_id=1, replica_groups=mesh['grp'=2,'sp'=16,'tp_0'=16,'tp_1'=2] {'tp_0','tp_1'}, dimensions={0} | all-to-all | bytes 32768 | tf_op jit(solution)/shard_map/all_to_all | solution.py:526
  161.0 1.4 final.1
Async XLA Ops:
  15.5 86.7 %all-to-all-start = ((bf16[16,32,128]{2,1,0:T(8,128)(2,1)}), bf16[16,32,128]{2,1,0:T(8,128)(2,1)S(1)}, u32[]{:S(2)}, u32[]{:S(2)}) async-start(bf16[16,32,128]{2,1,0:T(8,128)(2,1)} %get-tuple-element.29), calls=%async_computation | async-start | bytes 262144 | tf_op jit(solution)/shard_map/all_to_all | solution.py:482
  90.5 4.2 %collective-permute-start = (bf16[3,16,256]{2,1,0:T(8,128)(2,1)}, bf16[3,16,256]{2,1,0:T(8,128)(2,1)S(1)}, u32[]{:S(2)}, u32[]{:S(2)}) collective-permute-start(bf16[3,16,256]{2,1,0:T(8,128)(2,1)} %get-tuple-element.19), channel_id=1, source_target_pairs={{0,32},{32,64},{64,96},{96,128},{128,160},{160,192},{192,224},{224... | collective-permute-start | bytes 73736 | tf_op jit(solution)/shard_map/ppermute | solution.py:483
  94.7 7.6 %copy-start.1 = (bf16[3,16,256]{2,1,0:T(8,128)(2,1)}, bf16[3,16,256]{2,1,0:T(8,128)(2,1)S(1)}, u32[]{:S(2)}) copy-start(bf16[3,16,256]{2,1,0:T(8,128)(2,1)S(1)} %collective-permute-done.halo_ref) | copy-start | bytes 73732
  102.3 0.7 copy-start

commit v7 on v6

--- a/solution.py
+++ b/solution.py
@@ -66,10 +66,10 @@
 
 
 def local_body(
-    x_hbm, key_hbm, value_hbm, step_hbm, off_hbm, taps_ref, bias_ref, decay_ref,
+    x_hbm, key_hbm, value_hbm, step_hbm, off_hbm, vt_hbm, kt_hbm, bias_hbm, decay_hbm,
     state_hbm, lead_hbm, weight_hbm, logs_hbm,
-    x_ref, w_ref, value_ref, step_ref, off_ref, wide_ref, map_ref, rows_ref,
-    state_ref, lead_ref, weight_ref, logs_ref, small_sems, sems,
+    x_ref, w_ref, value_ref, step_ref, off_ref, vt_ref, kt_ref, bias_ref, decay_ref,
+    wide_ref, map_ref, rows_ref, state_ref, lead_ref, weight_ref, logs_ref, small_sems, sems,
     *, per,
 ):
     prompts, length, width = x_hbm.shape
@@ -81,6 +81,10 @@
         (step_hbm, step_ref),
         (key_hbm.at[:, pl.ds(at, STATE)], w_ref.at[:, pl.ds(LANES, STATE)]),
         (off_hbm, off_ref),
+        (vt_hbm, vt_ref),
+        (kt_hbm, kt_ref),
+        (bias_hbm, bias_ref),
+        (decay_hbm, decay_ref),
     )
     small = [pltpu.make_async_copy(*pair, small_sems.at[i]) for i, pair in enumerate(small)]
     for copy in small:
@@ -95,9 +99,10 @@
     small[1].wait()
     step_row = jnp.broadcast_to(pick_row(step_ref[...], head), (P_SIZE, width)).astype(BF16)
     w_ref[:, :LANES] = jnp.transpose(jnp.concatenate([value_ref[...], step_row], axis=0))
-    taps = taps_ref[:CONV]
+    for copy in small[3:]:
+        copy.wait()
+    taps = taps_of(vt_ref, kt_ref)
     rows_ref[...] = jnp.zeros_like(rows_ref)
-    small[3].wait()
     offset = off_ref[...]
     offset = jnp.where(iota(offset.shape, 1) == head, offset, 0.0)
     rows_ref[1, :prompts] = jnp.sum(offset, axis=1)
@@ -157,38 +162,26 @@
     return lax.axis_index("sp") >= lax.axis_size("sp") - 2
 
 
-def early_body(
-    x_hbm, key_hbm, value_hbm, step_hbm, off_hbm, vt_ref, kt_ref, bias_ref, decay_ref,
-    state_ref, lead_ref, weight_ref, logs_ref, taps_ref, *scratch, per,
-):
-    taps_ref[:CONV] = taps_of(vt_ref, kt_ref)
-
+def early_body(*refs, per):
     @pl.when(jnp.logical_not(is_late()))
     def _():
-        local_body(
-            x_hbm, key_hbm, value_hbm, step_hbm, off_hbm, taps_ref, bias_ref, decay_ref,
-            state_ref, lead_ref, weight_ref, logs_ref, *scratch, per=per,
-        )
-
-
-def late_body(
-    x_hbm, key_hbm, value_hbm, step_hbm, off_hbm, taps_ref, bias_ref, decay_ref, after_ref,
-    state_in, lead_in, weight_in, logs_in,
-    state_ref, lead_ref, weight_ref, logs_ref, *scratch, per,
-):
+        local_body(*refs, per=per)
+
+
+def late_body(*refs, operands, per):
+    passed = operands + 5
+
     @pl.when(is_late())
     def _():
-        local_body(
-            x_hbm, key_hbm, value_hbm, step_hbm, off_hbm, taps_ref, bias_ref, decay_ref,
-            state_ref, lead_ref, weight_ref, logs_ref, *scratch, per=per,
-        )
+        local_body(*refs[:operands], *refs[passed:], per=per)
 
 
 def token_body(
-    x_hbm, value_hbm, gate_hbm, step_hbm, key_hbm, query_hbm, next_ref, taps_ref, qt_ref,
-    bias_ref, decay_ref, skip_ref,
-    trail_ref, newest_ref, decay_out_ref, gate_out_ref,
-    x_ref, rows_ref, maps_ref, pad_ref, last_ref, sems,
+    x_hbm, value_hbm, gate_hbm, step_hbm, key_hbm, query_hbm, next_hbm, vt_hbm, kt_hbm, qt_hbm,
+    bias_hbm, decay_hbm, skip_hbm, after_hbm,
+    trail_ref, newest_ref, direct_ref, decay_out_ref, gate_out_ref,
+    x_ref, rows_ref, maps_ref, next_ref, vt_ref, kt_ref, qt_ref, bias_ref, decay_ref, skip_ref,
+    pad_ref, last_ref, sems,
 ):
     prompts, block, width = x_ref.shape
     head = lax.axis_index(TP)
@@ -203,18 +196,25 @@
         (gate_hbm, rows_ref.at[pl.ds(P_SIZE, P_SIZE)]),
         (step_hbm, rows_ref.at[pl.ds(2 * P_SIZE, heads)]),
         (x_hbm.at[:, pl.ds(tail, block)], x_ref),
+        (next_hbm, next_ref),
+        (vt_hbm, vt_ref),
+        (kt_hbm, kt_ref),
+        (qt_hbm, qt_ref),
+        (bias_hbm, bias_ref),
+        (decay_hbm, decay_ref),
+        (skip_hbm, skip_ref),
     )
     copies = [pltpu.make_async_copy(*pair, sems.at[i]) for i, pair in enumerate(copies)]
     for copy in copies:
         copy.start()
-    value_taps = taps_ref[:CONV, :P_SIZE]
-    key_taps = taps_ref[:CONV, LANES:]
+    for copy in copies:
+        copy.wait()
+    taps = taps_of(vt_ref, kt_ref)
+    value_taps, key_taps = taps[:, :P_SIZE], taps[:, LANES:]
     query_taps = qt_ref[:, pl.ds(at, STATE)].astype(F32)
     pad_ref[...] = jnp.zeros_like(pad_ref)
     pad_ref[:prompts] = next_ref[...].astype(F32)
     token = pad_ref[...].astype(BF16)
-    for copy in copies:
-        copy.wait()
     rows = jnp.concatenate([x_ref[...].reshape(prompts * block, width), token], axis=0)
     count = prompts * block
     maps = rounded(dot(rows, maps_ref[...]))
@@ -247,24 +247,23 @@
     speed = jnp.exp(pick(decay_ref[...], head))
     decay_out_ref[...] = jnp.broadcast_to(jnp.exp(-speed * step), decay_out_ref.shape)
     agreement = jnp.sum(new_in * new_out, axis=1, keepdims=True)
-    direct = new_input * (step * agreement + pick(skip_ref[...], head))
-    high = rounded(direct)
-    direct = jnp.concatenate([high, direct - high], axis=1)
-    newest = jnp.concatenate([new_out, direct], axis=0).astype(BF16)
+    direct_ref[...] = new_input * (step * agreement + pick(skip_ref[...], head))
+    newest = new_out.astype(BF16)
     for d in range(newest_ref.shape[0]):
         newest_ref[d] = newest
     gate_out_ref[...] = silu(new_gate)
 
 
 def pack_body(
-    halo_ref, lead_ref, weight_ref, logs_ref, taps_ref, state_ref, newest_ref, out_ref,
+    halo_ref, lead_ref, weight_ref, logs_ref, vt_ref, kt_ref, state_ref, newest_ref, direct_ref,
+    decay_ref, out_ref,
 ):
     prompts, rows, _ = state_ref.shape
     dests = out_ref.shape[0]
     keep = rows // dests
     padded = logs_ref.shape[0]
-    taps = taps_ref[...]
-    new_out = newest_ref[dests - 1, :padded, :].astype(F32)
+    taps = taps_of(vt_ref, kt_ref)
+    new_out = newest_ref[dests - 1].astype(F32)
     window = [halo_ref[k].astype(F32) for k in range(CONV - 1)]
     window = window + [lead_ref[k] for k in range(CONV - 1)]
     weighted, maps = [], []
@@ -299,6 +298,9 @@
             out_ref[2 * k, at : at + pair_rows, :] = even[k].astype(BF16)
             out_ref[2 * k + 1, at : at + pair_rows, :] = odd[k].astype(BF16)
     reads = jnp.transpose(reads)[:padded]
+    on_last = lax.axis_index("sp") == dests - 1
+    final = decay_ref[...] * reads[:, :P_SIZE] + direct_ref[...]
+    reads = jnp.where(on_last, final, reads[:, :P_SIZE])
     high = rounded(reads)
     extra = jnp.concatenate([high, reads - high], axis=1)
     corner = (padded, LANES)
@@ -312,7 +314,7 @@
 
 
 def read_body(
-    parts_ref, newest_ref, decay_ref, gate_ref, cache_ref, gated_ref, squares_ref, *, prompts,
+    parts_ref, decay_ref, gate_ref, cache_ref, gated_ref, squares_ref, *, prompts,
 ):
     sources, _, _ = parts_ref.shape
     padded = decay_ref.shape[0]
@@ -330,11 +332,12 @@
         per_row = jnp.sum(jnp.where(state_own, decay, 0.0), axis=1, keepdims=True)
         per_prompt = jnp.sum(jnp.where(read_own, decay, 0.0), axis=1, keepdims=True)
         total = total * per_row + parts_ref[s, :rows, :].astype(F32)
-        reads = reads * per_prompt + (extra[:, :P_SIZE] + extra[:, P_SIZE:])
+        reads = reads * per_prompt
+        if s == sources - 1:
+            reads = decay_ref[...] * reads
+        reads = reads + (extra[:, :P_SIZE] + extra[:, P_SIZE:])
     cache_ref[...] = total.astype(BF16)
-    direct = newest_ref[sources - 1, padded:, :].astype(F32)
-    direct = direct[:, :P_SIZE] + direct[:, P_SIZE:]
-    gated = (decay_ref[:, :P_SIZE] * reads + direct) * gate_ref[...]
+    gated = reads * gate_ref[...]
     gated = jnp.where(iota(gated.shape, 0) < prompts, gated, 0.0)
     squares = jnp.sum(gated * gated, axis=1, keepdims=True)
     squares = jnp.sum(jnp.where(read_own, squares, 0.0), axis=0, keepdims=True)
@@ -419,6 +422,10 @@
         value_rows,
         step_rows,
         offset_rows,
+        value_filter_taps,
+        key_filter_taps,
+        bias,
+        decay_rate,
     )
     away = [pl.BlockSpec(memory_space=pl.ANY)]
     local_scratch = [
@@ -427,33 +434,34 @@
         pltpu.VMEM(value_rows.shape, BF16),
         pltpu.VMEM(step_rows.shape, BF16),
         pltpu.VMEM(offset_rows.shape, F32),
+        pltpu.VMEM(value_filter_taps.shape, BF16),
+        pltpu.VMEM(key_filter_taps.shape, BF16),
+        pltpu.VMEM(bias.shape, F32),
+        pltpu.VMEM(decay_rate.shape, F32),
         pltpu.VMEM((prompts, P_SIZE, length), F32),
         pltpu.VMEM((prompts, length, STATE), BF16),
         pltpu.VMEM((2, padded, length), F32),
         *[pltpu.VMEM(result.shape, result.dtype) for result in local_outs],
-        pltpu.SemaphoreType.DMA((4,)),
+        pltpu.SemaphoreType.DMA((8,)),
         pltpu.SemaphoreType.DMA((prompts // per,)),
     ]
-    *early, taps = call(
+    early = call(
         lambda *refs: early_body(*refs, per=per),
-        [*local_outs, out((8, 2 * LANES), F32)],
+        local_outs,
         *local_operands,
-        value_filter_taps,
-        key_filter_taps,
-        bias,
-        decay_rate,
-        specs=away * 5 + whole(4),
-        out_specs=away * 4 + whole(1),
+        specs=away * len(local_operands),
+        out_specs=away * 4,
         scratch=local_scratch,
         name="early",
     )
     block = 16
-    trail, newest, new_decay, new_gate = call(
+    trail, newest, direct, new_decay, new_gate = call(
         token_body,
         [
             out((CONV - 1, padded, 2 * LANES), BF16),
-            out((dests, 2 * padded, LANES), BF16),
-            out((padded, LANES), F32),
+            out((dests, padded, LANES), BF16),
+            out((padded, P_SIZE), F32),
+            out((padded, P_SIZE), F32),
             out((padded, P_SIZE), F32),
         ],
         prompt_layer_input,
@@ -463,37 +471,44 @@
         key_projection,
         query_projection,
         next_token_input,
-        taps,
+        value_filter_taps,
+        key_filter_taps,
         query_filter_taps,
         bias,
         decay_rate,
         skip,
-        specs=away * 6 + whole(6),
+        early[3],
+        specs=away * 14,
         scratch=[
             pltpu.VMEM((prompts, block, width), BF16),
             pltpu.VMEM((2 * P_SIZE + step_rows.shape[0], width), BF16),
             pltpu.VMEM((width, 2 * STATE), BF16),
+            pltpu.VMEM(next_token_input.shape, BF16),
+            pltpu.VMEM(value_filter_taps.shape, BF16),
+            pltpu.VMEM(key_filter_taps.shape, BF16),
+            pltpu.VMEM(query_filter_taps.shape, BF16),
+            pltpu.VMEM(bias.shape, F32),
+            pltpu.VMEM(decay_rate.shape, F32),
+            pltpu.VMEM(skip.shape, F32),
             pltpu.VMEM((padded, width), F32),
             pltpu.VMEM((CONV - 1, padded, 3 * LANES), F32),
-            pltpu.SemaphoreType.DMA((6,)),
+            pltpu.SemaphoreType.DMA((13,)),
         ],
         name="token",
     )
     newest = lax.all_to_all(newest, "sp", 0, 0, tiled=True)
     halo = lax.ppermute(trail, "sp", [(i, i + 1) for i in range(dests - 1)])
+    count = len(local_operands)
     state, lead, weight, logs = call(
-        lambda *refs: late_body(*refs, per=per),
+        lambda *refs: late_body(*refs, operands=count, per=per),
         local_outs,
         *local_operands,
-        taps,
-        bias,
-        decay_rate,
         new_decay,
         *early,
-        specs=away * 5 + whole(3) + away * 5,
+        specs=away * (count + 5),
         out_specs=away * 4,
         scratch=local_scratch,
-        aliases=((9 + i, i) for i in range(4)),
+        aliases=((count + 1 + i, i) for i in range(4)),
         name="late",
     )
     (payload,) = call(
@@ -503,9 +518,12 @@
         lead,
         weight,
         logs,
-        taps,
+        value_filter_taps,
+        key_filter_taps,
         state,
         newest,
+        direct,
+        new_decay,
         name="pack",
     )
     received = lax.all_to_all(payload, "sp", 0, 0, tiled=True)
@@ -518,7 +536,6 @@
             out((tp_size, 1, LANES), F32),
         ],
         received,
-        newest,
         new_decay,
         new_gate,
         name="read",

time: 163 us -> 159 us (0.975)
  Pallas kernels: 22.5 us -> 19.4 us
    pallas_call x6, Pallas kernels: 22.5 us -> 19.4 us  [call(): pl.pallas_call(body, in_specs=specs or whole(len(operands)), out_specs=ou...]
  transfers between devices with their start and end apart: 2 -> 2, of which waited for: 2 -> 2; matrix products, arithmetic and copies ran while one was open for 0% -> 0% of each run, Pallas kernels for 1% -> 0%
where the time goes in v7:
time: 159 us
  starting transfers between devices  78 us (49%)
  blocking collectives  52.2 us (33%)
  Pallas kernels  19.4 us (12%)
  waiting for transfers between devices  8.11 us (5%)
    all_to_all x1, starting transfers between devices, shards(): newest = lax.all_to_all(newest, 'sp', 0, 0, tiled=True)  74.9 us
    all_to_all x1, blocking collectives, shards(): squares = lax.all_to_all(squares, TP, 0, 0, tiled=True)  33.4 us
    pallas_call x6, Pallas kernels, call(): pl.pallas_call(body, in_specs=specs or whole(len(operands)), out_specs=ou...  19.4 us
    all_to_all x1, blocking collectives, shards(): received = lax.all_to_all(payload, 'sp', 0, 0, tiled=True)  18.8 us
    all_to_all x1, waiting for transfers between devices, shards(): newest = lax.all_to_all(newest, 'sp', 0, 0, tiled=True)  7.13 us
  transfers between devices with their start and end apart: 2, of which 2 were waited for; matrix products, arithmetic and copies ran while one was open for 0% of the time, Pallas kernels for 0%

profile of v7, /device:TPU:5, one launch (start us, length us, event | category | flops | bytes accessed | tf_op | source)
XLA Modules:
  0.0 158.9 jit_solution(18130885847447448361)
XLA Ops:
  0.6 9.3 %early.1 = (f32[12,64,128]{2,1,0:T(8,128)}, f32[3,16,256]{2,1,0:T(8,128)}, f32[16,128]{1,0:T(8,128)}, f32[16,128]{1,0:T(8,128)}) custom-call(bf16[12,128,2048]{2,1,0:T(8,128)(2,1)} %refs_0_.3, bf16[2048,256]{1,0:T(8,128)(2,1)} %refs_1_.3, bf16[64,2048]{1,0:T(8,128)(2,1)} %bitcast.11, bf16[32,2048]{1,0:T(8,128)(2,1)} %bitcast.14, f32[12,32,128]{2,1,0:T(8,128)} %bitcast.17, ...), custom_call_target="tpu_custom_call" | custom-call | tf_op jit(solution)/shard_map/early/pallas_call | solution.py:371
  10.0 3.1 %token_.1 = (bf16[3,16,256]{2,1,0:T(8,128)(2,1)}, bf16[16,16,128]{2,1,0:T(8,128)(2,1)}, f32[16,64]{1,0:T(8,128)}, f32[16,64]{1,0:T(8,128)}, f32[16,64]{1,0:T(8,128)}) custom-call(bf16[12,128,2048]{2,1,0:T(8,128)(2,1)} %refs_0_.3, bf16[64,2048]{1,0:T(8,128)(2,1)} %bitcast.12, bf16[64,2048]{1,0:T(8,128)(2,1)} %bitcast.19, bf16[32,2048]{1,0:T(8,128)(2,1)} %bitcast.15, ...), custom_call_target="tpu_custom_call" | custom-call | tf_op jit(solution)/shard_map/token/pallas_call | solution.py:371
  13.1 74.9 %all-to-all-start = ((bf16[16,16,128]{2,1,0:T(8,128)(2,1)}), bf16[16,16,128]{2,1,0:T(8,128)(2,1)S(1)}, u32[]{:S(2)}, u32[]{:S(2)}) async-start(bf16[16,16,128]{2,1,0:T(8,128)(2,1)} %get-tuple-element.28), calls=%async_computation | async-start | bytes 131072 | tf_op jit(solution)/shard_map/all_to_all | solution.py:499
  88.1 3.1 %collective-permute-start = (bf16[3,16,256]{2,1,0:T(8,128)(2,1)}, bf16[3,16,256]{2,1,0:T(8,128)(2,1)S(1)}, u32[]{:S(2)}, u32[]{:S(2)}) collective-permute-start(bf16[3,16,256]{2,1,0:T(8,128)(2,1)} %get-tuple-element.19), channel_id=1, source_target_pairs={{0,32},{32,64},{64,96},{96,128},{128,160},{160,192},{192,224},{224... | collective-permute-start | bytes 73736 | tf_op jit(solution)/shard_map/ppermute | solution.py:500
  91.1 0.1 late.1
  91.3 1.0 collective-permute-done.halo_ref
  92.3 0.0 copy-start.1
  92.3 7.1 %all-to-all-done.newest_ref = bf16[16,16,128]{2,1,0:T(8,128)(2,1)S(1)} async-done(((bf16[16,16,128]{2,1,0:T(8,128)(2,1)}), bf16[16,16,128]{2,1,0:T(8,128)(2,1)S(1)}, u32[]{:S(2)}, u32[]{:S(2)}) %all-to-all-start) | async-done | bytes 65568 | tf_op jit(solution)/shard_map/all_to_all | solution.py:499
  99.4 0.0 copy-start
  99.4 0.0 copy-done.1
  99.4 0.6 copy-done
  100.0 3.2 %pack.1 = bf16[16,64,128]{2,1,0:T(8,128)(2,1)} custom-call(bf16[3,16,256]{2,1,0:T(8,128)(2,1)} %copy-done.1, f32[3,16,256]{2,1,0:T(8,128)} %get-tuple-element.24.lead_ref, f32[16,128]{1,0:T(8,128)} %get-tuple-element.25.weight_ref, f32[16,128]{1,0:T(8,128)} %get-tuple-element.26.logs_ref, bf16[4,2048]{1,0:T(4,128)(2,1)} %vt_ref.1, bf16[4,256]{1,0:T(4,128)(2,1)} %kt_ref.1, ...), custom_call_target="tpu_custom_call" | custom-call | tf_op jit(solution)/shard_map/pack/pallas_call | solution.py:371
  103.2 18.8 %all_to_all.15.refs_0_ = bf16[16,64,128]{2,1,0:T(8,128)(2,1)} all-to-all(bf16[16,64,128]{2,1,0:T(8,128)(2,1)} %pack.1), channel_id=1, replica_groups=mesh['grp'=2,'sp'=16,'tp_0'=16,'tp_1'=2] {'sp'}, dimensions={0} | all-to-all | bytes 524288 | tf_op jit(solution)/shard_map/all_to_all | solution.py:529
  122.0 2.1 %read.1 = (bf16[48,128]{1,0:T(8,128)(2,1)}, f32[8,128]{1,0:T(8,128)}, f32[32,1,128]{2,1,0:T(1,128)}) custom-call(bf16[16,64,128]{2,1,0:T(8,128)(2,1)} %all_to_all.15.refs_0_, f32[16,64]{1,0:T(8,128)} %get-tuple-element.20.refs_9_.decay_ref.refs_1_, f32[16,64]{1,0:T(8,128)} %get-tuple-element.30.refs_2_), custom_call_target="tpu_custom_call" | custom-call | tf_op jit(solution)/shard_map/read/pallas_call | solution.py:371
  124.1 33.4 %all_to_all.16.parts_ref = f32[32,1,128]{2,1,0:T(1,128)} all-to-all(f32[32,1,128]{2,1,0:T(1,128)} %get-tuple-element.32), channel_id=1, replica_groups=mesh['grp'=2,'sp'=16,'tp_0'=16,'tp_1'=2] {'tp_0','tp_1'}, dimensions={0} | all-to-all | bytes 32768 | tf_op jit(solution)/shard_map/all_to_all | solution.py:543
  157.5 1.4 final.1
Async XLA Ops:
  13.1 86.3 %all-to-all-start = ((bf16[16,16,128]{2,1,0:T(8,128)(2,1)}), bf16[16,16,128]{2,1,0:T(8,128)(2,1)S(1)}, u32[]{:S(2)}, u32[]{:S(2)}) async-start(bf16[16,16,128]{2,1,0:T(8,128)(2,1)} %get-tuple-element.28), calls=%async_computation | async-start | bytes 131072 | tf_op jit(solution)/shard_map/all_to_all | solution.py:499
  88.1 4.2 %collective-permute-start = (bf16[3,16,256]{2,1,0:T(8,128)(2,1)}, bf16[3,16,256]{2,1,0:T(8,128)(2,1)S(1)}, u32[]{:S(2)}, u32[]{:S(2)}) collective-permute-start(bf16[3,16,256]{2,1,0:T(8,128)(2,1)} %get-tuple-element.19), channel_id=1, source_target_pairs={{0,32},{32,64},{64,96},{96,128},{128,160},{160,192},{192,224},{224... | collective-permute-start | bytes 73736 | tf_op jit(solution)/shard_map/ppermute | solution.py:500
  92.3 7.1 %copy-start.1 = (bf16[3,16,256]{2,1,0:T(8,128)(2,1)}, bf16[3,16,256]{2,1,0:T(8,128)(2,1)S(1)}, u32[]{:S(2)}) copy-start(bf16[3,16,256]{2,1,0:T(8,128)(2,1)S(1)} %collective-permute-done.halo_ref) | copy-start | bytes 73732
  99.4 0.6 copy-start

commit v8 on v7

--- a/solution.py
+++ b/solution.py
@@ -248,7 +248,7 @@
     decay_out_ref[...] = jnp.broadcast_to(jnp.exp(-speed * step), decay_out_ref.shape)
     agreement = jnp.sum(new_in * new_out, axis=1, keepdims=True)
     direct_ref[...] = new_input * (step * agreement + pick(skip_ref[...], head))
-    newest = new_out.astype(BF16)
+    newest = new_out[:prompts].astype(BF16)
     for d in range(newest_ref.shape[0]):
         newest_ref[d] = newest
     gate_out_ref[...] = silu(new_gate)
@@ -459,7 +459,7 @@
         token_body,
         [
             out((CONV - 1, padded, 2 * LANES), BF16),
-            out((dests, padded, LANES), BF16),
+            out((dests, prompts, LANES), BF16),
             out((padded, P_SIZE), F32),
             out((padded, P_SIZE), F32),
             out((padded, P_SIZE), F32),

time: 159 us -> 159 us (level)
  no operation moved by 1% of the time
where the time goes in v8:
time: 159 us
  starting transfers between devices  78 us (49%)
  blocking collectives  52.2 us (33%)
  Pallas kernels  19.4 us (12%)
  waiting for transfers between devices  8.11 us (5%)
    all_to_all x1, starting transfers between devices, shards(): newest = lax.all_to_all(newest, 'sp', 0, 0, tiled=True)  74.9 us
    all_to_all x1, blocking collectives, shards(): squares = lax.all_to_all(squares, TP, 0, 0, tiled=True)  33.4 us
    pallas_call x6, Pallas kernels, call(): pl.pallas_call(body, in_specs=specs or whole(len(operands)), out_specs=ou...  19.4 us
    all_to_all x1, blocking collectives, shards(): received = lax.all_to_all(payload, 'sp', 0, 0, tiled=True)  18.8 us
    all_to_all x1, waiting for transfers between devices, shards(): newest = lax.all_to_all(newest, 'sp', 0, 0, tiled=True)  7.13 us
  transfers between devices with their start and end apart: 2, of which 2 were waited for; matrix products, arithmetic and copies ran while one was open for 0% of the time, Pallas kernels for 0%

profile of v8, /device:TPU:5, one launch (start us, length us, event | category | flops | bytes accessed | tf_op | source)
XLA Modules:
  0.0 158.9 jit_solution(7425241747840570086)
XLA Ops:
  0.6 9.3 %early.1 = (f32[12,64,128]{2,1,0:T(8,128)}, f32[3,16,256]{2,1,0:T(8,128)}, f32[16,128]{1,0:T(8,128)}, f32[16,128]{1,0:T(8,128)}) custom-call(bf16[12,128,2048]{2,1,0:T(8,128)(2,1)} %refs_0_.3, bf16[2048,256]{1,0:T(8,128)(2,1)} %refs_1_.3, bf16[64,2048]{1,0:T(8,128)(2,1)} %bitcast.11, bf16[32,2048]{1,0:T(8,128)(2,1)} %bitcast.14, f32[12,32,128]{2,1,0:T(8,128)} %bitcast.17, ...), custom_call_target="tpu_custom_call" | custom-call | tf_op jit(solution)/shard_map/early/pallas_call | solution.py:371
  10.0 3.1 %token_.1 = (bf16[3,16,256]{2,1,0:T(8,128)(2,1)}, bf16[16,12,128]{2,1,0:T(8,128)(2,1)}, f32[16,64]{1,0:T(8,128)}, f32[16,64]{1,0:T(8,128)}, f32[16,64]{1,0:T(8,128)}) custom-call(bf16[12,128,2048]{2,1,0:T(8,128)(2,1)} %refs_0_.3, bf16[64,2048]{1,0:T(8,128)(2,1)} %bitcast.12, bf16[64,2048]{1,0:T(8,128)(2,1)} %bitcast.19, bf16[32,2048]{1,0:T(8,128)(2,1)} %bitcast.15, ...), custom_call_target="tpu_custom_call" | custom-call | tf_op jit(solution)/shard_map/token/pallas_call | solution.py:371
  13.1 74.9 %all-to-all-start = ((bf16[16,12,128]{2,1,0:T(8,128)(2,1)}), bf16[16,12,128]{2,1,0:T(8,128)(2,1)S(1)}, u32[]{:S(2)}, u32[]{:S(2)}) async-start(bf16[16,12,128]{2,1,0:T(8,128)(2,1)} %get-tuple-element.28), calls=%async_computation | async-start | bytes 131072 | tf_op jit(solution)/shard_map/all_to_all | solution.py:499
  88.1 3.1 %collective-permute-start = (bf16[3,16,256]{2,1,0:T(8,128)(2,1)}, bf16[3,16,256]{2,1,0:T(8,128)(2,1)S(1)}, u32[]{:S(2)}, u32[]{:S(2)}) collective-permute-start(bf16[3,16,256]{2,1,0:T(8,128)(2,1)} %get-tuple-element.19), channel_id=1, source_target_pairs={{0,32},{32,64},{64,96},{96,128},{128,160},{160,192},{192,224},{224... | collective-permute-start | bytes 73736 | tf_op jit(solution)/shard_map/ppermute | solution.py:500
  91.1 0.1 late.1
  91.3 1.0 collective-permute-done.halo_ref
  92.3 0.0 copy-start.1
  92.3 7.1 %all-to-all-done.newest_ref = bf16[16,12,128]{2,1,0:T(8,128)(2,1)S(1)} async-done(((bf16[16,12,128]{2,1,0:T(8,128)(2,1)}), bf16[16,12,128]{2,1,0:T(8,128)(2,1)S(1)}, u32[]{:S(2)}, u32[]{:S(2)}) %all-to-all-start) | async-done | bytes 49184 | tf_op jit(solution)/shard_map/all_to_all | solution.py:499
  99.4 0.0 copy-start
  99.4 0.0 copy-done.1
  99.4 0.6 copy-done
  100.0 3.2 %pack.1 = bf16[16,64,128]{2,1,0:T(8,128)(2,1)} custom-call(bf16[3,16,256]{2,1,0:T(8,128)(2,1)} %copy-done.1, f32[3,16,256]{2,1,0:T(8,128)} %get-tuple-element.24.lead_ref, f32[16,128]{1,0:T(8,128)} %get-tuple-element.25.weight_ref, f32[16,128]{1,0:T(8,128)} %get-tuple-element.26.logs_ref, bf16[4,2048]{1,0:T(4,128)(2,1)} %vt_ref.1, bf16[4,256]{1,0:T(4,128)(2,1)} %kt_ref.1, ...), custom_call_target="tpu_custom_call" | custom-call | tf_op jit(solution)/shard_map/pack/pallas_call | solution.py:371
  103.2 18.8 %all_to_all.15.refs_0_ = bf16[16,64,128]{2,1,0:T(8,128)(2,1)} all-to-all(bf16[16,64,128]{2,1,0:T(8,128)(2,1)} %pack.1), channel_id=1, replica_groups=mesh['grp'=2,'sp'=16,'tp_0'=16,'tp_1'=2] {'sp'}, dimensions={0} | all-to-all | bytes 524288 | tf_op jit(solution)/shard_map/all_to_all | solution.py:529
  122.0 2.1 %read.1 = (bf16[48,128]{1,0:T(8,128)(2,1)}, f32[8,128]{1,0:T(8,128)}, f32[32,1,128]{2,1,0:T(1,128)}) custom-call(bf16[16,64,128]{2,1,0:T(8,128)(2,1)} %all_to_all.15.refs_0_, f32[16,64]{1,0:T(8,128)} %get-tuple-element.20.refs_9_.decay_ref.refs_1_, f32[16,64]{1,0:T(8,128)} %get-tuple-element.30.refs_2_), custom_call_target="tpu_custom_call" | custom-call | tf_op jit(solution)/shard_map/read/pallas_call | solution.py:371
  124.1 33.4 %all_to_all.16.parts_ref = f32[32,1,128]{2,1,0:T(1,128)} all-to-all(f32[32,1,128]{2,1,0:T(1,128)} %get-tuple-element.32), channel_id=1, replica_groups=mesh['grp'=2,'sp'=16,'tp_0'=16,'tp_1'=2] {'tp_0','tp_1'}, dimensions={0} | all-to-all | bytes 32768 | tf_op jit(solution)/shard_map/all_to_all | solution.py:543
  157.5 1.4 final.1
Async XLA Ops:
  13.1 86.3 %all-to-all-start = ((bf16[16,12,128]{2,1,0:T(8,128)(2,1)}), bf16[16,12,128]{2,1,0:T(8,128)(2,1)S(1)}, u32[]{:S(2)}, u32[]{:S(2)}) async-start(bf16[16,12,128]{2,1,0:T(8,128)(2,1)} %get-tuple-element.28), calls=%async_computation | async-start | bytes 131072 | tf_op jit(solution)/shard_map/all_to_all | solution.py:499
  88.1 4.2 %collective-permute-start = (bf16[3,16,256]{2,1,0:T(8,128)(2,1)}, bf16[3,16,256]{2,1,0:T(8,128)(2,1)S(1)}, u32[]{:S(2)}, u32[]{:S(2)}) collective-permute-start(bf16[3,16,256]{2,1,0:T(8,128)(2,1)} %get-tuple-element.19), channel_id=1, source_target_pairs={{0,32},{32,64},{64,96},{96,128},{128,160},{160,192},{192,224},{224... | collective-permute-start | bytes 73736 | tf_op jit(solution)/shard_map/ppermute | solution.py:500
  92.3 7.1 %copy-start.1 = (bf16[3,16,256]{2,1,0:T(8,128)(2,1)}, bf16[3,16,256]{2,1,0:T(8,128)(2,1)S(1)}, u32[]{:S(2)}) copy-start(bf16[3,16,256]{2,1,0:T(8,128)(2,1)S(1)} %collective-permute-done.halo_ref) | copy-start | bytes 73732
  99.4 0.6 copy-start
